TPU v7x, 512 devices: a whole 4x8x8 slice. The times are simulated.
512 devices in a mesh: ep: 32 (over z, x), tp: 16 (over y, core).
Axes of the slice: x: 4, y: 8, z: 8, core: 2. Of those that a mesh axis runs over, the one named last changes fastest.
Arguments:
- queries: bfloat16 [24576, 1024], P('ep', 'tp'), may hold values from -6.5 to 6.5
- keys: bfloat16 [24576, 1024], P('ep', 'tp'), may hold values from -6.5 to 6.5
- values: bfloat16 [24576, 1024], P('ep', 'tp'), may hold values from -6 to 6
- cum_gate: float32 [24576, 16], P('ep', 'tp'), may hold values from -3074 to 0, as said below
- head_gain: float32 [1024], P('tp'), may hold values from 0.1 to 1.9
- moe_in: bfloat16 [4096, 2048], P('ep'), may hold values from -6 to 6
- ffn_gain: float32 [2048], replicated, may hold values from 0.1 to 1.9
- routes: int32 [4096, 4], P('ep'), may hold values from 0 to 127, all different within a row; in each aligned block of 128 rows (0 to 127, 128 to 255, ...) at most 6 rows name the same one
- route_weight: float32 [4096, 4], P('ep'), may hold values from 0.2 to 1.2
- expert_gate: bfloat16 [128, 1024, 2048], P('ep', 'tp'), may hold values from -0.125 to 0.125
- expert_up: bfloat16 [128, 1024, 2048], P('ep', 'tp'), may hold values from -0.125 to 0.125
- expert_down: bfloat16 [128, 1024, 2048], P('ep', 'tp'), may hold values from -0.25 to 0.25
- shared_gate: bfloat16 [512, 2048], P('tp'), may hold values from -0.125 to 0.125
- shared_up: bfloat16 [512, 2048], P('tp'), may hold values from -0.125 to 0.125
- shared_down: bfloat16 [512, 2048], P('tp'), may hold values from -0.375 to 0.375
Outputs:
- mixed: bfloat16 [24576, 1024], P('ep', 'tp')
- expert_out: bfloat16 [4096, 2048], P('ep', 'tp')
Inputs may be any that keep to these rules, and one draw needn't show every extreme that they name: `routes`: in each aligned block of 128 rows (the tokens of one index of ep) no expert is named by more than 6 rows, a bound that some block reaches; a row names 4 different experts. Each head's cum_gate never rises from one position to the next.
All inputs are finite; a program needn't handle non-finite values.
Results may differ from a plain program's by a relative error of at most 0.019.
Values may be sent and summed in bfloat16 or wider, within the bound.
No kernel may reach another device: no remote copies, remote signals or barrier semaphores. Data moves between devices by JAX's collectives and lax.ppermute only.
A program may use at most 128 MiB of HBM per device.

v0:
```python
import math

import jax
import jax.numpy as jnp
from jax import lax
from jax.sharding import PartitionSpec as P

NORM_EPSILON = 1e-06


def joined_along(parts, dim):
    lengths = list(parts.shape[1:])
    lengths[dim] *= parts.shape[0]
    return jnp.moveaxis(parts, 0, dim).reshape(lengths)


def sent_to_all(shard, axis):
    length = lax.axis_size(axis)
    return lax.all_to_all(
        jnp.broadcast_to(shard[None], (length, *shard.shape)), axis, 0, 0, tiled=True
    )


def gather_directly(shard, axis, dim):
    return joined_along(sent_to_all(shard, axis), dim)


def in_one_piece(arrays, axis, dim, along):
    ends, at = ([], 0)
    for a in arrays[:-1]:
        at += a.shape[along]
        ends.append(at)
    both = jnp.concatenate(arrays, axis=along)
    return tuple(jnp.split(lax.all_gather(both, axis, axis=dim, tiled=True), ends, axis=along))


def keep_same(state_pair):
    return state_pair


def attend(queries, keys, values, cum_gate, head_gain):
    row_count, head_width = queries.shape
    head_count = cum_gate.shape[1]
    head_size = head_width // head_count
    score_scale = head_size ** (-0.5)
    first_row = lax.axis_index("ep") * row_count
    last_row = first_row + row_count - 1
    query_heads = queries.reshape(row_count, head_count, head_size)
    query_pos = first_row + jnp.arange(row_count, dtype=jnp.int32)
    query_gate = cum_gate.T
    all_gates = gather_directly(cum_gate, "ep", 0)
    start_state = (
        jnp.full((head_count, row_count), -1e30, jnp.float32),
        jnp.zeros((row_count, head_count, head_size), jnp.float32),
    )
    key_piece, value_piece = in_one_piece((keys, values), "ep", 0, 1)
    piece_len = key_piece.shape[0]
    block_len = math.gcd(piece_len, 512)

    def visit(block_num, state_pair):
        offset = block_num * block_len

        def update(pair_in):
            running, weighted = pair_in
            key_block = lax.dynamic_slice_in_dim(key_piece, offset, block_len, 0).reshape(
                block_len, head_count, head_size
            )
            value_block = lax.dynamic_slice_in_dim(value_piece, offset, block_len, 0).reshape(
                block_len, head_count, head_size
            )
            key_gate = lax.dynamic_slice_in_dim(all_gates, offset, block_len, 0).T
            key_pos = offset + jnp.arange(block_len, dtype=jnp.int32)
            scores = (
                jnp.einsum(
                    "qhd,khd->hqk", query_heads, key_block, preferred_element_type=jnp.float32
                )
                * score_scale
            )
            scores = scores + query_gate[:, :, None] - key_gate[:, None, :]
            scores = jnp.where(key_pos[None, None, :] <= query_pos[None, :, None], scores, -jnp.inf)
            new_peak = jnp.maximum(running, jnp.max(scores, axis=2))
            weights = jnp.exp(scores - new_peak[:, :, None]).astype(jnp.bfloat16)
            shrink = jnp.exp(running - new_peak).T
            weighted = weighted * shrink[:, :, None] + jnp.einsum(
                "hqk,khd->qhd", weights, value_block, preferred_element_type=jnp.float32
            )
            return (new_peak, weighted)

        return lax.cond(offset <= last_row, update, keep_same, state_pair)

    running, weighted = lax.fori_loop(0, piece_len // block_len, visit, start_state)
    mean_square = jnp.mean(weighted * weighted, axis=2, keepdims=True)
    normed = (
        weighted * lax.rsqrt(mean_square + NORM_EPSILON) * head_gain.reshape(head_count, head_size)
    )
    return normed.reshape(row_count, head_width).astype(jnp.bfloat16)


def slot_index(route_rows, experts, capacity):
    flat_routes = route_rows.reshape(-1)
    agreement_tally = (
        flat_routes[:, None] == jnp.arange(experts, dtype=jnp.int32)[None, :]
    ).astype(jnp.int32)
    earlier = jnp.sum((jnp.cumsum(agreement_tally, axis=0) - 1) * agreement_tally, axis=1)
    return flat_routes * capacity + earlier


def experts_half(
    moe_in,
    ffn_gain,
    routes,
    route_weight,
    expert_gate,
    expert_up,
    expert_down,
    shared_gate,
    shared_up,
    shared_down,
):
    tokens, model_width = moe_in.shape
    choose = routes.shape[1]
    per_group = expert_gate.shape[0]
    groups = lax.axis_size("ep")
    experts = per_group * groups
    capacity = max(2, 3 * tokens * choose // (2 * experts))
    slice_width = model_width // lax.axis_size("tp")
    source = moe_in.astype(jnp.float32)
    normed = (
        source
        * lax.rsqrt(jnp.mean(source * source, axis=1, keepdims=True) + NORM_EPSILON)
        * ffn_gain
    ).astype(jnp.bfloat16)
    shared_hidden = (
        jax.nn.silu(
            jnp.einsum("td,fd->tf", normed, shared_gate, preferred_element_type=jnp.float32)
        )
        * jnp.einsum("td,fd->tf", normed, shared_up, preferred_element_type=jnp.float32)
    ).astype(jnp.bfloat16)
    shared_term = jnp.dot(shared_hidden, shared_down, preferred_element_type=jnp.float32)
    slot_ids = slot_index(routes, experts, capacity)
    owner_row = (
        jnp.full((experts * capacity,), tokens, jnp.int32)
        .at[slot_ids]
        .set(jnp.arange(tokens * choose, dtype=jnp.int32) // choose)
    )
    padded = jnp.concatenate([normed, jnp.zeros((1, model_width), normed.dtype)], axis=0)
    arrived = lax.all_to_all(padded[owner_row], "ep", split_axis=0, concat_axis=0, tiled=True)
    arranged = arrived.reshape(groups, per_group, capacity, model_width)
    gate_value = jnp.einsum(
        "slcd,lfd->slcf", arranged, expert_gate, preferred_element_type=jnp.float32
    )
    up_value = jnp.einsum("slcd,lfd->slcf", arranged, expert_up, preferred_element_type=jnp.float32)
    hidden = (jax.nn.silu(gate_value) * up_value).astype(jnp.bfloat16)
    expert_term = jnp.einsum(
        "slcf,lfd->slcd", hidden, expert_down, preferred_element_type=jnp.float32
    ).reshape(groups * per_group * capacity, model_width)
    expert_sum, shared_sum = (
        lax.psum_scatter(
            expert_term.astype(jnp.bfloat16), "tp", scatter_dimension=1, tiled=True
        ).astype(jnp.float32),
        lax.psum_scatter(
            shared_term.astype(jnp.bfloat16), "tp", scatter_dimension=1, tiled=True
        ).astype(jnp.float32),
    )
    returned = lax.all_to_all(
        expert_sum.astype(jnp.bfloat16), "ep", split_axis=0, concat_axis=0, tiled=True
    )
    picked = returned[slot_ids].reshape(tokens, choose, slice_width).astype(jnp.float32)
    routed = jnp.sum(picked * route_weight[:, :, None], axis=1)
    return (shared_sum + routed).astype(jnp.bfloat16)


def on_device(
    queries,
    keys,
    values,
    cum_gate,
    head_gain,
    moe_in,
    ffn_gain,
    routes,
    route_weight,
    expert_gate,
    expert_up,
    expert_down,
    shared_gate,
    shared_up,
    shared_down,
):
    mixed = attend(queries, keys, values, cum_gate, head_gain)
    expert_out = experts_half(
        moe_in,
        ffn_gain,
        routes,
        route_weight,
        expert_gate,
        expert_up,
        expert_down,
        shared_gate,
        shared_up,
        shared_down,
    )
    return (mixed, expert_out)


def solution(mesh):
    in_specs = (
        P("ep", "tp"),
        P("ep", "tp"),
        P("ep", "tp"),
        P("ep", "tp"),
        P("tp"),
        P("ep", None),
        P(),
        P("ep", None),
        P("ep", None),
        P("ep", "tp", None),
        P("ep", "tp", None),
        P("ep", "tp", None),
        P("tp", None),
        P("tp", None),
        P("tp", None),
    )
    out_specs = (P("ep", "tp"), P("ep", "tp"))
    return jax.shard_map(
        on_device, mesh=mesh, in_specs=in_specs, out_specs=out_specs, check_vma=False
    )
```

profile of v0, /device:TPU:32, one launch (start us, length us, event | category | flops | bytes accessed | tf_op | source)
XLA Modules:
  0.0 345.4 jit_solution(4772509628623454861)
XLA Ops:
  8.0 0.0 copy-start
  8.0 0.0 reduce-scatter.7.cloned.1.call-start
  8.1 1.3 fusion.13
  9.4 1.2 fusion.15
  10.7 1.2 fusion.47
  11.8 1.8 convolution_convert_fusion.1
  13.6 1.0 copy.45
  14.6 0.0 reduce-scatter.7.cloned.1.call-update
  14.7 0.0 all-gather.2.cloned.1.call-start
  14.7 0.2 copy.32
  14.9 0.2 copy.33
  15.1 0.8 pad_maximum_fusion
  15.9 0.0 all-gather.2.cloned.1.call-update
  15.9 0.0 reduce-scatter.9.cloned.1.call-start
  16.0 0.1 copy.35
  16.1 0.1 eq.29
  16.2 0.1 eq.25
  16.3 0.1 copy.37
  16.4 0.2 fusion.27
  16.7 0.1 add_add_fusion
  16.8 0.1 copy.34
  16.9 0.1 mul.119
  17.0 0.1 concatenate.7
  17.1 0.2 fusion.26
  17.3 2.4 scatter_custom_fusion
  19.8 4.4 %gather_fusion = bf16[768,2048]{1,0:T(8,128)(2,1)} fusion(bf16[129,2048]{1,0:T(8,128)(2,1)S(1)} %concatenate.7, s32[1024]{0:T(1024)S(1)} %pad_clamp_fusion.1), kind=kCustom, calls=%fused_computation | custom fusion | bytes 6294528 | tf_op jit(solution)/shard_map/gather | solution.py:147
  24.2 107.7 %all_to_all.26 = bf16[32,24,2048]{2,1,0:T(8,128)(2,1)S(1)} all-to-all(bf16[32,24,2048]{2,1,0:T(8,128)(2,1)} %bitcast.76), channel_id=1, replica_groups=mesh['ep'=32,'tp'=16] {'ep'}, dimensions={0} | all-to-all | bytes 6291456 | tf_op jit(solution)/shard_map/all_to_all | solution.py:147
  131.8 1.7 copy.39
  133.6 1.7 copy-done.1
  135.3 1.0 convolution_bitcast_fusion.2
  136.3 0.2 copy-done.2
  136.5 5.5 %fusion.9 = bf16[32,4,6,2048]{3,0,2,1:T(8,128)(2,1)} fusion(bf16[32,4,6,2048]{3,0,2,1:T(8,128)(2,1)} %bitcast.75, bf16[4,64,2048]{2,1,0:T(8,128)(2,1)S(1)} %copy-done, bf16[4,64,2048]{2,1,0:T(8,128)(2,1)S(1)} %copy-done.2, f32[32,4,6,64]{3,0,2,1:T(8,128)S(1)} %convolution_bitcast_fusion.2), kind=kOutput, calls=%fused_computation.20 | convolution fusion | flops 404520960 | bytes 8585216 | tf_op jit(solution)/shard_map/slcf,lfd->slcd/dot_general | solution.py:154
  142.0 5.7 %copy.40 = bf16[32,4,6,2048]{3,2,1,0:T(8,128)(2,1)} copy(bf16[32,4,6,2048]{3,0,2,1:T(8,128)(2,1)} %fusion.9) | data formatting | bytes 6291456 | tf_op jit(solution)/shard_map/convert_element_type | solution.py:159
  147.6 6.3 %convert_element_type.71 = bf16[768,2048]{1,0:T(8,128)(2,1)} reshape(bf16[32,4,6,2048]{3,2,1,0:T(8,128)(2,1)} %copy.40) | data formatting | bytes 6291456 | tf_op jit(solution)/shard_map/convert_element_type | solution.py:159
  154.0 4.7 %copy.47 = bf16[768,2048]{0,1:T(8,128)(2,1)} copy(bf16[768,2048]{1,0:T(8,128)(2,1)} %convert_element_type.71) | data formatting | bytes 6291456
  158.6 0.0 reduce-scatter.9.cloned.1.call-update
  158.7 0.7 copy-done.3
  159.3 0.7 broadcast_in_dim.22
  160.0 5.5 %all-to-all-start = ((f32[32,768,1]{1,2,0:T(1,128)}), f32[32,768,1]{1,2,0:T(1,128)S(1)}, u32[]{:S(2)}, u32[]{:S(2)}) async-start(f32[32,768,1]{1,2,0:T(1,128)} %broadcast_in_dim.22), calls=%async_computation | async-start | bytes 196608 | tf_op jit(solution)/shard_map/all_to_all | solution.py:19
  165.5 0.0 copy-done.7
  165.5 0.1 copy.41
  165.7 0.0 reduce-scatter.7.cloned.1.call-done
  165.7 0.9 copy.46
  166.6 0.0 copy-start.10
  166.6 0.0 all-gather.2.cloned.1.call-done
  166.6 12.0 %fusion.46 = (bf16[24576,64]{1,0:T(8,128)(2,1)}, bf16[24576,64]{1,0:T(8,128)(2,1)}) fusion(bf16[24576,128]{1,0:T(8,128)(2,1)} %all-gather.2.cloned.1.call-done), kind=kLoop, calls=%fused_computation.83 | loop fusion | bytes 12582912 | tf_op jit(solution)/shard_map/split | solution.py:34
  178.7 0.0 all-to-all-done
  178.7 0.0 copy-start.8
  178.7 8.2 %while.16 = (s32[]{:T(128)}, f32[1,768]{1,0:T(1,128)S(1)}, f32[768,1,64]{0,2,1:T(8,128)S(1)}, s32[]{:T(128)}, bf16[24576,64]{1,0:T(8,128)(2,1)}, /*index=5*/bf16...) while((s32[]{:T(128)}, f32[1,768]{1,0:T(1,128)S(1)}, ...), condition=%wide.region_4.5_spmd.clone, body=%wide.region_0.4_spmd.clone.sunk | while | flops 103909376 | bytes 3956033 | solution.py:91
  178.7 2.8 conditional.3
  178.8 1.4 fusion.45
  180.2 1.3 fusion.2
  181.6 2.8 conditional.3
  181.7 1.4 fusion.45
  183.1 1.3 fusion.2
  187.0 30.1 %reduce-scatter.9.cloned.1.call-done = bf16[128,768]{1,0:T(8,128)(2,1)} async-done(((bf16[2048,768]{1,0:T(8,128)(2,1)}), bf16[128,768]{1,0:T(8,128)(2,1)}) %reduce-scatter.9.cloned.1.call-update) | async-done | bytes 196624
  217.1 1.7 copy.48
  218.8 106.1 %all-to-all-start.2 = ((bf16[32,24,128]{2,1,0:T(8,128)(2,1)}), bf16[32,24,128]{2,1,0:T(8,128)(2,1)S(1)}, u32[]{:S(2)}, u32[]{:S(2)}) async-start(bf16[32,24,128]{2,1,0:T(8,128)(2,1)} %bitcast.24), calls=%async_computation.2 | async-start | bytes 393216 | tf_op jit(solution)/shard_map/all_to_all | solution.py:165
  324.9 0.0 copy-done.8
  324.9 0.7 fusion.31
  325.6 10.2 %all-to-all-done.2 = bf16[32,24,128]{2,1,0:T(8,128)(2,1)S(1)} async-done(((bf16[32,24,128]{2,1,0:T(8,128)(2,1)}), bf16[32,24,128]{2,1,0:T(8,128)(2,1)S(1)}, u32[]{:S(2)}, u32[]{:S(2)}) %all-to-all-start.2) | async-done | bytes 196640 | tf_op jit(solution)/shard_map/all_to_all | solution.py:165
  335.8 1.3 gather_fusion.1
  337.1 0.2 fusion.25
  337.4 0.6 add_convert_fusion
  (134 shorter events, 1.0 us)
Async XLA Ops:
  8.0 128.2 %copy-start = (bf16[4,64,2048]{2,1,0:T(8,128)(2,1)S(1)}, bf16[4,64,2048]{2,1,0:T(8,128)(2,1)}, u32[]{:S(2)}) copy-start(bf16[4,64,2048]{2,1,0:T(8,128)(2,1)} %param.30) | copy-start | bytes 3145732
  8.0 6.7 %copy-start.4 = (bf16[768,64]{0,1:T(8,128)(2,1)S(1)}, bf16[768,64]{0,1:T(8,128)(2,1)}, u32[]{:S(2)}) copy-start(bf16[768,64]{0,1:T(8,128)(2,1)} %param.20) | copy-start | bytes 294916
  8.0 6.9 %copy-start.5 = (bf16[768,64]{0,1:T(8,128)(2,1)S(1)}, bf16[768,64]{0,1:T(8,128)(2,1)}, u32[]{:S(2)}) copy-start(bf16[768,64]{0,1:T(8,128)(2,1)} %param.21) | copy-start | bytes 294916
  8.0 7.9 %copy-start.6 = (s32[128,4]{0,1:T(4,128)S(1)}, s32[128,4]{0,1:T(4,128)}, u32[]{:S(2)}) copy-start(s32[128,4]{0,1:T(4,128)} %param.26) | copy-start | bytes 6148
  8.0 157.7 %reduce-scatter.7.cloned.1.call-start = ((), (), s32[]{:S(2)}) async-start(), calls=%async_computation.6 | async-start | bytes 557056
  14.7 151.9 %all-gather.2.cloned.1.call-start = ((), (), s32[]{:S(2)}) async-start(), calls=%async_computation.5 | async-start | bytes 6488064 | tf_op jit(solution)/shard_map/all_gather | solution.py:34
  15.9 201.2 %reduce-scatter.9.cloned.1.call-start = ((), (), s32[]{:S(2)}) async-start(), calls=%async_computation.7 | async-start | bytes 3342336
  131.8 3.4 copy-start.9
  133.6 1.7 copy-start.1
  135.3 1.2 copy-start.2
  158.6 0.7 copy-start.3
  158.6 6.9 %copy-start.7 = (f32[128,4]{0,1:T(4,128)S(1)}, f32[128,4]{0,1:T(4,128)}, u32[]{:S(2)}) copy-start(f32[128,4]{0,1:T(4,128)} %param.27) | copy-start | bytes 6148
  160.0 18.6 %all-to-all-start = ((f32[32,768,1]{1,2,0:T(1,128)}), f32[32,768,1]{1,2,0:T(1,128)S(1)}, u32[]{:S(2)}, u32[]{:S(2)}) async-start(f32[32,768,1]{1,2,0:T(1,128)} %broadcast_in_dim.22), calls=%async_computation | async-start | bytes 196608 | tf_op jit(solution)/shard_map/all_to_all | solution.py:19
  166.6 12.1 %copy-start.10 = (bf16[768,64]{0,1:T(8,128)(2,1)S(1)}, bf16[768,64]{0,1:T(8,128)(2,1)}, u32[]{:S(2)}) copy-start(bf16[768,64]{0,1:T(8,128)(2,1)} %param.19) | copy-start | bytes 294916
  178.7 146.2 %copy-start.8 = (f32[64]{0:T(128)S(1)}, f32[64]{0:T(128)}, u32[]{:S(2)}) copy-start(f32[64]{0:T(128)} %param.23) | copy-start | bytes 772
  218.8 117.0 %all-to-all-start.2 = ((bf16[32,24,128]{2,1,0:T(8,128)(2,1)}), bf16[32,24,128]{2,1,0:T(8,128)(2,1)S(1)}, u32[]{:S(2)}, u32[]{:S(2)}) async-start(bf16[32,24,128]{2,1,0:T(8,128)(2,1)} %bitcast.24), calls=%async_computation.2 | async-start | bytes 393216 | tf_op jit(solution)/shard_map/all_to_all | solution.py:165
Sparse Core Ops, SparseCore 0:
  14.8 63.3 reduce-scatter.6
  158.8 58.2 reduce-scatter.8
Sparse Core Ops, SparseCore 1:
  18.3 127.3 all-gather.1
where the time goes:
time: 348 us; the launch traced here: 345 us
  starting transfers between devices  112 us (32%)
  blocking collectives  108 us (31%)
  local copies, waits for them, and re-layouts  46.8 us (13%)
  waiting for transfers between devices  40.4 us (12%)
  between operations  15.8 us (5%)
  matrix products  14.8 us (4%)
  other arithmetic  5.67 us (2%)
    all_to_all x1, blocking collectives, experts_half(): lax.all_to_all(padded[owner_row], 'ep', split_axis=0, concat_axis=0, tile...  108 us
    all_to_all x1, starting transfers between devices, experts_half(): lax.all_to_all(expert_sum.astype(jnp.bfloat16), 'ep', split_axis=0, conca...  106 us
    unnamed x5, waiting for transfers between devices  30.2 us
    split x1, local copies, waits for them, and re-layouts, in_one_piece(): jnp.split(lax.all_gather(both, axis, axis=dim, tiled=True), ends, axis=al...  12 us
    convert_element_type x2, local copies, waits for them, and re-layouts, experts_half(): expert_term.astype(jnp.bfloat16)  12 us
    unnamed x30, local copies, waits for them, and re-layouts  11.5 us
    all_to_all x1, waiting for transfers between devices, experts_half(): lax.all_to_all(expert_sum.astype(jnp.bfloat16), 'ep', split_axis=0, conca...  10.2 us
  transfers between devices with their start and end apart: 5, of which 2 were waited for; matrix products, arithmetic and copies ran while one was open for 16% of the time, Pallas kernels for 0%

commit v1 on v0

v1 whole, which is shorter than its diff:
```python
import functools

import jax
import jax.numpy as jnp
import numpy as np
from jax import lax
from jax.experimental import pallas as pl
from jax.experimental.pallas import tpu as pltpu
from jax.sharding import Mesh
from jax.sharding import PartitionSpec as P


NORM_EPSILON = 1e-06
LOG2E = 1.4426950408889634
NEG = -1e30
NZ, NX, NY, NC = 8, 4, 8, 2
N_EP = NZ * NX
ROWS = 768
HEAD = 64
D = 2048
TOK = 128
CAP = 6
LOCAL = 2
SLOTS = N_EP * LOCAL * CAP
KG = HEAD + 16
KVG = KG + HEAD
F32 = jnp.float32
BF16 = jnp.bfloat16


def wide_slots():
    s = np.arange(2 * SLOTS)
    e, h, j = s // 24, (s % 24) // 12, s % 12
    return e, h, j // CAP, j % CAP


def slot_table():
    e, h, l, p = wide_slots()
    table = np.zeros((2 * SLOTS, 8), np.int32)
    table[:, 0] = 4 * e + l
    table[:, 1] = p
    table[:, 2] = h
    table[:, 3] = l * (SLOTS // 2) + e * CAP + p
    return table


def source_table():
    r = np.arange(SLOTS)
    l, e, p = r // (SLOTS // 2), (r % (SLOTS // 2)) // CAP, r % CAP
    table = np.zeros((SLOTS, 8), np.int32)
    table[:, 0] = e * 24 + l * CAP + p
    table[:, 1] = table[:, 0] + 12
    return table


def dot(a, b):
    return jnp.dot(a, b, preferred_element_type=F32)


def dot_t(a, b):
    return lax.dot_general(a, b, (((1,), (1,)), ((), ())), preferred_element_type=F32)


def three_pieces(v):
    hi = v.astype(BF16)
    rest = v - hi.astype(F32)
    mid = rest.astype(BF16)
    lo = (rest - mid.astype(F32)).astype(BF16)
    return hi, mid, lo


def call(body, out_shape, scalars, grid, in_specs, out_specs, args, scratch=(), flops=0, aliases=None):
    return pl.pallas_call(
        body,
        out_shape=out_shape,
        grid_spec=pltpu.PrefetchScalarGridSpec(
            num_scalar_prefetch=1,
            grid=grid,
            in_specs=in_specs,
            out_specs=out_specs,
            scratch_shapes=list(scratch),
        ),
        compiler_params=pltpu.CompilerParams(
            dimension_semantics=("arbitrary",) * len(grid), vmem_limit_bytes=56 * 2**20
        ),
        input_output_aliases=aliases or {},
        cost_estimate=pl.CostEstimate(flops=flops, bytes_accessed=4 << 20, transcendentals=0),
    )(scalars, *args)


def whole(shape):
    return pl.BlockSpec(shape, lambda i, s: (0,) * len(shape))


UNREAD = pl.BlockSpec(memory_space=pl.ANY)


def pack_body(ids, k_ref, v_ref, g_ref, out_ref):
    out_ref[0:HEAD, :] = k_ref[...]
    out_ref[KG:KVG, :] = v_ref[...]
    hi, mid, lo = three_pieces(g_ref[...] * (-LOG2E))
    row = lax.broadcasted_iota(jnp.int32, (16, ROWS), 0)
    zero = jnp.zeros((16, ROWS), F32)
    pieces = jnp.where(
        row == 0,
        hi.astype(F32),
        jnp.where(row == 1, mid.astype(F32), jnp.where(row == 2, lo.astype(F32), zero)),
    )
    out_ref[HEAD:KG, :] = pieces.astype(BF16)


def trade_body(ids, gate_ref, up_ref, down_ref, sgate_ref, sup_ref, sdown_ref, after_ref, out_ref):
    for i, ref in enumerate((gate_ref, up_ref, down_ref)):
        for l in range(LOCAL):
            out_ref[i * 128 + l * 64 : i * 128 + l * 64 + 64, :] = ref[l]
    for i, ref in enumerate((sgate_ref, sup_ref, sdown_ref)):
        out_ref[384 + i * 32 : 416 + i * 32, :] = ref[...]


QT = 384
DEPTH = 2 * HEAD + 16


def attend_body(turns, ids, q0_ref, q1_ref, kvg_ref, out0_ref, out1_ref, ka_ref):
    z, x = ids[0], ids[1]
    step = pl.program_id(0)
    per = ROWS // QT
    early = step < per
    sub = lax.rem(step, per)
    xq = lax.rem(x + jnp.where(early, turns[0], turns[1]), NX)

    @pl.when(step == 0)
    def _():
        ka_ref[:, 0:HEAD, :] = kvg_ref[:, 0:HEAD, :]
        ka_ref[:, HEAD:DEPTH, :] = kvg_ref[:, 0:KG, :]

    q0, q1 = q0_ref[...].astype(F32), q1_ref[...].astype(F32)
    scaled = jnp.where(early, q0, q1).T * (0.125 * LOG2E)
    hi = scaled.astype(BF16)
    lo = (scaled - hi.astype(F32)).astype(BF16)
    qa = jnp.concatenate([hi, lo, jnp.ones((QT, 16), BF16)], axis=1)

    def update(chunk, carry, masked):
        peak, acc = carry
        s = dot(qa, ka_ref[chunk])
        if masked:
            row = lax.broadcasted_iota(jnp.int32, (QT, ROWS), 0) + sub * QT
            col = lax.broadcasted_iota(jnp.int32, (QT, ROWS), 1)
            s = jnp.where(col <= row, s, NEG)
        new_peak = jnp.maximum(peak, jnp.max(s, axis=1, keepdims=True))
        w = jnp.exp2(s - new_peak).astype(BF16)
        acc = acc * jnp.exp2(peak - new_peak) + dot_t(w, kvg_ref[chunk, KG:KVG, :])
        return new_peak, acc

    start = (jnp.full((QT, 1), NEG, F32), jnp.zeros((QT, HEAD), F32))
    full = jnp.where(xq > x, z + 1, z)
    carry = lax.fori_loop(0, full, lambda i, c: update(i, c, False), start)
    peak, acc = lax.cond(xq == x, lambda c: update(z, c, True), lambda c: c, carry)
    p_hi, p_mid, p_lo = three_pieces(peak)
    lane = lax.broadcasted_iota(jnp.int32, (QT, HEAD), 1)
    tail = jnp.where(
        lane == 0,
        p_hi.astype(F32),
        jnp.where(
            lane == 1, p_mid.astype(F32), jnp.where(lane == 2, p_lo.astype(F32), jnp.zeros((), F32))
        ),
    )
    out = jnp.concatenate([acc, tail], axis=1).astype(BF16)
    at = pl.ds(pl.multiple_of(sub * QT, QT), QT)

    @pl.when(early)
    def _():
        out0_ref[at, :] = out

    @pl.when(jnp.logical_not(early))
    def _():
        out1_ref[at, :] = out


def combine_body(ids, gain_ref, *refs):
    out_ref, parts = refs[-1], refs[:-1]
    peaks = []
    for ref in parts:
        tail = ref[:, HEAD : HEAD + 3].astype(F32)
        peaks.append(tail[:, 0:1] + tail[:, 1:2] + tail[:, 2:3])
    top = jnp.maximum(jnp.maximum(peaks[0], peaks[1]), jnp.maximum(peaks[2], peaks[3]))
    total = jnp.zeros((ROWS, HEAD), F32)
    for ref, peak in zip(parts, peaks):
        total = total + ref[:, 0:HEAD].astype(F32) * jnp.exp2(peak - top)
    mean_square = jnp.mean(total * total, axis=1, keepdims=True)
    out = total * lax.rsqrt(mean_square + NORM_EPSILON) * gain_ref[...]
    out_ref[...] = out.T.astype(BF16)


def dispatch_body(ids, x_ref, gain_ref, routes_ref, table_ref, after_ref, normed_ref, send_ref):
    c = ids[2]
    x = x_ref[...].astype(F32)
    mean_square = jnp.mean(x * x, axis=1, keepdims=True)
    normed = (x * lax.rsqrt(mean_square + NORM_EPSILON) * gain_ref[...]).astype(BF16)
    normed_ref[...] = normed
    expert = table_ref[:, 0:1] + 2 * c
    member = jnp.zeros((2 * SLOTS, TOK), F32)
    for k in range(4):
        member = jnp.where(routes_ref[k : k + 1, :] == expert, 1.0, member)
    before = lax.broadcasted_iota(jnp.int32, (TOK, TOK), 0)
    after = lax.broadcasted_iota(jnp.int32, (TOK, TOK), 1)
    earlier = jnp.where(before < after, 1.0, 0.0).astype(BF16)
    rank = dot(member.astype(BF16), earlier)
    pick = jnp.where(rank == table_ref[:, 1:2].astype(F32), member, 0.0)
    half = table_ref[:, 2:3]
    first = jnp.where(half == 0, pick, 0.0).astype(BF16)
    second = jnp.where(half == 1, pick, 0.0).astype(BF16)
    send_ref[...] = (dot(first, normed[:, : D // 2]) + dot(second, normed[:, D // 2 :])).astype(
        BF16
    )


def split_down_body(ids, own_ref, got_ref, shared_ref, *outs):
    for turn, out_ref in enumerate(outs):
        to = lax.rem(ids[3] + turn, NY)
        cols = pl.ds(pl.multiple_of(to * 256, 256), 256)
        for l in range(LOCAL):
            out_ref[l * 128 : l * 128 + 64, :] = own_ref[l, :, cols]
            out_ref[l * 128 + 64 : l * 128 + 128, :] = got_ref[256 + l * 64 : 320 + l * 64, cols]
        out_ref[256:288, :] = shared_ref[:, cols]
        out_ref[288:320, :] = got_ref[448:480, cols]


def gated(g, u):
    return g / (1.0 + jnp.exp(-g)) * u


def hidden_body(
    ids, x_ref, gate_ref, up_ref, got_ref, normed_ref, sgate_ref, sup_ref, source_ref, out_ref
):
    c = ids[2]
    x = x_ref[...]
    lane = lax.broadcasted_iota(jnp.int32, (SLOTS, 2 * SLOTS), 1)
    x0 = dot(jnp.where(lane == source_ref[:, 0:1], 1.0, 0.0).astype(BF16), x).astype(BF16)
    x1 = dot(jnp.where(lane == source_ref[:, 1:2], 1.0, 0.0).astype(BF16), x).astype(BF16)
    n = SLOTS // 2
    for l in range(LOCAL):
        rows0, rows1 = x0[l * n : (l + 1) * n], x1[l * n : (l + 1) * n]
        wg = jnp.concatenate([gate_ref[l], got_ref[l * 64 : l * 64 + 64, :]], axis=0)
        wu = jnp.concatenate([up_ref[l], got_ref[128 + l * 64 : 128 + l * 64 + 64, :]], axis=0)
        g = dot_t(rows0, wg[:, : D // 2]) + dot_t(rows1, wg[:, D // 2 :])
        u = dot_t(rows0, wu[:, : D // 2]) + dot_t(rows1, wu[:, D // 2 :])
        h = gated(g, u).astype(BF16)
        for y in range(NY):
            out_ref[y, l * n : (l + 1) * n, :] = h
    tokens = normed_ref[pl.ds(pl.multiple_of(c * 64, 64), 64), :]
    wg = jnp.concatenate([sgate_ref[...], got_ref[384:416, :]], axis=0)
    wu = jnp.concatenate([sup_ref[...], got_ref[416:448, :]], axis=0)
    h = gated(dot_t(tokens, wg), dot_t(tokens, wu))
    h = jnp.concatenate([h, jnp.zeros((64, 64), F32)], axis=1).astype(BF16)
    for y in range(NY):
        out_ref[y, SLOTS : SLOTS + 64, :] = h


def down_body(ids, h_ref, table_ref, *rest):
    weights, (out_ref, shared_ref) = rest[:NY], rest[NY:]
    n = SLOTS // 2
    rows = [jnp.zeros((n, 256), F32) for _ in range(LOCAL)]
    shared = jnp.zeros((64, 256), F32)
    for turn, w_ref in enumerate(weights):
        y = lax.rem(ids[3] + NY - turn, NY)
        h = h_ref[y]
        for l in range(LOCAL):
            rows[l] = rows[l] + dot(h[l * n : (l + 1) * n], w_ref[l * 128 : l * 128 + 128, :])
        shared = shared + dot(h[SLOTS : SLOTS + 64, 0:64], w_ref[256:320, :])
    rows = [r.astype(BF16) for r in rows]
    shared_ref[...] = shared
    rows = jnp.concatenate(rows, axis=0)
    lane = lax.broadcasted_iota(jnp.int32, (2 * SLOTS, SLOTS), 1)
    place = jnp.where(lane == table_ref[:, 3:4], 1.0, 0.0)
    half = table_ref[:, 2:3]
    first = jnp.where(half == 0, place, 0.0).astype(BF16)
    second = jnp.where(half == 1, place, 0.0).astype(BF16)
    out_ref[...] = (dot(first, rows[:, :128]) + dot(second, rows[:, 128:])).astype(BF16)


def weigh_body(ids, y_ref, routes_ref, weight_ref, table_ref, shared_ref, own_ref, send_ref):
    c = ids[2]
    expert = table_ref[0:1, :] + 2 * c
    member = jnp.zeros((TOK, 2 * SLOTS), F32)
    weight = jnp.zeros((TOK, 2 * SLOTS), F32)
    for k in range(4):
        same = routes_ref[:, k : k + 1] == expert
        member = jnp.where(same, 1.0, member)
        weight = jnp.where(same, weight_ref[:, k : k + 1], weight)
    after = lax.broadcasted_iota(jnp.int32, (TOK, TOK), 0)
    before = lax.broadcasted_iota(jnp.int32, (TOK, TOK), 1)
    earlier = jnp.where(before < after, 1.0, 0.0).astype(BF16)
    rank = dot(earlier, member.astype(BF16))
    weight = jnp.where(rank == table_ref[1:2, :].astype(F32), weight, 0.0)
    half = table_ref[2:3, :]
    y = y_ref[...]
    row = lax.broadcasted_iota(jnp.int32, (TOK, 128), 0)
    mine = (row >= c * 64) & (row < c * 64 + 64)
    shared = shared_ref[...]
    shared = jnp.concatenate([shared, shared], axis=0)
    for which, ref in ((c, own_ref), (1 - c, send_ref)):
        part = jnp.where(half == which, weight, 0.0)
        total = jnp.zeros((TOK, 128), F32)
        for piece in three_pieces(part):
            total = total + dot(piece, y)
        columns = jnp.where(which == 0, shared[:, :128], shared[:, 128:])
        ref[...] = total + jnp.where(mine, columns, 0.0)


def on_device(
    queries,
    keys,
    values,
    cum_gate,
    head_gain,
    moe_in,
    ffn_gain,
    routes,
    route_weight,
    expert_gate,
    expert_up,
    expert_down,
    shared_gate,
    shared_up,
    shared_down,
):
    z, x, y, c = (lax.axis_index(a) for a in ("z", "x", "y", "c"))
    ids = jnp.stack([z, x, c, y]).astype(jnp.int32)
    table = jnp.asarray(slot_table())
    source = jnp.asarray(source_table())
    swap = [(0, 1), (1, 0)]

    packed = call(
        pack_body,
        jax.ShapeDtypeStruct((KVG, ROWS), BF16),
        ids,
        (1,),
        [whole((HEAD, ROWS)), whole((HEAD, ROWS)), whole((1, ROWS))],
        whole((KVG, ROWS)),
        (keys.T, values.T, cum_gate.reshape(1, ROWS)),
    )
    kvg = lax.all_gather(packed, "z", axis=0, tiled=True).reshape(NZ, KVG, ROWS)

    normed, sent = call(
        dispatch_body,
        (
            jax.ShapeDtypeStruct((TOK, D), BF16),
            jax.ShapeDtypeStruct((2 * SLOTS, D // 2), BF16),
        ),
        ids,
        (1,),
        [whole((TOK, D)), whole((1, D)), whole((4, TOK)), whole((2 * SLOTS, 8)), UNREAD],
        (whole((TOK, D)), whole((2 * SLOTS, D // 2))),
        (moe_in, ffn_gain.reshape(1, D), routes.T, table, packed),
        flops=1_000_000_000,
    )
    arrived = lax.all_to_all(sent, ("z", "x"), 0, 0, tiled=True)

    other = pl.BlockSpec((LOCAL, 64, D), lambda i, s: (1 - s[2], 0, 0))
    trade = call(
        trade_body,
        jax.ShapeDtypeStruct((480, D), BF16),
        ids,
        (1,),
        [other, other, other, whole((32, D)), whole((32, D)), whole((32, D)), UNREAD],
        whole((480, D)),
        (expert_gate, expert_up, expert_down, shared_gate, shared_up, shared_down, sent),
        flops=1_000_000_000,
    )
    got = lax.ppermute(trade, "c", swap)

    mine, _ = lax.optimization_barrier((queries.T, trade))
    q_all = [mine] + [
        lax.ppermute(mine, "x", [((i + d) % NX, i) for i in range(NX)]) for d in range(1, NX)
    ]

    down_sent = call(
        split_down_body,
        (jax.ShapeDtypeStruct((320, 256), BF16),) * NY,
        ids,
        (1,),
        [pl.BlockSpec((LOCAL, 64, D), lambda i, s: (s[2], 0, 0)), whole((480, D)), whole((32, D))],
        (whole((320, 256)),) * NY,
        (expert_down, got, shared_down),
        flops=1_000_000_000,
    )
    down = [down_sent[0]] + [
        lax.ppermute(down_sent[r], "y", [(i, (i + r) % NY) for i in range(NY)])
        for r in range(1, NY)
    ]

    hidden_sent = call(
        hidden_body,
        jax.ShapeDtypeStruct((NY, SLOTS + 64, 128), BF16),
        ids,
        (1,),
        [
            whole((2 * SLOTS, D // 2)),
            pl.BlockSpec((LOCAL, 64, D), lambda i, s: (s[2], 0, 0)),
            pl.BlockSpec((LOCAL, 64, D), lambda i, s: (s[2], 0, 0)),
            whole((480, D)),
            whole((TOK, D)),
            whole((32, D)),
            whole((32, D)),
            whole((SLOTS, 8)),
        ],
        whole((NY, SLOTS + 64, 128)),
        (arrived, expert_gate, expert_up, got, normed, shared_gate, shared_up, source),
        flops=1_000_000_000,
    )
    hidden = lax.all_to_all(hidden_sent, "y", 0, 0, tiled=True)

    def attend(turns):
        return call(
            functools.partial(attend_body, turns),
            (jax.ShapeDtypeStruct((ROWS, 128), BF16),) * 2,
            ids,
            (2 * (ROWS // QT),),
            [pl.BlockSpec((HEAD, QT), lambda i, s: (0, lax.rem(i, ROWS // QT)))] * 2
            + [whole((NZ, KVG, ROWS))],
            (whole((ROWS, 128)),) * 2,
            (q_all[turns[0]], q_all[turns[1]], kvg),
            scratch=[pltpu.VMEM((NZ, DEPTH, ROWS), BF16)],
            flops=10_000_000_000,
        )

    def send_part(part, d):
        return lax.ppermute(part, "x", [(i, (i + d) % NX) for i in range(NX)])

    part1, part2 = attend((1, 2))
    part1, part2 = send_part(part1, 1), send_part(part2, 2)

    rows, shared = call(
        down_body,
        (
            jax.ShapeDtypeStruct((2 * SLOTS, 128), BF16),
            jax.ShapeDtypeStruct((64, 256), F32),
        ),
        ids,
        (1,),
        [whole((NY, SLOTS + 64, 128)), whole((2 * SLOTS, 8))] + [whole((320, 256))] * NY,
        (whole((2 * SLOTS, 128)), whole((64, 256))),
        (hidden, table, *down),
        flops=1_000_000_000,
    )
    returned = lax.all_to_all(rows, ("z", "x"), 0, 0, tiled=True)

    part3, part0 = attend((3, 0))
    part3 = send_part(part3, 3)

    mixed = call(
        combine_body,
        jax.ShapeDtypeStruct((HEAD, ROWS), BF16),
        ids,
        (1,),
        [whole((1, HEAD))] + [whole((ROWS, 128))] * NX,
        whole((HEAD, ROWS)),
        (head_gain.reshape(1, HEAD), part0, part1, part2, part3),
    ).T

    own, give = call(
        weigh_body,
        (jax.ShapeDtypeStruct((TOK, 128), F32), jax.ShapeDtypeStruct((TOK, 128), F32)),
        ids,
        (1,),
        [
            whole((2 * SLOTS, 128)),
            whole((TOK, 4)),
            whole((TOK, 4)),
            whole((8, 2 * SLOTS)),
            whole((64, 256)),
        ],
        (whole((TOK, 128)), whole((TOK, 128))),
        (returned, routes, route_weight, table.T, shared),
        flops=1_000_000_000,
    )
    taken = lax.ppermute(give, "c", swap)
    expert_out = (own + taken).astype(BF16)
    return (mixed, expert_out)


def solution(mesh):
    fine = Mesh(mesh.devices.reshape(NZ, NX, NY, NC), ("z", "x", "y", "c"))
    ep, tp = ("z", "x"), ("y", "c")
    in_specs = (
        P(ep, tp),
        P(ep, tp),
        P(ep, tp),
        P(ep, tp),
        P(tp),
        P(ep, None),
        P(),
        P(ep, None),
        P(ep, None),
        P(ep, tp, None),
        P(ep, tp, None),
        P(ep, tp, None),
        P(tp, None),
        P(tp, None),
        P(tp, None),
    )
    out_specs = (P(ep, tp), P(ep, tp))

    return jax.shard_map(
        on_device, mesh=fine, in_specs=in_specs, out_specs=out_specs, check_vma=False
    )
```

time: 348 us -> 233 us (0.67)
  the two profiles are of different devices: /device:TPU:32 before, /device:TPU:505 now
where the time goes in v1:
time: 233 us; the launch traced here: 232 us
  Pallas kernels  88 us (38%)
  starting transfers between devices  83.8 us (36%)
  waiting for transfers between devices  38 us (16%)
  between operations  14.4 us (6%)
  local copies, waits for them, and re-layouts  5.78 us (2%)
    pallas_call x10, Pallas kernels, call(): pl.pallas_call(body, out_shape=out_shape, grid_spec=pltpu.PrefetchScalarG...  88 us
    all_to_all x1, waiting for transfers between devices, on_device(): arrived = lax.all_to_all(sent, ('z', 'x'), 0, 0, tiled=True)  30.2 us
    ppermute x7, starting transfers between devices, on_device(): lax.ppermute(down_sent[r], 'y', [(i, (i + r) % NY) for i in range(NY)])  30 us
    ppermute x1, starting transfers between devices, on_device(): taken = lax.ppermute(give, 'c', swap)  14.2 us
    all_to_all x1, starting transfers between devices, on_device(): returned = lax.all_to_all(rows, ('z', 'x'), 0, 0, tiled=True)  9.71 us
    ppermute x3, starting transfers between devices, on_device(): lax.ppermute(mine, 'x', [((i + d) % NX, i) for i in range(NX)])  7.28 us
    ppermute x3, starting transfers between devices, send_part(): return lax.ppermute(part, 'x', [(i, (i + d) % NX) for i in range(NX)])  6.68 us
    all_to_all x1, starting transfers between devices, on_device(): arrived = lax.all_to_all(sent, ('z', 'x'), 0, 0, tiled=True)  6.64 us
  transfers between devices with their start and end apart: 19, of which 5 were waited for; matrix products, arithmetic and copies ran while one was open for 1% of the time, Pallas kernels for 35%

profile of v1, /device:TPU:505, one launch (start us, length us, event | category | flops | bytes accessed | tf_op | source)
XLA Modules:
  0.0 232.1 jit_solution(1552345753120022559)
XLA Ops:
  7.2 0.7 pad_add_fusion.ids
  7.8 2.3 shard_map.176.after_ref
  10.2 4.4 %shard_map.177 = (bf16[128,2048]{1,0:T(8,128)(2,1)}, bf16[768,1024]{1,0:T(8,128)(2,1)}) custom-call(s32[4]{0:T(128)} %pad_add_fusion.ids, bf16[128,2048]{1,0:T(8,128)(2,1)} %x_ref.1, f32[1,2048]{1,0:T(1,128)} %bitcast.33, s32[4,128]{1,0:T(4,128)} %bitcast.25, s32[768,8]{1,0:T(8,128)} %constant.22.clone.table_ref, bf16[144,768]{1,0:T(8,128)(2,1)} %shard_map.176.after_ref), custom_call_target="tpu_custom_call" | custom-call | flops 1000000000 | bytes 4194304 | tf_op jit(solution)/shard_map/pallas_call | solution.py:73
  14.5 6.6 %all-to-all-start = ((bf16[32,24,1024]{2,1,0:T(8,128)(2,1)}), bf16[32,24,1024]{2,1,0:T(8,128)(2,1)S(1)}, u32[]{:S(2)}, u32[]{:S(2)}) async-start(bf16[32,24,1024]{2,1,0:T(8,128)(2,1)} %bitcast.17), calls=%async_computation | async-start | bytes 3145728 | tf_op jit(solution)/shard_map/all_to_all | solution.py:358
  21.2 0.0 all-gather.2.cloned.1.call-start
  21.2 0.7 all-gather.2.cloned.1.call-update
  21.9 3.6 %shard_map.178 = bf16[480,2048]{1,0:T(8,128)(2,1)} custom-call(s32[4]{0:T(128)} %pad_add_fusion.ids, bf16[4,64,2048]{2,1,0:T(8,128)(2,1)} %gate_ref.3, bf16[4,64,2048]{2,1,0:T(8,128)(2,1)} %up_ref.3, bf16[4,64,2048]{2,1,0:T(8,128)(2,1)} %own_ref.1, bf16[32,2048]{1,0:T(8,128)(2,1)} %sgate_ref.3, bf16[32,2048]{1,0:T(8,128)(2,1)} %sup_ref.3, ...), custom_call_target="tpu_custom_call" | custom-call | flops 1000000000 | bytes 4194304 | tf_op jit(solution)/shard_map/pallas_call | solution.py:73
  25.5 3.1 %collective-permute-start.6 = (bf16[480,2048]{1,0:T(8,128)(2,1)}, bf16[480,2048]{1,0:T(8,128)(2,1)S(1)}, u32[]{:S(2)}, u32[]{:S(2)}) collective-permute-start(bf16[480,2048]{1,0:T(8,128)(2,1)} %shard_map.178), channel_id=1, source_target_pairs={{0,1},{1,0},{2,3},{3,2},{4,5},{5,4},{6,7},{7,6},{8,9},{9,8},{10,11... | collective-permute-start | bytes 5898248 | tf_op jit(solution)/shard_map/ppermute | solution.py:371
  28.7 3.8 %collective-permute-done.6.got_ref = bf16[480,2048]{1,0:T(8,128)(2,1)S(1)} collective-permute-done((bf16[480,2048]{1,0:T(8,128)(2,1)}, bf16[480,2048]{1,0:T(8,128)(2,1)S(1)}, u32[]{:S(2)}, u32[]{:S(2)}) %collective-permute-start.6) | collective-permute-done | bytes 1966112 | tf_op jit(solution)/shard_map/ppermute | solution.py:371
  32.5 30.2 %all-to-all-done = bf16[32,24,1024]{2,1,0:T(8,128)(2,1)S(1)} async-done(((bf16[32,24,1024]{2,1,0:T(8,128)(2,1)}), bf16[32,24,1024]{2,1,0:T(8,128)(2,1)S(1)}, u32[]{:S(2)}, u32[]{:S(2)}) %all-to-all-start) | async-done | bytes 1572896 | tf_op jit(solution)/shard_map/all_to_all | solution.py:358
  62.6 1.2 copy-done
  63.8 6.6 %shard_map.182 = bf16[8,448,128]{2,1,0:T(8,128)(2,1)} custom-call(s32[4]{0:T(128)} %pad_add_fusion.ids, bf16[768,1024]{1,0:T(8,128)(2,1)} %bitcast.18, bf16[4,64,2048]{2,1,0:T(8,128)(2,1)} %gate_ref.3, bf16[4,64,2048]{2,1,0:T(8,128)(2,1)} %up_ref.3, bf16[480,2048]{1,0:T(8,128)(2,1)} %copy-done.1, bf16[128,2048]{1,0:T(8,128)(2,1)} %get-tuple-element.27.normed_ref, ...), custom_call_target="tpu_custom_call" | custom-call | flops 1000000000 | bytes 4194304 | tf_op jit(solution)/shard_map/pallas_call | solution.py:73
  70.4 6.1 %all-to-all-start.1 = ((bf16[8,448,128]{2,1,0:T(8,128)(2,1)}), bf16[8,448,128]{2,1,0:T(8,128)(2,1)S(1)}, u32[]{:S(2)}, u32[]{:S(2)}) async-start(bf16[8,448,128]{2,1,0:T(8,128)(2,1)} %shard_map.182), calls=%async_computation.1 | async-start | bytes 1835008 | tf_op jit(solution)/shard_map/all_to_all | solution.py:412
  76.5 3.7 %shard_map.183 = (bf16[320,256]{1,0:T(8,128)(2,1)}, bf16[320,256]{1,0:T(8,128)(2,1)}, bf16[320,256]{1,0:T(8,128)(2,1)}, bf16[320,256]{1,0:T(8,128)(2,1)}, bf16[3...) custom-call(s32[4]{0:T(128)} %pad_add_fusion.ids, ...), custom_call_target="tpu_custom_call" | custom-call | flops 1000000000 | bytes 4194304 | tf_op jit(solution)/shard_map/pallas_call | solution.py:73
  80.2 1.9 collective-permute-start.7
  82.1 4.3 %collective-permute-start.8 = (bf16[320,256]{1,0:T(8,128)(2,1)}, bf16[320,256]{1,0:T(8,128)(2,1)S(1)}, u32[]{:S(2)}, u32[]{:S(2)}) collective-permute-start(bf16[320,256]{1,0:T(8,128)(2,1)} %get-tuple-element.30), channel_id=1, source_target_pairs={{0,4},{2,6},{4,8},{6,10},{8,12},{10,14},{12,0},{14,2},{1,5},{3,7},... | collective-permute-start | bytes 491528 | tf_op jit(solution)/shard_map/ppermute | solution.py:389
  86.4 5.2 %collective-permute-start.9 = (bf16[320,256]{1,0:T(8,128)(2,1)}, bf16[320,256]{1,0:T(8,128)(2,1)S(1)}, u32[]{:S(2)}, u32[]{:S(2)}) collective-permute-start(bf16[320,256]{1,0:T(8,128)(2,1)} %get-tuple-element.31), channel_id=1, source_target_pairs={{0,6},{2,8},{4,10},{6,12},{8,14},{10,0},{12,2},{14,4},{1,7},{3,9},... | collective-permute-start | bytes 491528 | tf_op jit(solution)/shard_map/ppermute | solution.py:389
  91.6 3.3 %collective-permute-start.1 = (bf16[64,768]{1,0:T(8,128)(2,1)S(1)}, bf16[64,768]{1,0:T(8,128)(2,1)S(1)}, u32[]{:S(2)}, u32[]{:S(2)}) collective-permute-start(bf16[64,768]{1,0:T(8,128)(2,1)S(1)} %bitcast.30), channel_id=1, source_target_pairs={{16,0},{32,16},{48,32},{0,48},{17,1},{33,17},{49,33},{1,49},{18,2}... | collective-permute-start | bytes 294920 | tf_op jit(solution)/shard_map/ppermute | solution.py:375
  94.9 1.9 collective-permute-start.2
  96.8 0.4 collective-permute-done.1.q0_ref
  97.2 2.1 collective-permute-start
  99.3 2.4 %collective-permute-done.2.q1_ref = bf16[64,768]{1,0:T(8,128)(2,1)S(1)} collective-permute-done((bf16[64,768]{1,0:T(8,128)(2,1)S(1)}, bf16[64,768]{1,0:T(8,128)(2,1)S(1)}, u32[]{:S(2)}, u32[]{:S(2)}) %collective-permute-start.2) | collective-permute-done | bytes 98336 | tf_op jit(solution)/shard_map/ppermute | solution.py:375
  101.7 3.1 %collective-permute-start.10 = (bf16[320,256]{1,0:T(8,128)(2,1)}, bf16[320,256]{1,0:T(8,128)(2,1)S(1)}, u32[]{:S(2)}, u32[]{:S(2)}) collective-permute-start(bf16[320,256]{1,0:T(8,128)(2,1)} %get-tuple-element.32), channel_id=1, source_target_pairs={{0,8},{2,10},{4,12},{6,14},{8,0},{10,2},{12,4},{14,6},{1,9},{3,11}... | collective-permute-start | bytes 491528 | tf_op jit(solution)/shard_map/ppermute | solution.py:389
  104.8 0.0 collective-permute-done.7.rest_1_
  104.8 4.3 %collective-permute-start.11 = (bf16[320,256]{1,0:T(8,128)(2,1)}, bf16[320,256]{1,0:T(8,128)(2,1)S(1)}, u32[]{:S(2)}, u32[]{:S(2)}) collective-permute-start(bf16[320,256]{1,0:T(8,128)(2,1)} %get-tuple-element.33), channel_id=1, source_target_pairs={{0,10},{2,12},{4,14},{6,0},{8,2},{10,4},{12,6},{14,8},{1,11},{3,13... | collective-permute-start | bytes 491528 | tf_op jit(solution)/shard_map/ppermute | solution.py:389
  109.1 0.0 collective-permute-done.8.rest_2_
  109.2 4.9 %collective-permute-start.12 = (bf16[320,256]{1,0:T(8,128)(2,1)}, bf16[320,256]{1,0:T(8,128)(2,1)S(1)}, u32[]{:S(2)}, u32[]{:S(2)}) collective-permute-start(bf16[320,256]{1,0:T(8,128)(2,1)} %get-tuple-element.34), channel_id=1, source_target_pairs={{0,12},{2,14},{4,0},{6,2},{8,4},{10,6},{12,8},{14,10},{1,13},{3,15... | collective-permute-start | bytes 491528 | tf_op jit(solution)/shard_map/ppermute | solution.py:389
  114.1 0.4 collective-permute-done.9.rest_3_
  114.5 6.3 %collective-permute-start.13 = (bf16[320,256]{1,0:T(8,128)(2,1)}, bf16[320,256]{1,0:T(8,128)(2,1)S(1)}, u32[]{:S(2)}, u32[]{:S(2)}) collective-permute-start(bf16[320,256]{1,0:T(8,128)(2,1)} %get-tuple-element.35), channel_id=1, source_target_pairs={{0,14},{2,0},{4,2},{6,4},{8,6},{10,8},{12,10},{14,12},{1,15},{3,1}... | collective-permute-start | bytes 491528 | tf_op jit(solution)/shard_map/ppermute | solution.py:389
  120.8 0.0 all-gather.2.cloned.1.call-done
  120.9 28.1 %shard_map.180 = (bf16[768,128]{1,0:T(8,128)(2,1)}, bf16[768,128]{1,0:T(8,128)(2,1)}) custom-call(s32[4]{0:T(128)} %pad_add_fusion.ids, bf16[64,768]{1,0:T(8,128)(2,1)} %copy-done.18, bf16[64,768]{1,0:T(8,128)(2,1)} %copy-done.19, bf16[8,144,768]{2,1,0:T(8,128)(2,1)} %bitcast.27), custom_call_target="tpu_custom_call" | custom-call | flops 10000000000 | bytes 4194304 | tf_op jit(solution)/shard_map/pallas_call | solution.py:73
  149.0 0.0 collective-permute-done.10.rest_4_
  149.0 1.9 collective-permute-start.3
  150.9 0.0 collective-permute-done.11.rest_5_
  150.9 1.9 collective-permute-start.4
  152.9 0.0 collective-permute-done.12.rest_6_
  152.9 0.0 collective-permute-done.13.rest_7_
  152.9 0.0 all-to-all-done.1.h_ref
  152.9 0.6 copy-done.14
  153.5 0.1 copy-done.15
  153.6 0.3 copy-done.2
  153.9 4.3 %shard_map.184 = (bf16[768,128]{1,0:T(8,128)(2,1)}, f32[64,256]{1,0:T(8,128)}) custom-call(s32[4]{0:T(128)} %pad_add_fusion.ids, bf16[8,448,128]{2,1,0:T(8,128)(2,1)} %copy-done.2, s32[768,8]{1,0:T(8,128)} %constant.22.clone.table_ref, bf16[320,256]{1,0:T(8,128)(2,1)} %get-tuple-element.28.rest_0_, bf16[320,256]{1,0:T(8,128)(2,1)} %copy-done.9, ...), custom_call_target="tpu_custom_call" | custom-call | flops 1000000000 | bytes 4194304 | tf_op jit(solution)/shard_map/pallas_call | solution.py:73
  158.2 9.7 %all-to-all-start.2 = ((bf16[32,24,128]{2,1,0:T(8,128)(2,1)}), bf16[32,24,128]{2,1,0:T(8,128)(2,1)S(1)}, u32[]{:S(2)}, u32[]{:S(2)}) async-start(bf16[32,24,128]{2,1,0:T(8,128)(2,1)} %bitcast.19), calls=%async_computation.2 | async-start | bytes 393216 | tf_op jit(solution)/shard_map/all_to_all | solution.py:447
  168.0 0.0 copy-start.7
  168.0 0.0 copy-start.8
  168.0 0.0 collective-permute-done.q0_ref
  168.0 0.0 copy-start.17
  168.0 0.6 copy-done.17
  168.6 28.1 %shard_map.179 = (bf16[768,128]{1,0:T(8,128)(2,1)}, bf16[768,128]{1,0:T(8,128)(2,1)}) custom-call(s32[4]{0:T(128)} %pad_add_fusion.ids, bf16[64,768]{1,0:T(8,128)(2,1)} %copy-done.17, bf16[64,768]{1,0:T(8,128)(2,1)} %bitcast.29, bf16[8,144,768]{2,1,0:T(8,128)(2,1)} %bitcast.28), custom_call_target="tpu_custom_call" | custom-call | flops 10000000000 | bytes 4194304 | tf_op jit(solution)/shard_map/pallas_call | solution.py:73
  196.7 2.8 %collective-permute-start.5 = (bf16[768,128]{1,0:T(8,128)(2,1)}, bf16[768,128]{1,0:T(8,128)(2,1)S(1)}, u32[]{:S(2)}, u32[]{:S(2)}) collective-permute-start(bf16[768,128]{1,0:T(8,128)(2,1)} %get-tuple-element.26), channel_id=1, source_target_pairs={{0,48},{16,0},{32,16},{48,32},{1,49},{17,1},{33,17},{49,33},{2,50}... | collective-permute-start | bytes 589832 | tf_op jit(solution)/shard_map/ppermute | solution.py:429
  199.6 0.7 copy.19.routes_ref
  200.3 0.7 copy.20.weight_ref
  201.1 0.0 all-to-all-done.2
  201.1 0.7 copy-done.3
  201.8 3.2 %shard_map.185 = (f32[128,128]{1,0:T(8,128)}, f32[128,128]{1,0:T(8,128)}) custom-call(s32[4]{0:T(128)} %pad_add_fusion.ids, bf16[768,128]{1,0:T(8,128)(2,1)} %bitcast.20, s32[128,4]{1,0:T(8,128)} %copy.19.routes_ref, f32[128,4]{1,0:T(8,128)} %copy.20.weight_ref, s32[8,768]{1,0:T(8,128)} %constant.28.table_ref, f32[64,256]{1,0:T(8,128)} %get-tuple-element.37.shared_ref), custom_call_target="tpu_custom_call" | custom-call | flops 1000000000 | bytes 4194304 | tf_op jit(solution)/shard_map/pallas_call | solution.py:73
  204.9 14.2 %collective-permute-start.14 = (f32[128,128]{1,0:T(8,128)}, f32[128,128]{1,0:T(8,128)S(1)}, u32[]{:S(2)}, u32[]{:S(2)}) collective-permute-start(f32[128,128]{1,0:T(8,128)} %get-tuple-element.39), channel_id=1, source_target_pairs={{0,1},{1,0},{2,3},{3,2},{4,5},{5,4},{6,7},{7,6},{8,9},{9,8},{10,11... | collective-permute-start | bytes 196616 | tf_op jit(solution)/shard_map/ppermute | solution.py:478
  219.2 0.0 collective-permute-done.4.refs_2_
  219.2 0.0 collective-permute-done.5.refs_3_
  219.2 0.6 copy-done.4
  219.9 0.1 copy-done.5
  220.0 0.0 copy-done.6
  220.0 3.8 %shard_map.181 = bf16[64,768]{1,0:T(8,128)(2,1)} custom-call(s32[4]{0:T(128)} %pad_add_fusion.ids, f32[1,64]{1,0:T(1,128)} %bitcast.26, bf16[768,128]{1,0:T(8,128)(2,1)} %get-tuple-element.23.refs_0_, bf16[768,128]{1,0:T(8,128)(2,1)} %copy-done.4, bf16[768,128]{1,0:T(8,128)(2,1)} %copy-done.5, bf16[768,128]{1,0:T(8,128)(2,1)} %copy-done.6), custom_call_target="tpu_custom_call" | custom-call | bytes 4194304 | tf_op jit(solution)/shard_map/pallas_call | solution.py:73
  223.8 0.0 collective-permute-done.14
  223.8 1.5 add_convert_fusion
  (29 shorter events, 0.1 us)
Async XLA Ops:
  14.5 48.1 %all-to-all-start = ((bf16[32,24,1024]{2,1,0:T(8,128)(2,1)}), bf16[32,24,1024]{2,1,0:T(8,128)(2,1)S(1)}, u32[]{:S(2)}, u32[]{:S(2)}) async-start(bf16[32,24,1024]{2,1,0:T(8,128)(2,1)} %bitcast.17), calls=%async_computation | async-start | bytes 3145728 | tf_op jit(solution)/shard_map/all_to_all | solution.py:358
  21.2 99.7 %all-gather.2.cloned.1.call-start = ((), (), s32[]{:S(2)}) async-start(), calls=%async_computation.3 | async-start | bytes 1990656 | tf_op jit(solution)/shard_map/all_gather | solution.py:343
  25.5 6.9 %collective-permute-start.6 = (bf16[480,2048]{1,0:T(8,128)(2,1)}, bf16[480,2048]{1,0:T(8,128)(2,1)S(1)}, u32[]{:S(2)}, u32[]{:S(2)}) collective-permute-start(bf16[480,2048]{1,0:T(8,128)(2,1)} %shard_map.178), channel_id=1, source_target_pairs={{0,1},{1,0},{2,3},{3,2},{4,5},{5,4},{6,7},{7,6},{8,9},{9,8},{10,11... | collective-permute-start | bytes 5898248 | tf_op jit(solution)/shard_map/ppermute | solution.py:371
  32.5 30.2 %copy-start.1 = (bf16[480,2048]{1,0:T(8,128)(2,1)}, bf16[480,2048]{1,0:T(8,128)(2,1)S(1)}, u32[]{:S(2)}) copy-start(bf16[480,2048]{1,0:T(8,128)(2,1)S(1)} %collective-permute-done.6.got_ref) | copy-start | bytes 5898244
  62.6 1.2 copy-start
  70.4 82.5 %all-to-all-start.1 = ((bf16[8,448,128]{2,1,0:T(8,128)(2,1)}), bf16[8,448,128]{2,1,0:T(8,128)(2,1)S(1)}, u32[]{:S(2)}, u32[]{:S(2)}) async-start(bf16[8,448,128]{2,1,0:T(8,128)(2,1)} %shard_map.182), calls=%async_computation.1 | async-start | bytes 1835008 | tf_op jit(solution)/shard_map/all_to_all | solution.py:412
  76.5 15.1 %copy-start.16 = (bf16[768,64]{0,1:T(8,128)(2,1)S(1)}, bf16[768,64]{0,1:T(8,128)(2,1)}, u32[]{:S(2)}) copy-start(bf16[768,64]{0,1:T(8,128)(2,1)} %param.17) | copy-start | bytes 294916
  80.2 24.7 %collective-permute-start.7 = (bf16[320,256]{1,0:T(8,128)(2,1)}, bf16[320,256]{1,0:T(8,128)(2,1)S(1)}, u32[]{:S(2)}, u32[]{:S(2)}) collective-permute-start(bf16[320,256]{1,0:T(8,128)(2,1)} %get-tuple-element.29), channel_id=1, source_target_pairs={{0,2},{2,4},{4,6},{6,8},{8,10},{10,12},{12,14},{14,0},{1,3},{3,5},... | collective-permute-start | bytes 491528 | tf_op jit(solution)/shard_map/ppermute | solution.py:389
  82.1 27.1 %collective-permute-start.8 = (bf16[320,256]{1,0:T(8,128)(2,1)}, bf16[320,256]{1,0:T(8,128)(2,1)S(1)}, u32[]{:S(2)}, u32[]{:S(2)}) collective-permute-start(bf16[320,256]{1,0:T(8,128)(2,1)} %get-tuple-element.30), channel_id=1, source_target_pairs={{0,4},{2,6},{4,8},{6,10},{8,12},{10,14},{12,0},{14,2},{1,5},{3,7},... | collective-permute-start | bytes 491528 | tf_op jit(solution)/shard_map/ppermute | solution.py:389
  86.4 28.2 %collective-permute-start.9 = (bf16[320,256]{1,0:T(8,128)(2,1)}, bf16[320,256]{1,0:T(8,128)(2,1)S(1)}, u32[]{:S(2)}, u32[]{:S(2)}) collective-permute-start(bf16[320,256]{1,0:T(8,128)(2,1)} %get-tuple-element.31), channel_id=1, source_target_pairs={{0,6},{2,8},{4,10},{6,12},{8,14},{10,0},{12,2},{14,4},{1,7},{3,9},... | collective-permute-start | bytes 491528 | tf_op jit(solution)/shard_map/ppermute | solution.py:389
  91.6 5.7 %collective-permute-start.1 = (bf16[64,768]{1,0:T(8,128)(2,1)S(1)}, bf16[64,768]{1,0:T(8,128)(2,1)S(1)}, u32[]{:S(2)}, u32[]{:S(2)}) collective-permute-start(bf16[64,768]{1,0:T(8,128)(2,1)S(1)} %bitcast.30), channel_id=1, source_target_pairs={{16,0},{32,16},{48,32},{0,48},{17,1},{33,17},{49,33},{1,49},{18,2}... | collective-permute-start | bytes 294920 | tf_op jit(solution)/shard_map/ppermute | solution.py:375
  94.9 6.9 %collective-permute-start.2 = (bf16[64,768]{1,0:T(8,128)(2,1)S(1)}, bf16[64,768]{1,0:T(8,128)(2,1)S(1)}, u32[]{:S(2)}, u32[]{:S(2)}) collective-permute-start(bf16[64,768]{1,0:T(8,128)(2,1)S(1)} %bitcast.31), channel_id=1, source_target_pairs={{32,0},{48,16},{0,32},{16,48},{33,1},{49,17},{1,33},{17,49},{34,2}... | collective-permute-start | bytes 294920 | tf_op jit(solution)/shard_map/ppermute | solution.py:375
  97.2 23.6 %copy-start.18 = (bf16[64,768]{1,0:T(8,128)(2,1)}, bf16[64,768]{1,0:T(8,128)(2,1)S(1)}, u32[]{:S(2)}) copy-start(bf16[64,768]{1,0:T(8,128)(2,1)S(1)} %collective-permute-done.1.q0_ref) | copy-start | bytes 294916
  97.2 70.7 %collective-permute-start = (bf16[64,768]{1,0:T(8,128)(2,1)S(1)}, bf16[64,768]{1,0:T(8,128)(2,1)S(1)}, u32[]{:S(2)}, u32[]{:S(2)}) collective-permute-start(bf16[64,768]{1,0:T(8,128)(2,1)S(1)} %bitcast.32), channel_id=1, source_target_pairs={{48,0},{0,16},{16,32},{32,48},{49,1},{1,17},{17,33},{33,49},{50,2}... | collective-permute-start | bytes 294920 | tf_op jit(solution)/shard_map/ppermute | solution.py:375
  101.7 19.1 %copy-start.19 = (bf16[64,768]{1,0:T(8,128)(2,1)}, bf16[64,768]{1,0:T(8,128)(2,1)S(1)}, u32[]{:S(2)}) copy-start(bf16[64,768]{1,0:T(8,128)(2,1)S(1)} %collective-permute-done.2.q1_ref) | copy-start | bytes 294916
  101.7 47.2 %collective-permute-start.10 = (bf16[320,256]{1,0:T(8,128)(2,1)}, bf16[320,256]{1,0:T(8,128)(2,1)S(1)}, u32[]{:S(2)}, u32[]{:S(2)}) collective-permute-start(bf16[320,256]{1,0:T(8,128)(2,1)} %get-tuple-element.32), channel_id=1, source_target_pairs={{0,8},{2,10},{4,12},{6,14},{8,0},{10,2},{12,4},{14,6},{1,9},{3,11}... | collective-permute-start | bytes 491528 | tf_op jit(solution)/shard_map/ppermute | solution.py:389
  104.8 44.1 %copy-start.9 = (bf16[320,256]{1,0:T(8,128)(2,1)}, bf16[320,256]{1,0:T(8,128)(2,1)S(1)}, u32[]{:S(2)}) copy-start(bf16[320,256]{1,0:T(8,128)(2,1)S(1)} %collective-permute-done.7.rest_1_) | copy-start | bytes 491524
  104.8 46.1 %collective-permute-start.11 = (bf16[320,256]{1,0:T(8,128)(2,1)}, bf16[320,256]{1,0:T(8,128)(2,1)S(1)}, u32[]{:S(2)}, u32[]{:S(2)}) collective-permute-start(bf16[320,256]{1,0:T(8,128)(2,1)} %get-tuple-element.33), channel_id=1, source_target_pairs={{0,10},{2,12},{4,14},{6,0},{8,2},{10,4},{12,6},{14,8},{1,11},{3,13... | collective-permute-start | bytes 491528 | tf_op jit(solution)/shard_map/ppermute | solution.py:389
  109.2 39.8 %copy-start.10 = (bf16[320,256]{1,0:T(8,128)(2,1)}, bf16[320,256]{1,0:T(8,128)(2,1)S(1)}, u32[]{:S(2)}) copy-start(bf16[320,256]{1,0:T(8,128)(2,1)S(1)} %collective-permute-done.8.rest_2_) | copy-start | bytes 491524
  109.2 43.7 %collective-permute-start.12 = (bf16[320,256]{1,0:T(8,128)(2,1)}, bf16[320,256]{1,0:T(8,128)(2,1)S(1)}, u32[]{:S(2)}, u32[]{:S(2)}) collective-permute-start(bf16[320,256]{1,0:T(8,128)(2,1)} %get-tuple-element.34), channel_id=1, source_target_pairs={{0,12},{2,14},{4,0},{6,2},{8,4},{10,6},{12,8},{14,10},{1,13},{3,15... | collective-permute-start | bytes 491528 | tf_op jit(solution)/shard_map/ppermute | solution.py:389
  114.5 34.4 %copy-start.11 = (bf16[320,256]{1,0:T(8,128)(2,1)}, bf16[320,256]{1,0:T(8,128)(2,1)S(1)}, u32[]{:S(2)}) copy-start(bf16[320,256]{1,0:T(8,128)(2,1)S(1)} %collective-permute-done.9.rest_3_) | copy-start | bytes 491524
  114.5 38.4 %collective-permute-start.13 = (bf16[320,256]{1,0:T(8,128)(2,1)}, bf16[320,256]{1,0:T(8,128)(2,1)S(1)}, u32[]{:S(2)}, u32[]{:S(2)}) collective-permute-start(bf16[320,256]{1,0:T(8,128)(2,1)} %get-tuple-element.35), channel_id=1, source_target_pairs={{0,14},{2,0},{4,2},{6,4},{8,6},{10,8},{12,10},{14,12},{1,15},{3,1}... | collective-permute-start | bytes 491528 | tf_op jit(solution)/shard_map/ppermute | solution.py:389
  149.0 4.0 %copy-start.12 = (bf16[320,256]{1,0:T(8,128)(2,1)}, bf16[320,256]{1,0:T(8,128)(2,1)S(1)}, u32[]{:S(2)}) copy-start(bf16[320,256]{1,0:T(8,128)(2,1)S(1)} %collective-permute-done.10.rest_4_) | copy-start | bytes 491524
  149.0 70.2 %collective-permute-start.3 = (bf16[768,128]{1,0:T(8,128)(2,1)}, bf16[768,128]{1,0:T(8,128)(2,1)S(1)}, u32[]{:S(2)}, u32[]{:S(2)}) collective-permute-start(bf16[768,128]{1,0:T(8,128)(2,1)} %get-tuple-element.24), channel_id=1, source_target_pairs={{0,16},{16,32},{32,48},{48,0},{1,17},{17,33},{33,49},{49,1},{2,18}... | collective-permute-start | bytes 589832 | tf_op jit(solution)/shard_map/ppermute | solution.py:429
  150.9 2.0 copy-start.13
  150.9 68.3 %collective-permute-start.4 = (bf16[768,128]{1,0:T(8,128)(2,1)}, bf16[768,128]{1,0:T(8,128)(2,1)S(1)}, u32[]{:S(2)}, u32[]{:S(2)}) collective-permute-start(bf16[768,128]{1,0:T(8,128)(2,1)} %get-tuple-element.25), channel_id=1, source_target_pairs={{0,32},{16,48},{32,0},{48,16},{1,33},{17,49},{33,1},{49,17},{2,34}... | collective-permute-start | bytes 589832 | tf_op jit(solution)/shard_map/ppermute | solution.py:429
  152.9 0.7 copy-start.14
  152.9 0.7 copy-start.15
  152.9 1.0 copy-start.2
  158.2 42.8 %all-to-all-start.2 = ((bf16[32,24,128]{2,1,0:T(8,128)(2,1)}), bf16[32,24,128]{2,1,0:T(8,128)(2,1)S(1)}, u32[]{:S(2)}, u32[]{:S(2)}) async-start(bf16[32,24,128]{2,1,0:T(8,128)(2,1)} %bitcast.19), calls=%async_computation.2 | async-start | bytes 393216 | tf_op jit(solution)/shard_map/all_to_all | solution.py:447
  168.0 31.6 %copy-start.7 = (s32[128,4]{0,1:T(4,128)S(1)}, s32[128,4]{0,1:T(4,128)}, u32[]{:S(2)}) copy-start(s32[128,4]{0,1:T(4,128)} %param.24) | copy-start | bytes 6148
  168.0 32.4 %copy-start.8 = (f32[128,4]{0,1:T(4,128)S(1)}, f32[128,4]{0,1:T(4,128)}, u32[]{:S(2)}) copy-start(f32[128,4]{0,1:T(4,128)} %param.25) | copy-start | bytes 6148
  168.0 0.6 copy-start.17
  196.7 22.5 %collective-permute-start.5 = (bf16[768,128]{1,0:T(8,128)(2,1)}, bf16[768,128]{1,0:T(8,128)(2,1)S(1)}, u32[]{:S(2)}, u32[]{:S(2)}) collective-permute-start(bf16[768,128]{1,0:T(8,128)(2,1)} %get-tuple-element.26), channel_id=1, source_target_pairs={{0,48},{16,0},{32,16},{48,32},{1,49},{17,1},{33,17},{49,33},{2,50}... | collective-permute-start | bytes 589832 | tf_op jit(solution)/shard_map/ppermute | solution.py:429
  201.1 0.7 copy-start.3
  204.9 18.8 %collective-permute-start.14 = (f32[128,128]{1,0:T(8,128)}, f32[128,128]{1,0:T(8,128)S(1)}, u32[]{:S(2)}, u32[]{:S(2)}) collective-permute-start(f32[128,128]{1,0:T(8,128)} %get-tuple-element.39), channel_id=1, source_target_pairs={{0,1},{1,0},{2,3},{3,2},{4,5},{5,4},{6,7},{7,6},{8,9},{9,8},{10,11... | collective-permute-start | bytes 196616 | tf_op jit(solution)/shard_map/ppermute | solution.py:478
  219.2 0.7 copy-start.4
  219.2 0.7 copy-start.5
  219.2 0.8 copy-start.6
Sparse Core Ops, SparseCore 0:
  24.1 52.3 all-gather.1

commit v2 on v1

--- a/solution.py
+++ b/solution.py
@@ -117,64 +117,64 @@
         out_ref[384 + i * 32 : 416 + i * 32, :] = ref[...]
 
 
-QT = 384
+TILE = 384
+TILES = ROWS // TILE
 DEPTH = 2 * HEAD + 16
 
 
 def attend_body(turns, ids, q0_ref, q1_ref, kvg_ref, out0_ref, out1_ref, ka_ref):
     z, x = ids[0], ids[1]
-    step = pl.program_id(0)
-    per = ROWS // QT
-    early = step < per
-    sub = lax.rem(step, per)
-    xq = lax.rem(x + jnp.where(early, turns[0], turns[1]), NX)
-
-    @pl.when(step == 0)
-    def _():
-        ka_ref[:, 0:HEAD, :] = kvg_ref[:, 0:HEAD, :]
-        ka_ref[:, HEAD:DEPTH, :] = kvg_ref[:, 0:KG, :]
-
-    q0, q1 = q0_ref[...].astype(F32), q1_ref[...].astype(F32)
-    scaled = jnp.where(early, q0, q1).T * (0.125 * LOG2E)
-    hi = scaled.astype(BF16)
-    lo = (scaled - hi.astype(F32)).astype(BF16)
-    qa = jnp.concatenate([hi, lo, jnp.ones((QT, 16), BF16)], axis=1)
-
-    def update(chunk, carry, masked):
-        peak, acc = carry
-        s = dot(qa, ka_ref[chunk])
-        if masked:
-            row = lax.broadcasted_iota(jnp.int32, (QT, ROWS), 0) + sub * QT
-            col = lax.broadcasted_iota(jnp.int32, (QT, ROWS), 1)
-            s = jnp.where(col <= row, s, NEG)
+    ka_ref[:, 0:HEAD, :] = kvg_ref[:, 0:HEAD, :]
+    ka_ref[:, HEAD:DEPTH, :] = kvg_ref[:, 0:KG, :]
+    tiles = []
+    for ref in (q0_ref, q1_ref):
+        scaled = ref[...].astype(F32).T * (0.125 * LOG2E)
+        hi = scaled.astype(BF16)
+        lo = (scaled - hi.astype(F32)).astype(BF16)
+        rows = jnp.concatenate([hi, lo, jnp.ones((ROWS, 16), BF16)], axis=1)
+        tiles += [rows[i * TILE : (i + 1) * TILE] for i in range(TILES)]
+
+    def weigh(s, values, peak, acc):
         new_peak = jnp.maximum(peak, jnp.max(s, axis=1, keepdims=True))
         w = jnp.exp2(s - new_peak).astype(BF16)
-        acc = acc * jnp.exp2(peak - new_peak) + dot_t(w, kvg_ref[chunk, KG:KVG, :])
-        return new_peak, acc
-
-    start = (jnp.full((QT, 1), NEG, F32), jnp.zeros((QT, HEAD), F32))
-    full = jnp.where(xq > x, z + 1, z)
-    carry = lax.fori_loop(0, full, lambda i, c: update(i, c, False), start)
-    peak, acc = lax.cond(xq == x, lambda c: update(z, c, True), lambda c: c, carry)
-    p_hi, p_mid, p_lo = three_pieces(peak)
-    lane = lax.broadcasted_iota(jnp.int32, (QT, HEAD), 1)
-    tail = jnp.where(
-        lane == 0,
-        p_hi.astype(F32),
-        jnp.where(
-            lane == 1, p_mid.astype(F32), jnp.where(lane == 2, p_lo.astype(F32), jnp.zeros((), F32))
-        ),
-    )
-    out = jnp.concatenate([acc, tail], axis=1).astype(BF16)
-    at = pl.ds(pl.multiple_of(sub * QT, QT), QT)
-
-    @pl.when(early)
-    def _():
-        out0_ref[at, :] = out
-
-    @pl.when(jnp.logical_not(early))
-    def _():
-        out1_ref[at, :] = out
+        return new_peak, acc * jnp.exp2(peak - new_peak) + dot_t(w, values)
+
+    def update(chunk, carry, some, masked):
+        k, values = ka_ref[chunk], kvg_ref[chunk, KG:KVG, :]
+        scores = [dot(tile, k) for tile in some]
+        if masked:
+            for i in range(TILES):
+                row = lax.broadcasted_iota(jnp.int32, (TILE, ROWS), 0) + i * TILE
+                col = lax.broadcasted_iota(jnp.int32, (TILE, ROWS), 1)
+                scores[i] = jnp.where(col <= row, scores[i], NEG)
+        return tuple(weigh(s, values, *c) for s, c in zip(scores, carry))
+
+    start = ((jnp.full((TILE, 1), NEG, F32), jnp.zeros((TILE, HEAD), F32)),) * (2 * TILES)
+    carry = lax.fori_loop(0, z, lambda i, c: update(i, c, tiles, False), start)
+    lane = lax.broadcasted_iota(jnp.int32, (ROWS, HEAD), 1)
+    for n, (turn, ref) in enumerate(zip(turns, (out0_ref, out1_ref))):
+        mine = slice(n * TILES, (n + 1) * TILES)
+        if turn == 0:
+            last = update(z, carry[mine], tiles[mine], True)
+        else:
+            last = lax.cond(
+                lax.rem(x + turn, NX) > x,
+                lambda c, some=tiles[mine]: update(z, c, some, False),
+                lambda c: c,
+                carry[mine],
+            )
+        acc = jnp.concatenate([c[1] for c in last], axis=0)
+        p_hi, p_mid, p_lo = three_pieces(jnp.concatenate([c[0] for c in last], axis=0))
+        tail = jnp.where(
+            lane == 0,
+            p_hi.astype(F32),
+            jnp.where(
+                lane == 1,
+                p_mid.astype(F32),
+                jnp.where(lane == 2, p_lo.astype(F32), jnp.zeros((), F32)),
+            ),
+        )
+        ref[...] = jnp.concatenate([acc, tail], axis=1).astype(BF16)
 
 
 def combine_body(ids, gain_ref, *refs):
@@ -215,23 +215,23 @@
     )
 
 
-def split_down_body(ids, own_ref, got_ref, shared_ref, *outs):
-    for turn, out_ref in enumerate(outs):
-        to = lax.rem(ids[3] + turn, NY)
-        cols = pl.ds(pl.multiple_of(to * 256, 256), 256)
-        for l in range(LOCAL):
-            out_ref[l * 128 : l * 128 + 64, :] = own_ref[l, :, cols]
-            out_ref[l * 128 + 64 : l * 128 + 128, :] = got_ref[256 + l * 64 : 320 + l * 64, cols]
-        out_ref[256:288, :] = shared_ref[:, cols]
-        out_ref[288:320, :] = got_ref[448:480, cols]
-
-
 def gated(g, u):
     return g / (1.0 + jnp.exp(-g)) * u
 
 
-def hidden_body(
-    ids, x_ref, gate_ref, up_ref, got_ref, normed_ref, sgate_ref, sup_ref, source_ref, out_ref
+def experts_body(
+    ids,
+    x_ref,
+    gate_ref,
+    up_ref,
+    down_ref,
+    got_ref,
+    normed_ref,
+    sgate_ref,
+    sup_ref,
+    sdown_ref,
+    source_ref,
+    out_ref,
 ):
     c = ids[2]
     x = x_ref[...]
@@ -246,31 +246,25 @@
         g = dot_t(rows0, wg[:, : D // 2]) + dot_t(rows1, wg[:, D // 2 :])
         u = dot_t(rows0, wu[:, : D // 2]) + dot_t(rows1, wu[:, D // 2 :])
         h = gated(g, u).astype(BF16)
+        wd = jnp.concatenate([down_ref[l], got_ref[256 + l * 64 : 320 + l * 64, :]], axis=0)
         for y in range(NY):
-            out_ref[y, l * n : (l + 1) * n, :] = h
+            out_ref[y, l * n : (l + 1) * n, :] = dot(h, wd[:, y * 256 : y * 256 + 256]).astype(BF16)
     tokens = normed_ref[pl.ds(pl.multiple_of(c * 64, 64), 64), :]
     wg = jnp.concatenate([sgate_ref[...], got_ref[384:416, :]], axis=0)
     wu = jnp.concatenate([sup_ref[...], got_ref[416:448, :]], axis=0)
-    h = gated(dot_t(tokens, wg), dot_t(tokens, wu))
-    h = jnp.concatenate([h, jnp.zeros((64, 64), F32)], axis=1).astype(BF16)
+    h = gated(dot_t(tokens, wg), dot_t(tokens, wu)).astype(BF16)
+    wd = jnp.concatenate([sdown_ref[...], got_ref[448:480, :]], axis=0)
     for y in range(NY):
-        out_ref[y, SLOTS : SLOTS + 64, :] = h
-
-
-def down_body(ids, h_ref, table_ref, *rest):
-    weights, (out_ref, shared_ref) = rest[:NY], rest[NY:]
-    n = SLOTS // 2
-    rows = [jnp.zeros((n, 256), F32) for _ in range(LOCAL)]
-    shared = jnp.zeros((64, 256), F32)
-    for turn, w_ref in enumerate(weights):
-        y = lax.rem(ids[3] + NY - turn, NY)
-        h = h_ref[y]
-        for l in range(LOCAL):
-            rows[l] = rows[l] + dot(h[l * n : (l + 1) * n], w_ref[l * 128 : l * 128 + 128, :])
-        shared = shared + dot(h[SLOTS : SLOTS + 64, 0:64], w_ref[256:320, :])
-    rows = [r.astype(BF16) for r in rows]
-    shared_ref[...] = shared
-    rows = jnp.concatenate(rows, axis=0)
+        part = dot(h, wd[:, y * 256 : y * 256 + 256])
+        out_ref[y, SLOTS : SLOTS + 64, :] = part.astype(BF16)
+
+
+def sum_body(ids, part_ref, table_ref, out_ref, shared_ref):
+    total = jnp.zeros((SLOTS + 64, 256), F32)
+    for y in range(NY):
+        total = total + part_ref[y].astype(F32)
+    shared_ref[...] = total[SLOTS:]
+    rows = total[:SLOTS].astype(BF16)
     lane = lax.broadcasted_iota(jnp.int32, (2 * SLOTS, SLOTS), 1)
     place = jnp.where(lane == table_ref[:, 3:4], 1.0, 0.0)
     half = table_ref[:, 2:3]
@@ -375,50 +369,48 @@
         lax.ppermute(mine, "x", [((i + d) % NX, i) for i in range(NX)]) for d in range(1, NX)
     ]
 
-    down_sent = call(
-        split_down_body,
-        (jax.ShapeDtypeStruct((320, 256), BF16),) * NY,
-        ids,
-        (1,),
-        [pl.BlockSpec((LOCAL, 64, D), lambda i, s: (s[2], 0, 0)), whole((480, D)), whole((32, D))],
-        (whole((320, 256)),) * NY,
-        (expert_down, got, shared_down),
-        flops=1_000_000_000,
-    )
-    down = [down_sent[0]] + [
-        lax.ppermute(down_sent[r], "y", [(i, (i + r) % NY) for i in range(NY)])
-        for r in range(1, NY)
-    ]
-
-    hidden_sent = call(
-        hidden_body,
-        jax.ShapeDtypeStruct((NY, SLOTS + 64, 128), BF16),
+    mine = pl.BlockSpec((LOCAL, 64, D), lambda i, s: (s[2], 0, 0))
+    products = call(
+        experts_body,
+        jax.ShapeDtypeStruct((NY, SLOTS + 64, 256), BF16),
         ids,
         (1,),
         [
             whole((2 * SLOTS, D // 2)),
-            pl.BlockSpec((LOCAL, 64, D), lambda i, s: (s[2], 0, 0)),
-            pl.BlockSpec((LOCAL, 64, D), lambda i, s: (s[2], 0, 0)),
+            mine,
+            mine,
+            mine,
             whole((480, D)),
             whole((TOK, D)),
             whole((32, D)),
             whole((32, D)),
+            whole((32, D)),
             whole((SLOTS, 8)),
         ],
-        whole((NY, SLOTS + 64, 128)),
-        (arrived, expert_gate, expert_up, got, normed, shared_gate, shared_up, source),
+        whole((NY, SLOTS + 64, 256)),
+        (
+            arrived,
+            expert_gate,
+            expert_up,
+            expert_down,
+            got,
+            normed,
+            shared_gate,
+            shared_up,
+            shared_down,
+            source,
+        ),
         flops=1_000_000_000,
     )
-    hidden = lax.all_to_all(hidden_sent, "y", 0, 0, tiled=True)
+    products = lax.all_to_all(products, "y", 0, 0, tiled=True)
 
     def attend(turns):
         return call(
             functools.partial(attend_body, turns),
             (jax.ShapeDtypeStruct((ROWS, 128), BF16),) * 2,
             ids,
-            (2 * (ROWS // QT),),
-            [pl.BlockSpec((HEAD, QT), lambda i, s: (0, lax.rem(i, ROWS // QT)))] * 2
-            + [whole((NZ, KVG, ROWS))],
+            (1,),
+            [whole((HEAD, ROWS))] * 2 + [whole((NZ, KVG, ROWS))],
             (whole((ROWS, 128)),) * 2,
             (q_all[turns[0]], q_all[turns[1]], kvg),
             scratch=[pltpu.VMEM((NZ, DEPTH, ROWS), BF16)],
@@ -431,23 +423,23 @@
     part1, part2 = attend((1, 2))
     part1, part2 = send_part(part1, 1), send_part(part2, 2)
 
+    part3, part0 = attend((3, 0))
+    part3 = send_part(part3, 3)
+
     rows, shared = call(
-        down_body,
+        sum_body,
         (
             jax.ShapeDtypeStruct((2 * SLOTS, 128), BF16),
             jax.ShapeDtypeStruct((64, 256), F32),
         ),
         ids,
         (1,),
-        [whole((NY, SLOTS + 64, 128)), whole((2 * SLOTS, 8))] + [whole((320, 256))] * NY,
+        [whole((NY, SLOTS + 64, 256)), whole((2 * SLOTS, 8))],
         (whole((2 * SLOTS, 128)), whole((64, 256))),
-        (hidden, table, *down),
+        (products, table),
         flops=1_000_000_000,
     )
     returned = lax.all_to_all(rows, ("z", "x"), 0, 0, tiled=True)
-
-    part3, part0 = attend((3, 0))
-    part3 = send_part(part3, 3)
 
     mixed = call(
         combine_body,

time: 233 us -> 182 us (0.78)
  the two profiles are of different devices: /device:TPU:505 before, /device:TPU:449 now
where the time goes in v2:
time: 182 us; the launch traced here: 181 us
  Pallas kernels  64.8 us (36%)
  starting transfers between devices  49.3 us (27%)
  waiting for transfers between devices  44.3 us (24%)
  between operations  14.2 us (8%)
  local copies, waits for them, and re-layouts  6.66 us (4%)
  other arithmetic  2.12 us (1%)
    pallas_call x9, Pallas kernels, call(): pl.pallas_call(body, out_shape=out_shape, grid_spec=pltpu.PrefetchScalarG...  64.8 us
    all_to_all x1, waiting for transfers between devices, on_device(): arrived = lax.all_to_all(sent, ('z', 'x'), 0, 0, tiled=True)  28.8 us
    all_to_all x1, starting transfers between devices, on_device(): returned = lax.all_to_all(rows, ('z', 'x'), 0, 0, tiled=True)  13.9 us
    all_to_all x1, waiting for transfers between devices, on_device(): products = lax.all_to_all(products, 'y', 0, 0, tiled=True)  9.32 us
    ppermute x3, starting transfers between devices, on_device(): lax.ppermute(mine, 'x', [((i + d) % NX, i) for i in range(NX)])  7.85 us
    ppermute x3, starting transfers between devices, send_part(): return lax.ppermute(part, 'x', [(i, (i + d) % NX) for i in range(NX)])  7.34 us
    all_to_all x1, starting transfers between devices, on_device(): products = lax.all_to_all(products, 'y', 0, 0, tiled=True)  7.15 us
    unnamed x28, local copies, waits for them, and re-layouts  6.66 us
  transfers between devices with their start and end apart: 12, of which 4 were waited for; matrix products, arithmetic and copies ran while one was open for 1% of the time, Pallas kernels for 32%

profile of v2, /device:TPU:449, one launch (start us, length us, event | category | flops | bytes accessed | tf_op | source)
XLA Modules:
  0.0 181.4 jit_solution(14516140575104748679)
XLA Ops:
  7.2 0.7 pad_add_fusion.ids
  7.8 2.4 %shard_map.176.after_ref = bf16[144,768]{1,0:T(8,128)(2,1)} custom-call(s32[4]{0:T(128)} %pad_add_fusion.ids, bf16[64,768]{1,0:T(8,128)(2,1)} %bitcast.21, bf16[64,768]{1,0:T(8,128)(2,1)} %bitcast.22, f32[1,768]{1,0:T(1,128)} %bitcast.24), custom_call_target="tpu_custom_call" | custom-call | bytes 4194304 | tf_op jit(solution)/shard_map/pallas_call | solution.py:73
  10.2 4.3 %shard_map.177 = (bf16[128,2048]{1,0:T(8,128)(2,1)}, bf16[768,1024]{1,0:T(8,128)(2,1)}) custom-call(s32[4]{0:T(128)} %pad_add_fusion.ids, bf16[128,2048]{1,0:T(8,128)(2,1)} %x_ref.1, f32[1,2048]{1,0:T(1,128)} %bitcast.33, s32[4,128]{1,0:T(4,128)} %bitcast.25, s32[768,8]{1,0:T(8,128)} %constant.22.clone.table_ref, bf16[144,768]{1,0:T(8,128)(2,1)} %shard_map.176.after_ref), custom_call_target="tpu_custom_call" | custom-call | flops 1000000000 | bytes 4194304 | tf_op jit(solution)/shard_map/pallas_call | solution.py:73
  14.5 6.6 %all-to-all-start = ((bf16[32,24,1024]{2,1,0:T(8,128)(2,1)}), bf16[32,24,1024]{2,1,0:T(8,128)(2,1)S(1)}, u32[]{:S(2)}, u32[]{:S(2)}) async-start(bf16[32,24,1024]{2,1,0:T(8,128)(2,1)} %bitcast.18), calls=%async_computation | async-start | bytes 3145728 | tf_op jit(solution)/shard_map/all_to_all | solution.py:352
  21.2 0.0 all-gather.2.cloned.1.call-start
  21.2 3.6 %shard_map.178 = bf16[480,2048]{1,0:T(8,128)(2,1)} custom-call(s32[4]{0:T(128)} %pad_add_fusion.ids, bf16[4,64,2048]{2,1,0:T(8,128)(2,1)} %gate_ref.3, bf16[4,64,2048]{2,1,0:T(8,128)(2,1)} %up_ref.3, bf16[4,64,2048]{2,1,0:T(8,128)(2,1)} %down_ref.3, bf16[32,2048]{1,0:T(8,128)(2,1)} %sgate_ref.3, bf16[32,2048]{1,0:T(8,128)(2,1)} %sup_ref.3, ...), custom_call_target="tpu_custom_call" | custom-call | flops 1000000000 | bytes 4194304 | tf_op jit(solution)/shard_map/pallas_call | solution.py:73
  24.8 3.1 %collective-permute-start.6 = (bf16[480,2048]{1,0:T(8,128)(2,1)}, bf16[480,2048]{1,0:T(8,128)(2,1)S(1)}, u32[]{:S(2)}, u32[]{:S(2)}) collective-permute-start(bf16[480,2048]{1,0:T(8,128)(2,1)} %shard_map.178), channel_id=1, source_target_pairs={{0,1},{1,0},{2,3},{3,2},{4,5},{5,4},{6,7},{7,6},{8,9},{9,8},{10,11... | collective-permute-start | bytes 5898248 | tf_op jit(solution)/shard_map/ppermute | solution.py:365
  27.9 0.0 all-gather.2.cloned.1.call-update
  28.0 3.8 %collective-permute-done.6.got_ref = bf16[480,2048]{1,0:T(8,128)(2,1)S(1)} collective-permute-done((bf16[480,2048]{1,0:T(8,128)(2,1)}, bf16[480,2048]{1,0:T(8,128)(2,1)S(1)}, u32[]{:S(2)}, u32[]{:S(2)}) %collective-permute-start.6) | collective-permute-done | bytes 1966112 | tf_op jit(solution)/shard_map/ppermute | solution.py:365
  31.7 0.0 copy-start.1
  31.7 28.8 %all-to-all-done = bf16[32,24,1024]{2,1,0:T(8,128)(2,1)S(1)} async-done(((bf16[32,24,1024]{2,1,0:T(8,128)(2,1)}), bf16[32,24,1024]{2,1,0:T(8,128)(2,1)S(1)}, u32[]{:S(2)}, u32[]{:S(2)}) %all-to-all-start) | async-done | bytes 1572896 | tf_op jit(solution)/shard_map/all_to_all | solution.py:352
  60.5 0.0 copy-start
  60.5 0.0 copy-done.1
  60.5 1.2 copy-done
  61.7 7.9 %shard_map.182 = bf16[8,448,256]{2,1,0:T(8,128)(2,1)} custom-call(s32[4]{0:T(128)} %pad_add_fusion.ids, bf16[768,1024]{1,0:T(8,128)(2,1)} %bitcast.17, bf16[4,64,2048]{2,1,0:T(8,128)(2,1)} %gate_ref.3, bf16[4,64,2048]{2,1,0:T(8,128)(2,1)} %up_ref.3, bf16[4,64,2048]{2,1,0:T(8,128)(2,1)} %down_ref.3, bf16[480,2048]{1,0:T(8,128)(2,1)} %copy-done.1, ...), custom_call_target="tpu_custom_call" | custom-call | flops 1000000000 | bytes 4194304 | tf_op jit(solution)/shard_map/pallas_call | solution.py:73
  69.6 0.0 copy-start.9
  69.6 7.2 %all-to-all-start.1 = ((bf16[8,448,256]{2,1,0:T(8,128)(2,1)}), bf16[8,448,256]{2,1,0:T(8,128)(2,1)S(1)}, u32[]{:S(2)}, u32[]{:S(2)}) async-start(bf16[8,448,256]{2,1,0:T(8,128)(2,1)} %shard_map.182), calls=%async_computation.1 | async-start | bytes 3670016 | tf_op jit(solution)/shard_map/all_to_all | solution.py:405
  76.8 0.0 copy-done.9
  76.8 3.4 %collective-permute-start.1 = (bf16[64,768]{1,0:T(8,128)(2,1)S(1)}, bf16[64,768]{1,0:T(8,128)(2,1)S(1)}, u32[]{:S(2)}, u32[]{:S(2)}) collective-permute-start(bf16[64,768]{1,0:T(8,128)(2,1)S(1)} %bitcast.30), channel_id=1, source_target_pairs={{16,0},{32,16},{48,32},{0,48},{17,1},{33,17},{49,33},{1,49},{18,2}... | collective-permute-start | bytes 294920 | tf_op jit(solution)/shard_map/ppermute | solution.py:369
  80.2 2.2 %collective-permute-start.2 = (bf16[64,768]{1,0:T(8,128)(2,1)S(1)}, bf16[64,768]{1,0:T(8,128)(2,1)S(1)}, u32[]{:S(2)}, u32[]{:S(2)}) collective-permute-start(bf16[64,768]{1,0:T(8,128)(2,1)S(1)} %bitcast.31), channel_id=1, source_target_pairs={{32,0},{48,16},{0,32},{16,48},{33,1},{49,17},{1,33},{17,49},{34,2}... | collective-permute-start | bytes 294920 | tf_op jit(solution)/shard_map/ppermute | solution.py:369
  82.4 2.3 %collective-permute-start = (bf16[64,768]{1,0:T(8,128)(2,1)S(1)}, bf16[64,768]{1,0:T(8,128)(2,1)S(1)}, u32[]{:S(2)}, u32[]{:S(2)}) collective-permute-start(bf16[64,768]{1,0:T(8,128)(2,1)S(1)} %bitcast.32), channel_id=1, source_target_pairs={{48,0},{0,16},{16,32},{32,48},{49,1},{1,17},{17,33},{33,49},{50,2}... | collective-permute-start | bytes 294920 | tf_op jit(solution)/shard_map/ppermute | solution.py:369
  84.6 0.0 collective-permute-done.1.q0_ref
  84.7 0.0 copy-start.11
  84.7 2.4 %collective-permute-done.2.q1_ref = bf16[64,768]{1,0:T(8,128)(2,1)S(1)} collective-permute-done((bf16[64,768]{1,0:T(8,128)(2,1)S(1)}, bf16[64,768]{1,0:T(8,128)(2,1)S(1)}, u32[]{:S(2)}, u32[]{:S(2)}) %collective-permute-start.2) | collective-permute-done | bytes 98336 | tf_op jit(solution)/shard_map/ppermute | solution.py:369
  87.0 0.0 copy-start.12
  87.1 0.0 all-gather.2.cloned.1.call-done
  87.1 0.0 copy-done.11
  87.1 0.6 copy-done.12
  87.7 18.3 %shard_map.180 = (bf16[768,128]{1,0:T(8,128)(2,1)}, bf16[768,128]{1,0:T(8,128)(2,1)}) custom-call(s32[4]{0:T(128)} %pad_add_fusion.ids, bf16[64,768]{1,0:T(8,128)(2,1)} %copy-done.11, bf16[64,768]{1,0:T(8,128)(2,1)} %copy-done.12, bf16[8,144,768]{2,1,0:T(8,128)(2,1)} %bitcast.27), custom_call_target="tpu_custom_call" | custom-call | flops 10000000000 | bytes 4194304 | tf_op jit(solution)/shard_map/pallas_call | solution.py:73
  106.0 2.0 %collective-permute-start.3 = (bf16[768,128]{1,0:T(8,128)(2,1)}, bf16[768,128]{1,0:T(8,128)(2,1)S(1)}, u32[]{:S(2)}, u32[]{:S(2)}) collective-permute-start(bf16[768,128]{1,0:T(8,128)(2,1)} %get-tuple-element.16), channel_id=1, source_target_pairs={{0,16},{16,32},{32,48},{48,0},{1,17},{17,33},{33,49},{49,1},{2,18}... | collective-permute-start | bytes 589832 | tf_op jit(solution)/shard_map/ppermute | solution.py:421
  108.0 1.9 %collective-permute-start.4 = (bf16[768,128]{1,0:T(8,128)(2,1)}, bf16[768,128]{1,0:T(8,128)(2,1)S(1)}, u32[]{:S(2)}, u32[]{:S(2)}) collective-permute-start(bf16[768,128]{1,0:T(8,128)(2,1)} %get-tuple-element.17), channel_id=1, source_target_pairs={{0,32},{16,48},{32,0},{48,16},{1,33},{17,49},{33,1},{49,17},{2,34}... | collective-permute-start | bytes 589832 | tf_op jit(solution)/shard_map/ppermute | solution.py:421
  109.9 9.3 %all-to-all-done.1.part_ref = bf16[8,448,256]{2,1,0:T(8,128)(2,1)S(1)} async-done(((bf16[8,448,256]{2,1,0:T(8,128)(2,1)}), bf16[8,448,256]{2,1,0:T(8,128)(2,1)S(1)}, u32[]{:S(2)}, u32[]{:S(2)}) %all-to-all-start.1) | async-done | bytes 1835040 | tf_op jit(solution)/shard_map/all_to_all | solution.py:405
  119.2 0.0 copy-start.2
  119.2 1.3 copy-done.2
  120.5 3.7 %shard_map.183 = (bf16[768,128]{1,0:T(8,128)(2,1)}, f32[64,256]{1,0:T(8,128)}) custom-call(s32[4]{0:T(128)} %pad_add_fusion.ids, bf16[8,448,256]{2,1,0:T(8,128)(2,1)} %copy-done.2, s32[768,8]{1,0:T(8,128)} %constant.22.clone.table_ref), custom_call_target="tpu_custom_call" | custom-call | flops 1000000000 | bytes 4194304 | tf_op jit(solution)/shard_map/pallas_call | solution.py:73
  124.2 13.9 %all-to-all-start.2 = ((bf16[32,24,128]{2,1,0:T(8,128)(2,1)}), bf16[32,24,128]{2,1,0:T(8,128)(2,1)S(1)}, u32[]{:S(2)}, u32[]{:S(2)}) async-start(bf16[32,24,128]{2,1,0:T(8,128)(2,1)} %bitcast.20), calls=%async_computation.2 | async-start | bytes 393216 | tf_op jit(solution)/shard_map/all_to_all | solution.py:442
  138.1 0.0 copy-start.7
  138.1 0.0 copy-start.8
  138.1 0.0 collective-permute-done.q0_ref
  138.2 0.0 copy-start.10
  138.2 0.6 copy-done.10
  138.8 17.7 %shard_map.179 = (bf16[768,128]{1,0:T(8,128)(2,1)}, bf16[768,128]{1,0:T(8,128)(2,1)}) custom-call(s32[4]{0:T(128)} %pad_add_fusion.ids, bf16[64,768]{1,0:T(8,128)(2,1)} %copy-done.10, bf16[64,768]{1,0:T(8,128)(2,1)} %bitcast.29, bf16[8,144,768]{2,1,0:T(8,128)(2,1)} %bitcast.28), custom_call_target="tpu_custom_call" | custom-call | flops 10000000000 | bytes 4194304 | tf_op jit(solution)/shard_map/pallas_call | solution.py:73
  156.4 3.5 %collective-permute-start.5 = (bf16[768,128]{1,0:T(8,128)(2,1)}, bf16[768,128]{1,0:T(8,128)(2,1)S(1)}, u32[]{:S(2)}, u32[]{:S(2)}) collective-permute-start(bf16[768,128]{1,0:T(8,128)(2,1)} %get-tuple-element.18), channel_id=1, source_target_pairs={{0,48},{16,0},{32,16},{48,32},{1,49},{17,1},{33,17},{49,33},{2,50}... | collective-permute-start | bytes 589832 | tf_op jit(solution)/shard_map/ppermute | solution.py:421
  159.9 0.0 copy-done.7
  159.9 0.7 copy.19.routes_ref
  160.7 0.0 copy-done.8
  160.7 0.7 copy.20.weight_ref
  161.4 0.0 all-to-all-done.2
  161.4 0.0 copy-start.3
  161.4 0.7 copy-done.3
  162.1 3.2 %shard_map.184 = (f32[128,128]{1,0:T(8,128)}, f32[128,128]{1,0:T(8,128)}) custom-call(s32[4]{0:T(128)} %pad_add_fusion.ids, bf16[768,128]{1,0:T(8,128)(2,1)} %bitcast.19, s32[128,4]{1,0:T(8,128)} %copy.19.routes_ref, f32[128,4]{1,0:T(8,128)} %copy.20.weight_ref, s32[8,768]{1,0:T(8,128)} %constant.28.table_ref, f32[64,256]{1,0:T(8,128)} %get-tuple-element.21.shared_ref), custom_call_target="tpu_custom_call" | custom-call | flops 1000000000 | bytes 4194304 | tf_op jit(solution)/shard_map/pallas_call | solution.py:73
  165.3 3.2 %collective-permute-start.7 = (f32[128,128]{1,0:T(8,128)}, f32[128,128]{1,0:T(8,128)S(1)}, u32[]{:S(2)}, u32[]{:S(2)}) collective-permute-start(f32[128,128]{1,0:T(8,128)} %get-tuple-element.23), channel_id=1, source_target_pairs={{0,1},{1,0},{2,3},{3,2},{4,5},{5,4},{6,7},{7,6},{8,9},{9,8},{10,11... | collective-permute-start | bytes 196616 | tf_op jit(solution)/shard_map/ppermute | solution.py:470
  168.5 0.0 collective-permute-done.3.refs_1_
  168.5 0.0 copy-start.4
  168.5 0.0 collective-permute-done.4.refs_2_
  168.5 0.0 copy-start.5
  168.6 0.0 collective-permute-done.5.refs_3_
  168.6 0.0 copy-start.6
  168.6 0.6 copy-done.4
  169.2 0.1 copy-done.5
  169.3 0.1 copy-done.6
  169.3 3.8 %shard_map.181 = bf16[64,768]{1,0:T(8,128)(2,1)} custom-call(s32[4]{0:T(128)} %pad_add_fusion.ids, f32[1,64]{1,0:T(1,128)} %bitcast.26, bf16[768,128]{1,0:T(8,128)(2,1)} %get-tuple-element.15.refs_0_, bf16[768,128]{1,0:T(8,128)(2,1)} %copy-done.4, bf16[768,128]{1,0:T(8,128)(2,1)} %copy-done.5, bf16[768,128]{1,0:T(8,128)(2,1)} %copy-done.6), custom_call_target="tpu_custom_call" | custom-call | bytes 4194304 | tf_op jit(solution)/shard_map/pallas_call | solution.py:73
  173.1 0.0 collective-permute-done.7
  173.1 1.5 add_convert_fusion
Async XLA Ops:
  14.5 46.0 %all-to-all-start = ((bf16[32,24,1024]{2,1,0:T(8,128)(2,1)}), bf16[32,24,1024]{2,1,0:T(8,128)(2,1)S(1)}, u32[]{:S(2)}, u32[]{:S(2)}) async-start(bf16[32,24,1024]{2,1,0:T(8,128)(2,1)} %bitcast.18), calls=%async_computation | async-start | bytes 3145728 | tf_op jit(solution)/shard_map/all_to_all | solution.py:352
  21.2 65.9 %all-gather.2.cloned.1.call-start = ((), (), s32[]{:S(2)}) async-start(), calls=%async_computation.3 | async-start | bytes 1990656 | tf_op jit(solution)/shard_map/all_gather | solution.py:337
  24.8 6.9 %collective-permute-start.6 = (bf16[480,2048]{1,0:T(8,128)(2,1)}, bf16[480,2048]{1,0:T(8,128)(2,1)S(1)}, u32[]{:S(2)}, u32[]{:S(2)}) collective-permute-start(bf16[480,2048]{1,0:T(8,128)(2,1)} %shard_map.178), channel_id=1, source_target_pairs={{0,1},{1,0},{2,3},{3,2},{4,5},{5,4},{6,7},{7,6},{8,9},{9,8},{10,11... | collective-permute-start | bytes 5898248 | tf_op jit(solution)/shard_map/ppermute | solution.py:365
  31.7 28.8 %copy-start.1 = (bf16[480,2048]{1,0:T(8,128)(2,1)}, bf16[480,2048]{1,0:T(8,128)(2,1)S(1)}, u32[]{:S(2)}) copy-start(bf16[480,2048]{1,0:T(8,128)(2,1)S(1)} %collective-permute-done.6.got_ref) | copy-start | bytes 5898244
  60.5 1.2 copy-start
  69.6 7.2 %copy-start.9 = (bf16[768,64]{0,1:T(8,128)(2,1)S(1)}, bf16[768,64]{0,1:T(8,128)(2,1)}, u32[]{:S(2)}) copy-start(bf16[768,64]{0,1:T(8,128)(2,1)} %param.17) | copy-start | bytes 294916
  69.6 49.6 %all-to-all-start.1 = ((bf16[8,448,256]{2,1,0:T(8,128)(2,1)}), bf16[8,448,256]{2,1,0:T(8,128)(2,1)S(1)}, u32[]{:S(2)}, u32[]{:S(2)}) async-start(bf16[8,448,256]{2,1,0:T(8,128)(2,1)} %shard_map.182), calls=%async_computation.1 | async-start | bytes 3670016 | tf_op jit(solution)/shard_map/all_to_all | solution.py:405
  76.8 7.9 %collective-permute-start.1 = (bf16[64,768]{1,0:T(8,128)(2,1)S(1)}, bf16[64,768]{1,0:T(8,128)(2,1)S(1)}, u32[]{:S(2)}, u32[]{:S(2)}) collective-permute-start(bf16[64,768]{1,0:T(8,128)(2,1)S(1)} %bitcast.30), channel_id=1, source_target_pairs={{16,0},{32,16},{48,32},{0,48},{17,1},{33,17},{49,33},{1,49},{18,2}... | collective-permute-start | bytes 294920 | tf_op jit(solution)/shard_map/ppermute | solution.py:369
  80.2 6.9 %collective-permute-start.2 = (bf16[64,768]{1,0:T(8,128)(2,1)S(1)}, bf16[64,768]{1,0:T(8,128)(2,1)S(1)}, u32[]{:S(2)}, u32[]{:S(2)}) collective-permute-start(bf16[64,768]{1,0:T(8,128)(2,1)S(1)} %bitcast.31), channel_id=1, source_target_pairs={{32,0},{48,16},{0,32},{16,48},{33,1},{49,17},{1,33},{17,49},{34,2}... | collective-permute-start | bytes 294920 | tf_op jit(solution)/shard_map/ppermute | solution.py:369
  82.4 55.8 %collective-permute-start = (bf16[64,768]{1,0:T(8,128)(2,1)S(1)}, bf16[64,768]{1,0:T(8,128)(2,1)S(1)}, u32[]{:S(2)}, u32[]{:S(2)}) collective-permute-start(bf16[64,768]{1,0:T(8,128)(2,1)S(1)} %bitcast.32), channel_id=1, source_target_pairs={{48,0},{0,16},{16,32},{32,48},{49,1},{1,17},{17,33},{33,49},{50,2}... | collective-permute-start | bytes 294920 | tf_op jit(solution)/shard_map/ppermute | solution.py:369
  84.7 2.4 %copy-start.11 = (bf16[64,768]{1,0:T(8,128)(2,1)}, bf16[64,768]{1,0:T(8,128)(2,1)S(1)}, u32[]{:S(2)}) copy-start(bf16[64,768]{1,0:T(8,128)(2,1)S(1)} %collective-permute-done.1.q0_ref) | copy-start | bytes 294916
  87.0 0.6 copy-start.12
  106.0 62.5 %collective-permute-start.3 = (bf16[768,128]{1,0:T(8,128)(2,1)}, bf16[768,128]{1,0:T(8,128)(2,1)S(1)}, u32[]{:S(2)}, u32[]{:S(2)}) collective-permute-start(bf16[768,128]{1,0:T(8,128)(2,1)} %get-tuple-element.16), channel_id=1, source_target_pairs={{0,16},{16,32},{32,48},{48,0},{1,17},{17,33},{33,49},{49,1},{2,18}... | collective-permute-start | bytes 589832 | tf_op jit(solution)/shard_map/ppermute | solution.py:421
  108.0 60.6 %collective-permute-start.4 = (bf16[768,128]{1,0:T(8,128)(2,1)}, bf16[768,128]{1,0:T(8,128)(2,1)S(1)}, u32[]{:S(2)}, u32[]{:S(2)}) collective-permute-start(bf16[768,128]{1,0:T(8,128)(2,1)} %get-tuple-element.17), channel_id=1, source_target_pairs={{0,32},{16,48},{32,0},{48,16},{1,33},{17,49},{33,1},{49,17},{2,34}... | collective-permute-start | bytes 589832 | tf_op jit(solution)/shard_map/ppermute | solution.py:421
  119.2 1.3 copy-start.2
  124.2 37.3 %all-to-all-start.2 = ((bf16[32,24,128]{2,1,0:T(8,128)(2,1)}), bf16[32,24,128]{2,1,0:T(8,128)(2,1)S(1)}, u32[]{:S(2)}, u32[]{:S(2)}) async-start(bf16[32,24,128]{2,1,0:T(8,128)(2,1)} %bitcast.20), calls=%async_computation.2 | async-start | bytes 393216 | tf_op jit(solution)/shard_map/all_to_all | solution.py:442
  138.1 21.8 %copy-start.7 = (s32[128,4]{0,1:T(4,128)S(1)}, s32[128,4]{0,1:T(4,128)}, u32[]{:S(2)}) copy-start(s32[128,4]{0,1:T(4,128)} %param.24) | copy-start | bytes 6148
  138.1 22.6 %copy-start.8 = (f32[128,4]{0,1:T(4,128)S(1)}, f32[128,4]{0,1:T(4,128)}, u32[]{:S(2)}) copy-start(f32[128,4]{0,1:T(4,128)} %param.25) | copy-start | bytes 6148
  138.2 0.6 copy-start.10
  156.4 12.1 %collective-permute-start.5 = (bf16[768,128]{1,0:T(8,128)(2,1)}, bf16[768,128]{1,0:T(8,128)(2,1)S(1)}, u32[]{:S(2)}, u32[]{:S(2)}) collective-permute-start(bf16[768,128]{1,0:T(8,128)(2,1)} %get-tuple-element.18), channel_id=1, source_target_pairs={{0,48},{16,0},{32,16},{48,32},{1,49},{17,1},{33,17},{49,33},{2,50}... | collective-permute-start | bytes 589832 | tf_op jit(solution)/shard_map/ppermute | solution.py:421
  161.4 0.7 copy-start.3
  165.3 7.8 %collective-permute-start.7 = (f32[128,128]{1,0:T(8,128)}, f32[128,128]{1,0:T(8,128)S(1)}, u32[]{:S(2)}, u32[]{:S(2)}) collective-permute-start(f32[128,128]{1,0:T(8,128)} %get-tuple-element.23), channel_id=1, source_target_pairs={{0,1},{1,0},{2,3},{3,2},{4,5},{5,4},{6,7},{7,6},{8,9},{9,8},{10,11... | collective-permute-start | bytes 196616 | tf_op jit(solution)/shard_map/ppermute | solution.py:470
  168.5 0.7 copy-start.4
  168.5 0.7 copy-start.5
  168.6 0.8 copy-start.6
Sparse Core Ops, SparseCore 0:
  28.1 49.4 all-gather.1

commit v3 on v2

--- a/solution.py
+++ b/solution.py
@@ -122,10 +122,14 @@
 DEPTH = 2 * HEAD + 16
 
 
-def attend_body(turns, ids, q0_ref, q1_ref, kvg_ref, out0_ref, out1_ref, ka_ref):
+def attend_body(turns, ids, q0_ref, q1_ref, *refs):
+    chunks, (out0_ref, out1_ref, ka_ref, v_ref) = refs[:NZ], refs[NZ:]
     z, x = ids[0], ids[1]
-    ka_ref[:, 0:HEAD, :] = kvg_ref[:, 0:HEAD, :]
-    ka_ref[:, HEAD:DEPTH, :] = kvg_ref[:, 0:KG, :]
+    for back, ref in enumerate(chunks):
+        place = lax.rem(z + NZ - back, NZ)
+        ka_ref[place, 0:HEAD, :] = ref[0:HEAD, :]
+        ka_ref[place, HEAD:DEPTH, :] = ref[0:KG, :]
+        v_ref[place] = ref[KG:KVG, :]
     tiles = []
     for ref in (q0_ref, q1_ref):
         scaled = ref[...].astype(F32).T * (0.125 * LOG2E)
@@ -140,7 +144,7 @@
         return new_peak, acc * jnp.exp2(peak - new_peak) + dot_t(w, values)
 
     def update(chunk, carry, some, masked):
-        k, values = ka_ref[chunk], kvg_ref[chunk, KG:KVG, :]
+        k, values = ka_ref[chunk], v_ref[chunk]
         scores = [dot(tile, k) for tile in some]
         if masked:
             for i in range(TILES):
@@ -210,9 +214,10 @@
     half = table_ref[:, 2:3]
     first = jnp.where(half == 0, pick, 0.0).astype(BF16)
     second = jnp.where(half == 1, pick, 0.0).astype(BF16)
-    send_ref[...] = (dot(first, normed[:, : D // 2]) + dot(second, normed[:, D // 2 :])).astype(
-        BF16
-    )
+    at = lax.rem(ids[3], 2) * (D // 2)
+    low = normed_ref[:, pl.ds(pl.multiple_of(at, D // 2), D // 4)]
+    high = normed_ref[:, pl.ds(pl.multiple_of(at + D // 4, D // 4), D // 4)]
+    send_ref[...] = (dot(first, low) + dot(second, high)).astype(BF16)
 
 
 def gated(g, u):
@@ -222,6 +227,7 @@
 def experts_body(
     ids,
     x_ref,
+    x_got_ref,
     gate_ref,
     up_ref,
     down_ref,
@@ -232,19 +238,33 @@
     sdown_ref,
     source_ref,
     out_ref,
+    low_ref,
+    high_ref,
 ):
     c = ids[2]
-    x = x_ref[...]
+    even = lax.rem(ids[3], 2) == 0
+
+    @pl.when(even)
+    def _():
+        low_ref[...] = x_ref[...]
+        high_ref[...] = x_got_ref[...]
+
+    @pl.when(jnp.logical_not(even))
+    def _():
+        low_ref[...] = x_got_ref[...]
+        high_ref[...] = x_ref[...]
+
     lane = lax.broadcasted_iota(jnp.int32, (SLOTS, 2 * SLOTS), 1)
-    x0 = dot(jnp.where(lane == source_ref[:, 0:1], 1.0, 0.0).astype(BF16), x).astype(BF16)
-    x1 = dot(jnp.where(lane == source_ref[:, 1:2], 1.0, 0.0).astype(BF16), x).astype(BF16)
+    x0 = jnp.where(lane == source_ref[:, 0:1], 1.0, 0.0).astype(BF16)
+    x1 = jnp.where(lane == source_ref[:, 1:2], 1.0, 0.0).astype(BF16)
+    low, high = low_ref[...], high_ref[...]
+    rows = jnp.concatenate([dot(x0, low), dot(x1, low), dot(x0, high), dot(x1, high)], axis=1)
+    rows = rows.astype(BF16)
     n = SLOTS // 2
     for l in range(LOCAL):
-        rows0, rows1 = x0[l * n : (l + 1) * n], x1[l * n : (l + 1) * n]
         wg = jnp.concatenate([gate_ref[l], got_ref[l * 64 : l * 64 + 64, :]], axis=0)
         wu = jnp.concatenate([up_ref[l], got_ref[128 + l * 64 : 128 + l * 64 + 64, :]], axis=0)
-        g = dot_t(rows0, wg[:, : D // 2]) + dot_t(rows1, wg[:, D // 2 :])
-        u = dot_t(rows0, wu[:, : D // 2]) + dot_t(rows1, wu[:, D // 2 :])
+        g, u = dot_t(rows[l * n : (l + 1) * n], wg), dot_t(rows[l * n : (l + 1) * n], wu)
         h = gated(g, u).astype(BF16)
         wd = jnp.concatenate([down_ref[l], got_ref[256 + l * 64 : 320 + l * 64, :]], axis=0)
         for y in range(NY):
@@ -334,22 +354,30 @@
         whole((KVG, ROWS)),
         (keys.T, values.T, cum_gate.reshape(1, ROWS)),
     )
-    kvg = lax.all_gather(packed, "z", axis=0, tiled=True).reshape(NZ, KVG, ROWS)
+    later = [(i, (i + 1) % NZ) for i in range(NZ)]
+    earlier = [(i, (i - 1) % NZ) for i in range(NZ)]
+    rising, falling = [packed], [packed]
+    for turn in range(1, 5):
+        rising.append(lax.ppermute(rising[-1], "z", later))
+        if turn < 4:
+            falling.append(lax.ppermute(falling[-1], "z", earlier))
+    kvg = rising + falling[:0:-1]
 
     normed, sent = call(
         dispatch_body,
         (
             jax.ShapeDtypeStruct((TOK, D), BF16),
-            jax.ShapeDtypeStruct((2 * SLOTS, D // 2), BF16),
+            jax.ShapeDtypeStruct((2 * SLOTS, D // 4), BF16),
         ),
         ids,
         (1,),
         [whole((TOK, D)), whole((1, D)), whole((4, TOK)), whole((2 * SLOTS, 8)), UNREAD],
-        (whole((TOK, D)), whole((2 * SLOTS, D // 2))),
+        (whole((TOK, D)), whole((2 * SLOTS, D // 4))),
         (moe_in, ffn_gain.reshape(1, D), routes.T, table, packed),
         flops=1_000_000_000,
     )
     arrived = lax.all_to_all(sent, ("z", "x"), 0, 0, tiled=True)
+    arrived_too = lax.ppermute(arrived, "y", [(i, i ^ 1) for i in range(NY)])
 
     other = pl.BlockSpec((LOCAL, 64, D), lambda i, s: (1 - s[2], 0, 0))
     trade = call(
@@ -376,7 +404,8 @@
         ids,
         (1,),
         [
-            whole((2 * SLOTS, D // 2)),
+            whole((2 * SLOTS, D // 4)),
+            whole((2 * SLOTS, D // 4)),
             mine,
             mine,
             mine,
@@ -390,6 +419,7 @@
         whole((NY, SLOTS + 64, 256)),
         (
             arrived,
+            arrived_too,
             expert_gate,
             expert_up,
             expert_down,
@@ -400,6 +430,7 @@
             shared_down,
             source,
         ),
+        scratch=[pltpu.VMEM((2 * SLOTS, D // 4), BF16)] * 2,
         flops=1_000_000_000,
     )
     products = lax.all_to_all(products, "y", 0, 0, tiled=True)
@@ -410,10 +441,10 @@
             (jax.ShapeDtypeStruct((ROWS, 128), BF16),) * 2,
             ids,
             (1,),
-            [whole((HEAD, ROWS))] * 2 + [whole((NZ, KVG, ROWS))],
+            [whole((HEAD, ROWS))] * 2 + [whole((KVG, ROWS))] * NZ,
             (whole((ROWS, 128)),) * 2,
-            (q_all[turns[0]], q_all[turns[1]], kvg),
-            scratch=[pltpu.VMEM((NZ, DEPTH, ROWS), BF16)],
+            (q_all[turns[0]], q_all[turns[1]], *kvg),
+            scratch=[pltpu.VMEM((NZ, DEPTH, ROWS), BF16), pltpu.VMEM((NZ, HEAD, ROWS), BF16)],
             flops=10_000_000_000,
         )
 

time: 182 us -> 189 us (1.038)
  the two profiles are of different devices: /device:TPU:449 before, /device:TPU:457 now
where the time goes in v3:
time: 189 us; the launch traced here: 188 us
  starting transfers between devices  78.8 us (42%)
  Pallas kernels  64.1 us (34%)
  waiting for transfers between devices  35.6 us (19%)
  local copies, waits for them, and re-layouts  6.52 us (3%)
  other arithmetic  2.06 us (1%)
    pallas_call x9, Pallas kernels, call(): pl.pallas_call(body, out_shape=out_shape, grid_spec=pltpu.PrefetchScalarG...  64.1 us
    ppermute x4, starting transfers between devices, on_device(): rising.append(lax.ppermute(rising[-1], 'z', later))  16.5 us
    ppermute x1, waiting for transfers between devices, on_device(): arrived_too = lax.ppermute(arrived, 'y', [(i, i ^ 1) for i in range(NY)])  16.2 us
    all_to_all x1, waiting for transfers between devices, on_device(): arrived = lax.all_to_all(sent, ('z', 'x'), 0, 0, tiled=True)  11.8 us
    ppermute x1, starting transfers between devices, on_device(): taken = lax.ppermute(give, 'c', swap)  11.4 us
    ppermute x3, starting transfers between devices, on_device(): lax.ppermute(mine, 'x', [((i + d) % NX, i) for i in range(NX)])  9.76 us
    ppermute x3, starting transfers between devices, on_device(): falling.append(lax.ppermute(falling[-1], 'z', earlier))  7.52 us
    ppermute x3, starting transfers between devices, send_part(): return lax.ppermute(part, 'x', [(i, (i + d) % NX) for i in range(NX)])  7.31 us
  transfers between devices with their start and end apart: 19, of which 8 were waited for; matrix products, arithmetic and copies ran while one was open for 1% of the time, Pallas kernels for 27%

profile of v3, /device:TPU:457, one launch (start us, length us, event | category | flops | bytes accessed | tf_op | source)
XLA Modules:
  0.0 188.0 jit_solution(3606461626314284839)
XLA Ops:
  0.6 0.6 pad_add_fusion.ids
  1.2 2.4 %shard_map.176.after_ref.refs_0_ = bf16[144,768]{1,0:T(8,128)(2,1)} custom-call(s32[4]{0:T(128)} %pad_add_fusion.ids, bf16[64,768]{1,0:T(8,128)(2,1)} %bitcast.21, bf16[64,768]{1,0:T(8,128)(2,1)} %bitcast.22, f32[1,768]{1,0:T(1,128)} %bitcast.24), custom_call_target="tpu_custom_call" | custom-call | bytes 4194304 | tf_op jit(solution)/shard_map/pallas_call | solution.py:73
  3.6 3.8 %shard_map.177 = (bf16[128,2048]{1,0:T(8,128)(2,1)}, bf16[768,512]{1,0:T(8,128)(2,1)}) custom-call(s32[4]{0:T(128)} %pad_add_fusion.ids, bf16[128,2048]{1,0:T(8,128)(2,1)} %x_ref.1, f32[1,2048]{1,0:T(1,128)} %bitcast.27, s32[4,128]{1,0:T(4,128)} %bitcast.25, s32[768,8]{1,0:T(8,128)} %constant.22.clone.table_ref, bf16[144,768]{1,0:T(8,128)(2,1)} %shard_map.176.after_ref.refs_0_), custom_call_target="tpu_custom_call" | custom-call | flops 1000000000 | bytes 4194304 | tf_op jit(solution)/shard_map/pallas_call | solution.py:73
  7.4 6.6 %all-to-all-start = ((bf16[32,24,512]{2,1,0:T(8,128)(2,1)}), bf16[32,24,512]{2,1,0:T(8,128)(2,1)S(1)}, u32[]{:S(2)}, u32[]{:S(2)}) async-start(bf16[32,24,512]{2,1,0:T(8,128)(2,1)} %bitcast.18), calls=%async_computation | async-start | bytes 1572864 | tf_op jit(solution)/shard_map/all_to_all | solution.py:379
  14.0 3.6 %shard_map.178 = bf16[480,2048]{1,0:T(8,128)(2,1)} custom-call(s32[4]{0:T(128)} %pad_add_fusion.ids, bf16[4,64,2048]{2,1,0:T(8,128)(2,1)} %gate_ref.3, bf16[4,64,2048]{2,1,0:T(8,128)(2,1)} %up_ref.3, bf16[4,64,2048]{2,1,0:T(8,128)(2,1)} %down_ref.3, bf16[32,2048]{1,0:T(8,128)(2,1)} %sgate_ref.3, bf16[32,2048]{1,0:T(8,128)(2,1)} %sup_ref.3, ...), custom_call_target="tpu_custom_call" | custom-call | flops 1000000000 | bytes 4194304 | tf_op jit(solution)/shard_map/pallas_call | solution.py:73
  17.6 3.1 %collective-permute-start.14 = (bf16[480,2048]{1,0:T(8,128)(2,1)}, bf16[480,2048]{1,0:T(8,128)(2,1)S(1)}, u32[]{:S(2)}, u32[]{:S(2)}) collective-permute-start(bf16[480,2048]{1,0:T(8,128)(2,1)} %shard_map.178), channel_id=1, source_target_pairs={{0,1},{1,0},{2,3},{3,2},{4,5},{5,4},{6,7},{7,6},{8,9},{9,8},{10,11... | collective-permute-start | bytes 5898248 | tf_op jit(solution)/shard_map/ppermute | solution.py:393
  20.8 11.8 %all-to-all-done = bf16[32,24,512]{2,1,0:T(8,128)(2,1)S(1)} async-done(((bf16[32,24,512]{2,1,0:T(8,128)(2,1)}), bf16[32,24,512]{2,1,0:T(8,128)(2,1)S(1)}, u32[]{:S(2)}, u32[]{:S(2)}) %all-to-all-start) | async-done | bytes 786464 | tf_op jit(solution)/shard_map/all_to_all | solution.py:379
  32.5 2.1 %collective-permute-start.13 = (bf16[768,512]{1,0:T(8,128)(2,1)S(1)}, bf16[768,512]{1,0:T(8,128)(2,1)S(1)}, u32[]{:S(2)}, u32[]{:S(2)}) collective-permute-start(bf16[768,512]{1,0:T(8,128)(2,1)S(1)} %bitcast.16), channel_id=1, source_target_pairs={{0,2},{2,0},{4,6},{6,4},{8,10},{10,8},{12,14},{14,12},{1,3},{3,1},... | collective-permute-start | bytes 2359304 | tf_op jit(solution)/shard_map/ppermute | solution.py:380
  34.6 0.0 collective-permute-done.14.got_ref
  34.6 16.2 %collective-permute-done.13.x_got_ref = bf16[768,512]{1,0:T(8,128)(2,1)S(1)} collective-permute-done((bf16[768,512]{1,0:T(8,128)(2,1)S(1)}, bf16[768,512]{1,0:T(8,128)(2,1)S(1)}, u32[]{:S(2)}, u32[]{:S(2)}) %collective-permute-start.13) | collective-permute-done | bytes 786464 | tf_op jit(solution)/shard_map/ppermute | solution.py:380
  50.9 0.9 copy-done.3
  51.8 7.9 %shard_map.182 = bf16[8,448,256]{2,1,0:T(8,128)(2,1)} custom-call(s32[4]{0:T(128)} %pad_add_fusion.ids, bf16[768,512]{1,0:T(8,128)(2,1)} %bitcast.17, bf16[768,512]{1,0:T(8,128)(2,1)} %copy-done.3, bf16[4,64,2048]{2,1,0:T(8,128)(2,1)} %gate_ref.3, bf16[4,64,2048]{2,1,0:T(8,128)(2,1)} %up_ref.3, bf16[4,64,2048]{2,1,0:T(8,128)(2,1)} %down_ref.3, ...), custom_call_target="tpu_custom_call" | custom-call | flops 1000000000 | bytes 4194304 | tf_op jit(solution)/shard_map/pallas_call | solution.py:73
  59.7 7.1 %all-to-all-start.1 = ((bf16[8,448,256]{2,1,0:T(8,128)(2,1)}), bf16[8,448,256]{2,1,0:T(8,128)(2,1)S(1)}, u32[]{:S(2)}, u32[]{:S(2)}) async-start(bf16[8,448,256]{2,1,0:T(8,128)(2,1)} %shard_map.182), calls=%async_computation.1 | async-start | bytes 3670016 | tf_op jit(solution)/shard_map/all_to_all | solution.py:436
  66.8 4.5 %collective-permute-start.1 = (bf16[144,768]{1,0:T(8,128)(2,1)S(1)}, bf16[144,768]{1,0:T(8,128)(2,1)S(1)}, u32[]{:S(2)}, u32[]{:S(2)}) collective-permute-start(bf16[144,768]{1,0:T(8,128)(2,1)S(1)} %copy-done.4), channel_id=1, source_target_pairs={{0,64},{64,128},{128,192},{192,256},{256,320},{320,384},{384,448},... | collective-permute-start | bytes 663560 | tf_op jit(solution)/shard_map/ppermute | solution.py:361
  71.4 3.4 %collective-permute-start.5 = (bf16[144,768]{1,0:T(8,128)(2,1)S(1)}, bf16[144,768]{1,0:T(8,128)(2,1)S(1)}, u32[]{:S(2)}, u32[]{:S(2)}) collective-permute-start(bf16[144,768]{1,0:T(8,128)(2,1)S(1)} %copy-done.4), channel_id=1, source_target_pairs={{0,448},{64,0},{128,64},{192,128},{256,192},{320,256},{384,320},{4... | collective-permute-start | bytes 663560 | tf_op jit(solution)/shard_map/ppermute | solution.py:363
  74.8 1.7 collective-permute-done.1.refs_1_
  76.5 2.8 %collective-permute-start.2 = (bf16[144,768]{1,0:T(8,128)(2,1)S(1)}, bf16[144,768]{1,0:T(8,128)(2,1)S(1)}, u32[]{:S(2)}, u32[]{:S(2)}) collective-permute-start(bf16[144,768]{1,0:T(8,128)(2,1)S(1)} %collective-permute-done.1.refs_1_), channel_id=1, source_target_pairs={{0,64},{64,128},{128,192},{192,256},{256,320},{320,384},{384,448},... | collective-permute-start | bytes 663560 | tf_op jit(solution)/shard_map/ppermute | solution.py:361
  79.3 0.3 collective-permute-done.5.refs_7_
  79.6 2.2 %collective-permute-start.6 = (bf16[144,768]{1,0:T(8,128)(2,1)S(1)}, bf16[144,768]{1,0:T(8,128)(2,1)S(1)}, u32[]{:S(2)}, u32[]{:S(2)}) collective-permute-start(bf16[144,768]{1,0:T(8,128)(2,1)S(1)} %collective-permute-done.5.refs_7_), channel_id=1, source_target_pairs={{0,448},{64,0},{128,64},{192,128},{256,192},{320,256},{384,320},{4... | collective-permute-start | bytes 663560 | tf_op jit(solution)/shard_map/ppermute | solution.py:363
  81.8 1.7 collective-permute-done.2.refs_2_
  83.4 4.0 %collective-permute-start.3 = (bf16[144,768]{1,0:T(8,128)(2,1)S(1)}, bf16[144,768]{1,0:T(8,128)(2,1)S(1)}, u32[]{:S(2)}, u32[]{:S(2)}) collective-permute-start(bf16[144,768]{1,0:T(8,128)(2,1)S(1)} %collective-permute-done.2.refs_2_), channel_id=1, source_target_pairs={{0,64},{64,128},{128,192},{192,256},{256,320},{320,384},{384,448},... | collective-permute-start | bytes 663560 | tf_op jit(solution)/shard_map/ppermute | solution.py:361
  87.4 0.3 collective-permute-done.6.refs_6_
  87.7 1.9 %collective-permute-start.7 = (bf16[144,768]{1,0:T(8,128)(2,1)S(1)}, bf16[144,768]{1,0:T(8,128)(2,1)S(1)}, u32[]{:S(2)}, u32[]{:S(2)}) collective-permute-start(bf16[144,768]{1,0:T(8,128)(2,1)S(1)} %collective-permute-done.6.refs_6_), channel_id=1, source_target_pairs={{0,448},{64,0},{128,64},{192,128},{256,192},{320,256},{384,320},{4... | collective-permute-start | bytes 663560 | tf_op jit(solution)/shard_map/ppermute | solution.py:363
  89.7 0.7 collective-permute-done.3.refs_3_
  90.4 5.2 %collective-permute-start.4 = (bf16[144,768]{1,0:T(8,128)(2,1)S(1)}, bf16[144,768]{1,0:T(8,128)(2,1)S(1)}, u32[]{:S(2)}, u32[]{:S(2)}) collective-permute-start(bf16[144,768]{1,0:T(8,128)(2,1)S(1)} %collective-permute-done.3.refs_3_), channel_id=1, source_target_pairs={{0,64},{64,128},{128,192},{192,256},{256,320},{320,384},{384,448},... | collective-permute-start | bytes 663560 | tf_op jit(solution)/shard_map/ppermute | solution.py:361
  95.6 5.4 %collective-permute-start.8 = (bf16[64,768]{1,0:T(8,128)(2,1)}, bf16[64,768]{1,0:T(8,128)(2,1)S(1)}, u32[]{:S(2)}, u32[]{:S(2)}) collective-permute-start(bf16[64,768]{1,0:T(8,128)(2,1)} %bitcast.5.q1_ref), channel_id=1, source_target_pairs={{16,0},{32,16},{48,32},{0,48},{17,1},{33,17},{49,33},{1,49},{18,2}... | collective-permute-start | bytes 294920 | tf_op jit(solution)/shard_map/ppermute | solution.py:397
  101.0 2.3 %collective-permute-start.9 = (bf16[64,768]{1,0:T(8,128)(2,1)}, bf16[64,768]{1,0:T(8,128)(2,1)S(1)}, u32[]{:S(2)}, u32[]{:S(2)}) collective-permute-start(bf16[64,768]{1,0:T(8,128)(2,1)} %bitcast.5.q1_ref), channel_id=1, source_target_pairs={{32,0},{48,16},{0,32},{16,48},{33,1},{49,17},{1,33},{17,49},{34,2}... | collective-permute-start | bytes 294920 | tf_op jit(solution)/shard_map/ppermute | solution.py:397
  103.2 2.1 %collective-permute-start = (bf16[64,768]{1,0:T(8,128)(2,1)}, bf16[64,768]{1,0:T(8,128)(2,1)}, u32[]{:S(2)}, u32[]{:S(2)}) collective-permute-start(bf16[64,768]{1,0:T(8,128)(2,1)} %bitcast.5.q1_ref), channel_id=1, source_target_pairs={{48,0},{0,16},{16,32},{32,48},{49,1},{1,17},{17,33},{33,49},{50,2}... | collective-permute-start | bytes 294920 | tf_op jit(solution)/shard_map/ppermute | solution.py:397
  105.4 0.0 collective-permute-done.8.q0_ref
  105.4 0.0 copy-start.18
  105.4 2.9 %collective-permute-done.9.q1_ref = bf16[64,768]{1,0:T(8,128)(2,1)S(1)} collective-permute-done((bf16[64,768]{1,0:T(8,128)(2,1)}, bf16[64,768]{1,0:T(8,128)(2,1)S(1)}, u32[]{:S(2)}, u32[]{:S(2)}) %collective-permute-start.9) | collective-permute-done | bytes 98336 | tf_op jit(solution)/shard_map/ppermute | solution.py:397
  108.3 0.0 collective-permute-done.7.refs_5_
  108.3 0.0 collective-permute-done.4.refs_4_
  108.4 0.6 copy-done.19
  109.0 0.1 copy-done.16
  109.1 0.7 copy-done.17
  109.8 18.2 %shard_map.180 = (bf16[768,128]{1,0:T(8,128)(2,1)}, bf16[768,128]{1,0:T(8,128)(2,1)}) custom-call(s32[4]{0:T(128)} %pad_add_fusion.ids, bf16[64,768]{1,0:T(8,128)(2,1)} %copy-done.18, bf16[64,768]{1,0:T(8,128)(2,1)} %copy-done.19, bf16[144,768]{1,0:T(8,128)(2,1)} %shard_map.176.after_ref.refs_0_, bf16[144,768]{1,0:T(8,128)(2,1)} %copy-done.11, ...), custom_call_target="tpu_custom_call" | custom-call | flops 10000000000 | bytes 4194304 | tf_op jit(solution)/shard_map/pallas_call | solution.py:73
  128.0 1.9 %collective-permute-start.10 = (bf16[768,128]{1,0:T(8,128)(2,1)}, bf16[768,128]{1,0:T(8,128)(2,1)S(1)}, u32[]{:S(2)}, u32[]{:S(2)}) collective-permute-start(bf16[768,128]{1,0:T(8,128)(2,1)} %get-tuple-element.16), channel_id=1, source_target_pairs={{0,16},{16,32},{32,48},{48,0},{1,17},{17,33},{33,49},{49,1},{2,18}... | collective-permute-start | bytes 589832 | tf_op jit(solution)/shard_map/ppermute | solution.py:452
  129.9 1.9 %collective-permute-start.11 = (bf16[768,128]{1,0:T(8,128)(2,1)}, bf16[768,128]{1,0:T(8,128)(2,1)S(1)}, u32[]{:S(2)}, u32[]{:S(2)}) collective-permute-start(bf16[768,128]{1,0:T(8,128)(2,1)} %get-tuple-element.17), channel_id=1, source_target_pairs={{0,32},{16,48},{32,0},{48,16},{1,33},{17,49},{33,1},{49,17},{2,34}... | collective-permute-start | bytes 589832 | tf_op jit(solution)/shard_map/ppermute | solution.py:452
  131.8 0.0 all-to-all-done.1.part_ref
  131.8 1.3 copy-done.2
  133.1 3.7 %shard_map.183 = (bf16[768,128]{1,0:T(8,128)(2,1)}, f32[64,256]{1,0:T(8,128)}) custom-call(s32[4]{0:T(128)} %pad_add_fusion.ids, bf16[8,448,256]{2,1,0:T(8,128)(2,1)} %copy-done.2, s32[768,8]{1,0:T(8,128)} %constant.22.clone.table_ref), custom_call_target="tpu_custom_call" | custom-call | flops 1000000000 | bytes 4194304 | tf_op jit(solution)/shard_map/pallas_call | solution.py:73
  136.8 7.3 %all-to-all-start.2 = ((bf16[32,24,128]{2,1,0:T(8,128)(2,1)}), bf16[32,24,128]{2,1,0:T(8,128)(2,1)S(1)}, u32[]{:S(2)}, u32[]{:S(2)}) async-start(bf16[32,24,128]{2,1,0:T(8,128)(2,1)} %bitcast.20), calls=%async_computation.2 | async-start | bytes 393216 | tf_op jit(solution)/shard_map/all_to_all | solution.py:473
  144.1 0.0 copy-start.9
  144.1 0.0 copy-start.10
  144.1 0.0 collective-permute-done.q0_ref
  144.1 17.5 %shard_map.179 = (bf16[768,128]{1,0:T(8,128)(2,1)}, bf16[768,128]{1,0:T(8,128)(2,1)}) custom-call(s32[4]{0:T(128)} %pad_add_fusion.ids, bf16[64,768]{1,0:T(8,128)(2,1)} %collective-permute-done.q0_ref, bf16[64,768]{1,0:T(8,128)(2,1)} %bitcast.5.q1_ref, bf16[144,768]{1,0:T(8,128)(2,1)} %shard_map.176.after_ref.refs_0_, bf16[144,768]{1,0:T(8,128)(2,1)} %copy-done.11, ...), custom_call_target="tpu_custom_call" | custom-call | flops 10000000000 | bytes 4194304 | tf_op jit(solution)/shard_map/pallas_call | solution.py:73
  161.7 3.5 %collective-permute-start.12 = (bf16[768,128]{1,0:T(8,128)(2,1)}, bf16[768,128]{1,0:T(8,128)(2,1)S(1)}, u32[]{:S(2)}, u32[]{:S(2)}) collective-permute-start(bf16[768,128]{1,0:T(8,128)(2,1)} %get-tuple-element.18), channel_id=1, source_target_pairs={{0,48},{16,0},{32,16},{48,32},{1,49},{17,1},{33,17},{49,33},{2,50}... | collective-permute-start | bytes 589832 | tf_op jit(solution)/shard_map/ppermute | solution.py:452
  165.2 0.0 copy-done.9
  165.2 0.7 copy.19.routes_ref
  165.9 0.7 copy.20.weight_ref
  166.7 0.0 all-to-all-done.2
  166.7 0.7 copy-done.5
  167.3 3.2 %shard_map.184 = (f32[128,128]{1,0:T(8,128)}, f32[128,128]{1,0:T(8,128)}) custom-call(s32[4]{0:T(128)} %pad_add_fusion.ids, bf16[768,128]{1,0:T(8,128)(2,1)} %bitcast.19, s32[128,4]{1,0:T(8,128)} %copy.19.routes_ref, f32[128,4]{1,0:T(8,128)} %copy.20.weight_ref, s32[8,768]{1,0:T(8,128)} %constant.28.table_ref, f32[64,256]{1,0:T(8,128)} %get-tuple-element.21.shared_ref), custom_call_target="tpu_custom_call" | custom-call | flops 1000000000 | bytes 4194304 | tf_op jit(solution)/shard_map/pallas_call | solution.py:73
  170.5 11.4 %collective-permute-start.15 = (f32[128,128]{1,0:T(8,128)}, f32[128,128]{1,0:T(8,128)S(1)}, u32[]{:S(2)}, u32[]{:S(2)}) collective-permute-start(f32[128,128]{1,0:T(8,128)} %get-tuple-element.23), channel_id=1, source_target_pairs={{0,1},{1,0},{2,3},{3,2},{4,5},{5,4},{6,7},{7,6},{8,9},{9,8},{10,11... | collective-permute-start | bytes 196616 | tf_op jit(solution)/shard_map/ppermute | solution.py:501
  181.9 0.0 collective-permute-done.10.refs_1_
  182.0 0.0 collective-permute-done.11.refs_2_
  182.0 0.0 collective-permute-done.12.refs_3_
  182.0 0.6 copy-done.6
  182.6 0.1 copy-done.7
  182.7 0.1 copy-done.8
  182.8 3.8 %shard_map.181 = bf16[64,768]{1,0:T(8,128)(2,1)} custom-call(s32[4]{0:T(128)} %pad_add_fusion.ids, f32[1,64]{1,0:T(1,128)} %bitcast.26, bf16[768,128]{1,0:T(8,128)(2,1)} %get-tuple-element.15.refs_0_, bf16[768,128]{1,0:T(8,128)(2,1)} %copy-done.6, bf16[768,128]{1,0:T(8,128)(2,1)} %copy-done.7, bf16[768,128]{1,0:T(8,128)(2,1)} %copy-done.8), custom_call_target="tpu_custom_call" | custom-call | bytes 4194304 | tf_op jit(solution)/shard_map/pallas_call | solution.py:73
  186.6 0.0 collective-permute-done.15
  186.6 1.5 add_convert_fusion
  (27 shorter events, 0.1 us)
Async XLA Ops:
  7.4 25.2 %all-to-all-start = ((bf16[32,24,512]{2,1,0:T(8,128)(2,1)}), bf16[32,24,512]{2,1,0:T(8,128)(2,1)S(1)}, u32[]{:S(2)}, u32[]{:S(2)}) async-start(bf16[32,24,512]{2,1,0:T(8,128)(2,1)} %bitcast.18), calls=%async_computation | async-start | bytes 1572864 | tf_op jit(solution)/shard_map/all_to_all | solution.py:379
  17.6 17.0 %collective-permute-start.14 = (bf16[480,2048]{1,0:T(8,128)(2,1)}, bf16[480,2048]{1,0:T(8,128)(2,1)S(1)}, u32[]{:S(2)}, u32[]{:S(2)}) collective-permute-start(bf16[480,2048]{1,0:T(8,128)(2,1)} %shard_map.178), channel_id=1, source_target_pairs={{0,1},{1,0},{2,3},{3,2},{4,5},{5,4},{6,7},{7,6},{8,9},{9,8},{10,11... | collective-permute-start | bytes 5898248 | tf_op jit(solution)/shard_map/ppermute | solution.py:393
  32.5 18.3 %copy-start = (bf16[32,24,512]{2,1,0:T(8,128)(2,1)}, bf16[32,24,512]{2,1,0:T(8,128)(2,1)S(1)}, u32[]{:S(2)}) copy-start(bf16[32,24,512]{2,1,0:T(8,128)(2,1)S(1)} %all-to-all-done) | copy-start | bytes 2359300
  32.5 18.3 %collective-permute-start.13 = (bf16[768,512]{1,0:T(8,128)(2,1)S(1)}, bf16[768,512]{1,0:T(8,128)(2,1)S(1)}, u32[]{:S(2)}, u32[]{:S(2)}) collective-permute-start(bf16[768,512]{1,0:T(8,128)(2,1)S(1)} %bitcast.16), channel_id=1, source_target_pairs={{0,2},{2,0},{4,6},{6,4},{8,10},{10,8},{12,14},{14,12},{1,3},{3,1},... | collective-permute-start | bytes 2359304 | tf_op jit(solution)/shard_map/ppermute | solution.py:380
  34.6 16.3 %copy-start.1 = (bf16[480,2048]{1,0:T(8,128)(2,1)}, bf16[480,2048]{1,0:T(8,128)(2,1)S(1)}, u32[]{:S(2)}) copy-start(bf16[480,2048]{1,0:T(8,128)(2,1)S(1)} %collective-permute-done.14.got_ref) | copy-start | bytes 5898244
  50.9 0.9 copy-start.3
  59.7 7.1 %copy-start.4 = (bf16[144,768]{1,0:T(8,128)(2,1)S(1)}, bf16[144,768]{1,0:T(8,128)(2,1)}, u32[]{:S(2)}) copy-start(bf16[144,768]{1,0:T(8,128)(2,1)} %shard_map.176.after_ref.refs_0_) | copy-start | bytes 663556
  59.7 72.1 %all-to-all-start.1 = ((bf16[8,448,256]{2,1,0:T(8,128)(2,1)}), bf16[8,448,256]{2,1,0:T(8,128)(2,1)S(1)}, u32[]{:S(2)}, u32[]{:S(2)}) async-start(bf16[8,448,256]{2,1,0:T(8,128)(2,1)} %shard_map.182), calls=%async_computation.1 | async-start | bytes 3670016 | tf_op jit(solution)/shard_map/all_to_all | solution.py:436
  66.8 9.6 %collective-permute-start.1 = (bf16[144,768]{1,0:T(8,128)(2,1)S(1)}, bf16[144,768]{1,0:T(8,128)(2,1)S(1)}, u32[]{:S(2)}, u32[]{:S(2)}) collective-permute-start(bf16[144,768]{1,0:T(8,128)(2,1)S(1)} %copy-done.4), channel_id=1, source_target_pairs={{0,64},{64,128},{128,192},{192,256},{256,320},{320,384},{384,448},... | collective-permute-start | bytes 663560 | tf_op jit(solution)/shard_map/ppermute | solution.py:361
  71.4 8.2 %collective-permute-start.5 = (bf16[144,768]{1,0:T(8,128)(2,1)S(1)}, bf16[144,768]{1,0:T(8,128)(2,1)S(1)}, u32[]{:S(2)}, u32[]{:S(2)}) collective-permute-start(bf16[144,768]{1,0:T(8,128)(2,1)S(1)} %copy-done.4), channel_id=1, source_target_pairs={{0,448},{64,0},{128,64},{192,128},{256,192},{320,256},{384,320},{4... | collective-permute-start | bytes 663560 | tf_op jit(solution)/shard_map/ppermute | solution.py:363
  76.5 31.9 %copy-start.11 = (bf16[144,768]{1,0:T(8,128)(2,1)}, bf16[144,768]{1,0:T(8,128)(2,1)S(1)}, u32[]{:S(2)}) copy-start(bf16[144,768]{1,0:T(8,128)(2,1)S(1)} %collective-permute-done.1.refs_1_) | copy-start | bytes 663556
  76.5 7.0 %collective-permute-start.2 = (bf16[144,768]{1,0:T(8,128)(2,1)S(1)}, bf16[144,768]{1,0:T(8,128)(2,1)S(1)}, u32[]{:S(2)}, u32[]{:S(2)}) collective-permute-start(bf16[144,768]{1,0:T(8,128)(2,1)S(1)} %collective-permute-done.1.refs_1_), channel_id=1, source_target_pairs={{0,64},{64,128},{128,192},{192,256},{256,320},{320,384},{384,448},... | collective-permute-start | bytes 663560 | tf_op jit(solution)/shard_map/ppermute | solution.py:361
  79.6 28.8 %copy-start.12 = (bf16[144,768]{1,0:T(8,128)(2,1)}, bf16[144,768]{1,0:T(8,128)(2,1)S(1)}, u32[]{:S(2)}) copy-start(bf16[144,768]{1,0:T(8,128)(2,1)S(1)} %collective-permute-done.5.refs_7_) | copy-start | bytes 663556
  79.6 8.2 %collective-permute-start.6 = (bf16[144,768]{1,0:T(8,128)(2,1)S(1)}, bf16[144,768]{1,0:T(8,128)(2,1)S(1)}, u32[]{:S(2)}, u32[]{:S(2)}) collective-permute-start(bf16[144,768]{1,0:T(8,128)(2,1)S(1)} %collective-permute-done.5.refs_7_), channel_id=1, source_target_pairs={{0,448},{64,0},{128,64},{192,128},{256,192},{320,256},{384,320},{4... | collective-permute-start | bytes 663560 | tf_op jit(solution)/shard_map/ppermute | solution.py:363
  83.4 24.9 %copy-start.13 = (bf16[144,768]{1,0:T(8,128)(2,1)}, bf16[144,768]{1,0:T(8,128)(2,1)S(1)}, u32[]{:S(2)}) copy-start(bf16[144,768]{1,0:T(8,128)(2,1)S(1)} %collective-permute-done.2.refs_2_) | copy-start | bytes 663556
  83.4 7.0 %collective-permute-start.3 = (bf16[144,768]{1,0:T(8,128)(2,1)S(1)}, bf16[144,768]{1,0:T(8,128)(2,1)S(1)}, u32[]{:S(2)}, u32[]{:S(2)}) collective-permute-start(bf16[144,768]{1,0:T(8,128)(2,1)S(1)} %collective-permute-done.2.refs_2_), channel_id=1, source_target_pairs={{0,64},{64,128},{128,192},{192,256},{256,320},{320,384},{384,448},... | collective-permute-start | bytes 663560 | tf_op jit(solution)/shard_map/ppermute | solution.py:361
  87.7 20.6 %copy-start.14 = (bf16[144,768]{1,0:T(8,128)(2,1)}, bf16[144,768]{1,0:T(8,128)(2,1)S(1)}, u32[]{:S(2)}) copy-start(bf16[144,768]{1,0:T(8,128)(2,1)S(1)} %collective-permute-done.6.refs_6_) | copy-start | bytes 663556
  87.7 20.6 %collective-permute-start.7 = (bf16[144,768]{1,0:T(8,128)(2,1)S(1)}, bf16[144,768]{1,0:T(8,128)(2,1)S(1)}, u32[]{:S(2)}, u32[]{:S(2)}) collective-permute-start(bf16[144,768]{1,0:T(8,128)(2,1)S(1)} %collective-permute-done.6.refs_6_), channel_id=1, source_target_pairs={{0,448},{64,0},{128,64},{192,128},{256,192},{320,256},{384,320},{4... | collective-permute-start | bytes 663560 | tf_op jit(solution)/shard_map/ppermute | solution.py:363
  90.4 18.0 %copy-start.15 = (bf16[144,768]{1,0:T(8,128)(2,1)}, bf16[144,768]{1,0:T(8,128)(2,1)S(1)}, u32[]{:S(2)}) copy-start(bf16[144,768]{1,0:T(8,128)(2,1)S(1)} %collective-permute-done.3.refs_3_) | copy-start | bytes 663556
  90.4 18.0 %collective-permute-start.4 = (bf16[144,768]{1,0:T(8,128)(2,1)S(1)}, bf16[144,768]{1,0:T(8,128)(2,1)S(1)}, u32[]{:S(2)}, u32[]{:S(2)}) collective-permute-start(bf16[144,768]{1,0:T(8,128)(2,1)S(1)} %collective-permute-done.3.refs_3_), channel_id=1, source_target_pairs={{0,64},{64,128},{128,192},{192,256},{256,320},{320,384},{384,448},... | collective-permute-start | bytes 663560 | tf_op jit(solution)/shard_map/ppermute | solution.py:361
  95.6 9.8 %collective-permute-start.8 = (bf16[64,768]{1,0:T(8,128)(2,1)}, bf16[64,768]{1,0:T(8,128)(2,1)S(1)}, u32[]{:S(2)}, u32[]{:S(2)}) collective-permute-start(bf16[64,768]{1,0:T(8,128)(2,1)} %bitcast.5.q1_ref), channel_id=1, source_target_pairs={{16,0},{32,16},{48,32},{0,48},{17,1},{33,17},{49,33},{1,49},{18,2}... | collective-permute-start | bytes 294920 | tf_op jit(solution)/shard_map/ppermute | solution.py:397
  101.0 7.4 %collective-permute-start.9 = (bf16[64,768]{1,0:T(8,128)(2,1)}, bf16[64,768]{1,0:T(8,128)(2,1)S(1)}, u32[]{:S(2)}, u32[]{:S(2)}) collective-permute-start(bf16[64,768]{1,0:T(8,128)(2,1)} %bitcast.5.q1_ref), channel_id=1, source_target_pairs={{32,0},{48,16},{0,32},{16,48},{33,1},{49,17},{1,33},{17,49},{34,2}... | collective-permute-start | bytes 294920 | tf_op jit(solution)/shard_map/ppermute | solution.py:397
  103.2 40.9 %collective-permute-start = (bf16[64,768]{1,0:T(8,128)(2,1)}, bf16[64,768]{1,0:T(8,128)(2,1)}, u32[]{:S(2)}, u32[]{:S(2)}) collective-permute-start(bf16[64,768]{1,0:T(8,128)(2,1)} %bitcast.5.q1_ref), channel_id=1, source_target_pairs={{48,0},{0,16},{16,32},{32,48},{49,1},{1,17},{17,33},{33,49},{50,2}... | collective-permute-start | bytes 294920 | tf_op jit(solution)/shard_map/ppermute | solution.py:397
  105.4 3.0 %copy-start.18 = (bf16[64,768]{1,0:T(8,128)(2,1)}, bf16[64,768]{1,0:T(8,128)(2,1)S(1)}, u32[]{:S(2)}) copy-start(bf16[64,768]{1,0:T(8,128)(2,1)S(1)} %collective-permute-done.8.q0_ref) | copy-start | bytes 294916
  108.3 0.6 copy-start.19
  108.3 0.7 copy-start.16
  109.1 0.7 copy-start.17
  128.0 54.0 %collective-permute-start.10 = (bf16[768,128]{1,0:T(8,128)(2,1)}, bf16[768,128]{1,0:T(8,128)(2,1)S(1)}, u32[]{:S(2)}, u32[]{:S(2)}) collective-permute-start(bf16[768,128]{1,0:T(8,128)(2,1)} %get-tuple-element.16), channel_id=1, source_target_pairs={{0,16},{16,32},{32,48},{48,0},{1,17},{17,33},{33,49},{49,1},{2,18}... | collective-permute-start | bytes 589832 | tf_op jit(solution)/shard_map/ppermute | solution.py:452
  129.9 52.1 %collective-permute-start.11 = (bf16[768,128]{1,0:T(8,128)(2,1)}, bf16[768,128]{1,0:T(8,128)(2,1)S(1)}, u32[]{:S(2)}, u32[]{:S(2)}) collective-permute-start(bf16[768,128]{1,0:T(8,128)(2,1)} %get-tuple-element.17), channel_id=1, source_target_pairs={{0,32},{16,48},{32,0},{48,16},{1,33},{17,49},{33,1},{49,17},{2,34}... | collective-permute-start | bytes 589832 | tf_op jit(solution)/shard_map/ppermute | solution.py:452
  131.8 1.3 copy-start.2
  136.8 29.9 %all-to-all-start.2 = ((bf16[32,24,128]{2,1,0:T(8,128)(2,1)}), bf16[32,24,128]{2,1,0:T(8,128)(2,1)S(1)}, u32[]{:S(2)}, u32[]{:S(2)}) async-start(bf16[32,24,128]{2,1,0:T(8,128)(2,1)} %bitcast.20), calls=%async_computation.2 | async-start | bytes 393216 | tf_op jit(solution)/shard_map/all_to_all | solution.py:473
  144.1 21.1 %copy-start.9 = (s32[128,4]{0,1:T(4,128)S(1)}, s32[128,4]{0,1:T(4,128)}, u32[]{:S(2)}) copy-start(s32[128,4]{0,1:T(4,128)} %param.24) | copy-start | bytes 6148
  144.1 21.8 %copy-start.10 = (f32[128,4]{0,1:T(4,128)S(1)}, f32[128,4]{0,1:T(4,128)}, u32[]{:S(2)}) copy-start(f32[128,4]{0,1:T(4,128)} %param.25) | copy-start | bytes 6148
  161.7 20.3 %collective-permute-start.12 = (bf16[768,128]{1,0:T(8,128)(2,1)}, bf16[768,128]{1,0:T(8,128)(2,1)S(1)}, u32[]{:S(2)}, u32[]{:S(2)}) collective-permute-start(bf16[768,128]{1,0:T(8,128)(2,1)} %get-tuple-element.18), channel_id=1, source_target_pairs={{0,48},{16,0},{32,16},{48,32},{1,49},{17,1},{33,17},{49,33},{2,50}... | collective-permute-start | bytes 589832 | tf_op jit(solution)/shard_map/ppermute | solution.py:452
  166.7 0.7 copy-start.5
  170.5 16.0 %collective-permute-start.15 = (f32[128,128]{1,0:T(8,128)}, f32[128,128]{1,0:T(8,128)S(1)}, u32[]{:S(2)}, u32[]{:S(2)}) collective-permute-start(f32[128,128]{1,0:T(8,128)} %get-tuple-element.23), channel_id=1, source_target_pairs={{0,1},{1,0},{2,3},{3,2},{4,5},{5,4},{6,7},{7,6},{8,9},{9,8},{10,11... | collective-permute-start | bytes 196616 | tf_op jit(solution)/shard_map/ppermute | solution.py:501
  182.0 0.7 copy-start.6
  182.0 0.7 copy-start.7
  182.0 0.8 copy-start.8

commit v4 on v3

--- a/solution.py
+++ b/solution.py
@@ -95,7 +95,7 @@
 UNREAD = pl.BlockSpec(memory_space=pl.ANY)
 
 
-def pack_body(ids, k_ref, v_ref, g_ref, out_ref):
+def pack_body(ids, k_ref, v_ref, g_ref, after_ref, out_ref):
     out_ref[0:HEAD, :] = k_ref[...]
     out_ref[KG:KVG, :] = v_ref[...]
     hi, mid, lo = three_pieces(g_ref[...] * (-LOG2E))
@@ -196,7 +196,7 @@
     out_ref[...] = out.T.astype(BF16)
 
 
-def dispatch_body(ids, x_ref, gain_ref, routes_ref, table_ref, after_ref, normed_ref, send_ref):
+def dispatch_body(ids, x_ref, gain_ref, routes_ref, table_ref, normed_ref, send_ref):
     c = ids[2]
     x = x_ref[...].astype(F32)
     mean_square = jnp.mean(x * x, axis=1, keepdims=True)
@@ -345,14 +345,30 @@
     source = jnp.asarray(source_table())
     swap = [(0, 1), (1, 0)]
 
+    normed, sent = call(
+        dispatch_body,
+        (
+            jax.ShapeDtypeStruct((TOK, D), BF16),
+            jax.ShapeDtypeStruct((2 * SLOTS, D // 4), BF16),
+        ),
+        ids,
+        (1,),
+        [whole((TOK, D)), whole((1, D)), whole((4, TOK)), whole((2 * SLOTS, 8))],
+        (whole((TOK, D)), whole((2 * SLOTS, D // 4))),
+        (moe_in, ffn_gain.reshape(1, D), routes.T, table),
+        flops=1_000_000_000,
+    )
+    arrived = lax.all_to_all(sent, ("z", "x"), 0, 0, tiled=True)
+    arrived_too = lax.ppermute(arrived, "y", [(i, i ^ 1) for i in range(NY)])
+
     packed = call(
         pack_body,
         jax.ShapeDtypeStruct((KVG, ROWS), BF16),
         ids,
         (1,),
-        [whole((HEAD, ROWS)), whole((HEAD, ROWS)), whole((1, ROWS))],
+        [whole((HEAD, ROWS)), whole((HEAD, ROWS)), whole((1, ROWS)), UNREAD],
         whole((KVG, ROWS)),
-        (keys.T, values.T, cum_gate.reshape(1, ROWS)),
+        (keys.T, values.T, cum_gate.reshape(1, ROWS), sent),
     )
     later = [(i, (i + 1) % NZ) for i in range(NZ)]
     earlier = [(i, (i - 1) % NZ) for i in range(NZ)]
@@ -363,22 +379,6 @@
             falling.append(lax.ppermute(falling[-1], "z", earlier))
     kvg = rising + falling[:0:-1]
 
-    normed, sent = call(
-        dispatch_body,
-        (
-            jax.ShapeDtypeStruct((TOK, D), BF16),
-            jax.ShapeDtypeStruct((2 * SLOTS, D // 4), BF16),
-        ),
-        ids,
-        (1,),
-        [whole((TOK, D)), whole((1, D)), whole((4, TOK)), whole((2 * SLOTS, 8)), UNREAD],
-        (whole((TOK, D)), whole((2 * SLOTS, D // 4))),
-        (moe_in, ffn_gain.reshape(1, D), routes.T, table, packed),
-        flops=1_000_000_000,
-    )
-    arrived = lax.all_to_all(sent, ("z", "x"), 0, 0, tiled=True)
-    arrived_too = lax.ppermute(arrived, "y", [(i, i ^ 1) for i in range(NY)])
-
     other = pl.BlockSpec((LOCAL, 64, D), lambda i, s: (1 - s[2], 0, 0))
     trade = call(
         trade_body,
@@ -393,9 +393,9 @@
     got = lax.ppermute(trade, "c", swap)
 
     mine, _ = lax.optimization_barrier((queries.T, trade))
-    q_all = [mine] + [
-        lax.ppermute(mine, "x", [((i + d) % NX, i) for i in range(NX)]) for d in range(1, NX)
-    ]
+    q_all = [mine]
+    for d in range(1, NX):
+        q_all.append(lax.ppermute(mine, "x", [((i + d) % NX, i) for i in range(NX)]))
 
     mine = pl.BlockSpec((LOCAL, 64, D), lambda i, s: (s[2], 0, 0))
     products = call(

time: 189 us -> 189 us (level)
  the two profiles are of different devices: /device:TPU:457 before, /device:TPU:473 now
where the time goes in v4:
time: 189 us; the launch traced here: 188 us
  starting transfers between devices  79.1 us (42%)
  Pallas kernels  64 us (34%)
  waiting for transfers between devices  35.2 us (19%)
  local copies, waits for them, and re-layouts  6.45 us (3%)
  other arithmetic  2.06 us (1%)
    pallas_call x9, Pallas kernels, call(): pl.pallas_call(body, out_shape=out_shape, grid_spec=pltpu.PrefetchScalarG...  64 us
    ppermute x4, starting transfers between devices, on_device(): rising.append(lax.ppermute(rising[-1], 'z', later))  17.2 us
    ppermute x1, waiting for transfers between devices, on_device(): arrived_too = lax.ppermute(arrived, 'y', [(i, i ^ 1) for i in range(NY)])  16.2 us
    all_to_all x1, waiting for transfers between devices, on_device(): arrived = lax.all_to_all(sent, ('z', 'x'), 0, 0, tiled=True)  11.8 us
    ppermute x1, starting transfers between devices, on_device(): taken = lax.ppermute(give, 'c', swap)  11.7 us
    ppermute x3, starting transfers between devices, on_device(): lax.ppermute(mine, 'x', [((i + d) % NX, i) for i in range(NX)])  9.48 us
    ppermute x3, starting transfers between devices, on_device(): falling.append(lax.ppermute(falling[-1], 'z', earlier))  7.51 us
    ppermute x3, starting transfers between devices, send_part(): return lax.ppermute(part, 'x', [(i, (i + d) % NX) for i in range(NX)])  7.33 us
  transfers between devices with their start and end apart: 19, of which 6 were waited for; matrix products, arithmetic and copies ran while one was open for 1% of the time, Pallas kernels for 28%

profile of v4, /device:TPU:473, one launch (start us, length us, event | category | flops | bytes accessed | tf_op | source)
XLA Modules:
  0.0 187.8 jit_solution(11434679258586897349)
XLA Ops:
  0.6 0.6 pad_add_fusion.ids
  1.2 3.8 %shard_map.176 = (bf16[128,2048]{1,0:T(8,128)(2,1)}, bf16[768,512]{1,0:T(8,128)(2,1)}) custom-call(s32[4]{0:T(128)} %pad_add_fusion.ids, bf16[128,2048]{1,0:T(8,128)(2,1)} %x_ref.1, f32[1,2048]{1,0:T(1,128)} %bitcast.27, s32[4,128]{1,0:T(4,128)} %bitcast.25, s32[768,8]{1,0:T(8,128)} %constant.22.clone.table_ref), custom_call_target="tpu_custom_call" | custom-call | flops 1000000000 | bytes 4194304 | tf_op jit(solution)/shard_map/pallas_call | solution.py:73
  5.0 6.6 %all-to-all-start = ((bf16[32,24,512]{2,1,0:T(8,128)(2,1)}), bf16[32,24,512]{2,1,0:T(8,128)(2,1)S(1)}, u32[]{:S(2)}, u32[]{:S(2)}) async-start(bf16[32,24,512]{2,1,0:T(8,128)(2,1)} %bitcast.16), calls=%async_computation | async-start | bytes 1572864 | tf_op jit(solution)/shard_map/all_to_all | solution.py:361
  11.7 3.6 %shard_map.177 = bf16[480,2048]{1,0:T(8,128)(2,1)} custom-call(s32[4]{0:T(128)} %pad_add_fusion.ids, bf16[4,64,2048]{2,1,0:T(8,128)(2,1)} %gate_ref.3, bf16[4,64,2048]{2,1,0:T(8,128)(2,1)} %up_ref.3, bf16[4,64,2048]{2,1,0:T(8,128)(2,1)} %down_ref.3, bf16[32,2048]{1,0:T(8,128)(2,1)} %sgate_ref.3, bf16[32,2048]{1,0:T(8,128)(2,1)} %sup_ref.3, ...), custom_call_target="tpu_custom_call" | custom-call | flops 1000000000 | bytes 4194304 | tf_op jit(solution)/shard_map/pallas_call | solution.py:73
  15.3 3.1 %collective-permute-start.14 = (bf16[480,2048]{1,0:T(8,128)(2,1)}, bf16[480,2048]{1,0:T(8,128)(2,1)S(1)}, u32[]{:S(2)}, u32[]{:S(2)}) collective-permute-start(bf16[480,2048]{1,0:T(8,128)(2,1)} %shard_map.177), channel_id=1, source_target_pairs={{0,1},{1,0},{2,3},{3,2},{4,5},{5,4},{6,7},{7,6},{8,9},{9,8},{10,11... | collective-permute-start | bytes 5898248 | tf_op jit(solution)/shard_map/ppermute | solution.py:393
  18.4 11.8 %all-to-all-done = bf16[32,24,512]{2,1,0:T(8,128)(2,1)S(1)} async-done(((bf16[32,24,512]{2,1,0:T(8,128)(2,1)}), bf16[32,24,512]{2,1,0:T(8,128)(2,1)S(1)}, u32[]{:S(2)}, u32[]{:S(2)}) %all-to-all-start) | async-done | bytes 786464 | tf_op jit(solution)/shard_map/all_to_all | solution.py:361
  30.2 2.1 %collective-permute-start.13 = (bf16[768,512]{1,0:T(8,128)(2,1)S(1)}, bf16[768,512]{1,0:T(8,128)(2,1)S(1)}, u32[]{:S(2)}, u32[]{:S(2)}) collective-permute-start(bf16[768,512]{1,0:T(8,128)(2,1)S(1)} %bitcast.17), channel_id=1, source_target_pairs={{0,2},{2,0},{4,6},{6,4},{8,10},{10,8},{12,14},{14,12},{1,3},{3,1},... | collective-permute-start | bytes 2359304 | tf_op jit(solution)/shard_map/ppermute | solution.py:362
  32.3 0.0 collective-permute-done.14.got_ref
  32.3 16.2 %collective-permute-done.13.x_got_ref = bf16[768,512]{1,0:T(8,128)(2,1)S(1)} collective-permute-done((bf16[768,512]{1,0:T(8,128)(2,1)S(1)}, bf16[768,512]{1,0:T(8,128)(2,1)S(1)}, u32[]{:S(2)}, u32[]{:S(2)}) %collective-permute-start.13) | collective-permute-done | bytes 786464 | tf_op jit(solution)/shard_map/ppermute | solution.py:362
  48.5 0.9 copy-done.3
  49.4 7.9 %shard_map.182 = bf16[8,448,256]{2,1,0:T(8,128)(2,1)} custom-call(s32[4]{0:T(128)} %pad_add_fusion.ids, bf16[768,512]{1,0:T(8,128)(2,1)} %bitcast.18, bf16[768,512]{1,0:T(8,128)(2,1)} %copy-done.3, bf16[4,64,2048]{2,1,0:T(8,128)(2,1)} %gate_ref.3, bf16[4,64,2048]{2,1,0:T(8,128)(2,1)} %up_ref.3, bf16[4,64,2048]{2,1,0:T(8,128)(2,1)} %down_ref.3, ...), custom_call_target="tpu_custom_call" | custom-call | flops 1000000000 | bytes 4194304 | tf_op jit(solution)/shard_map/pallas_call | solution.py:73
  57.4 6.8 %all-to-all-start.1 = ((bf16[8,448,256]{2,1,0:T(8,128)(2,1)}), bf16[8,448,256]{2,1,0:T(8,128)(2,1)S(1)}, u32[]{:S(2)}, u32[]{:S(2)}) async-start(bf16[8,448,256]{2,1,0:T(8,128)(2,1)} %shard_map.182), calls=%async_computation.1 | async-start | bytes 3670016 | tf_op jit(solution)/shard_map/all_to_all | solution.py:436
  64.1 2.3 %shard_map.178.refs_0_ = bf16[144,768]{1,0:T(8,128)(2,1)} custom-call(s32[4]{0:T(128)} %pad_add_fusion.ids, bf16[64,768]{1,0:T(8,128)(2,1)} %bitcast.21, bf16[64,768]{1,0:T(8,128)(2,1)} %bitcast.22, f32[1,768]{1,0:T(1,128)} %bitcast.24, bf16[768,512]{1,0:T(8,128)(2,1)} %get-tuple-element.13.after_ref), custom_call_target="tpu_custom_call" | custom-call | bytes 4194304 | tf_op jit(solution)/shard_map/pallas_call | solution.py:73
  66.4 4.5 %collective-permute-start.1 = (bf16[144,768]{1,0:T(8,128)(2,1)}, bf16[144,768]{1,0:T(8,128)(2,1)S(1)}, u32[]{:S(2)}, u32[]{:S(2)}) collective-permute-start(bf16[144,768]{1,0:T(8,128)(2,1)} %shard_map.178.refs_0_), channel_id=1, source_target_pairs={{0,64},{64,128},{128,192},{192,256},{256,320},{320,384},{384,448},... | collective-permute-start | bytes 663560 | tf_op jit(solution)/shard_map/ppermute | solution.py:377
  71.0 3.4 %collective-permute-start.5 = (bf16[144,768]{1,0:T(8,128)(2,1)}, bf16[144,768]{1,0:T(8,128)(2,1)S(1)}, u32[]{:S(2)}, u32[]{:S(2)}) collective-permute-start(bf16[144,768]{1,0:T(8,128)(2,1)} %shard_map.178.refs_0_), channel_id=1, source_target_pairs={{0,448},{64,0},{128,64},{192,128},{256,192},{320,256},{384,320},{4... | collective-permute-start | bytes 663560 | tf_op jit(solution)/shard_map/ppermute | solution.py:379
  74.4 1.9 %collective-permute-done.1.refs_1_ = bf16[144,768]{1,0:T(8,128)(2,1)S(1)} collective-permute-done((bf16[144,768]{1,0:T(8,128)(2,1)}, bf16[144,768]{1,0:T(8,128)(2,1)S(1)}, u32[]{:S(2)}, u32[]{:S(2)}) %collective-permute-start.1) | collective-permute-done | bytes 221216 | tf_op jit(solution)/shard_map/ppermute | solution.py:377
  76.3 3.1 %collective-permute-start.2 = (bf16[144,768]{1,0:T(8,128)(2,1)S(1)}, bf16[144,768]{1,0:T(8,128)(2,1)S(1)}, u32[]{:S(2)}, u32[]{:S(2)}) collective-permute-start(bf16[144,768]{1,0:T(8,128)(2,1)S(1)} %collective-permute-done.1.refs_1_), channel_id=1, source_target_pairs={{0,64},{64,128},{128,192},{192,256},{256,320},{320,384},{384,448},... | collective-permute-start | bytes 663560 | tf_op jit(solution)/shard_map/ppermute | solution.py:377
  79.4 0.0 collective-permute-done.5.refs_7_
  79.4 2.2 %collective-permute-start.6 = (bf16[144,768]{1,0:T(8,128)(2,1)S(1)}, bf16[144,768]{1,0:T(8,128)(2,1)S(1)}, u32[]{:S(2)}, u32[]{:S(2)}) collective-permute-start(bf16[144,768]{1,0:T(8,128)(2,1)S(1)} %collective-permute-done.5.refs_7_), channel_id=1, source_target_pairs={{0,448},{64,0},{128,64},{192,128},{256,192},{320,256},{384,320},{4... | collective-permute-start | bytes 663560 | tf_op jit(solution)/shard_map/ppermute | solution.py:379
  81.6 1.7 collective-permute-done.2.refs_2_
  83.2 4.3 %collective-permute-start.3 = (bf16[144,768]{1,0:T(8,128)(2,1)S(1)}, bf16[144,768]{1,0:T(8,128)(2,1)S(1)}, u32[]{:S(2)}, u32[]{:S(2)}) collective-permute-start(bf16[144,768]{1,0:T(8,128)(2,1)S(1)} %collective-permute-done.2.refs_2_), channel_id=1, source_target_pairs={{0,64},{64,128},{128,192},{192,256},{256,320},{320,384},{384,448},... | collective-permute-start | bytes 663560 | tf_op jit(solution)/shard_map/ppermute | solution.py:377
  87.5 0.0 collective-permute-done.6.refs_6_
  87.6 1.9 %collective-permute-start.7 = (bf16[144,768]{1,0:T(8,128)(2,1)S(1)}, bf16[144,768]{1,0:T(8,128)(2,1)S(1)}, u32[]{:S(2)}, u32[]{:S(2)}) collective-permute-start(bf16[144,768]{1,0:T(8,128)(2,1)S(1)} %collective-permute-done.6.refs_6_), channel_id=1, source_target_pairs={{0,448},{64,0},{128,64},{192,128},{256,192},{320,256},{384,320},{4... | collective-permute-start | bytes 663560 | tf_op jit(solution)/shard_map/ppermute | solution.py:379
  89.5 0.9 collective-permute-done.3.refs_3_
  90.4 5.3 %collective-permute-start.4 = (bf16[144,768]{1,0:T(8,128)(2,1)S(1)}, bf16[144,768]{1,0:T(8,128)(2,1)S(1)}, u32[]{:S(2)}, u32[]{:S(2)}) collective-permute-start(bf16[144,768]{1,0:T(8,128)(2,1)S(1)} %collective-permute-done.3.refs_3_), channel_id=1, source_target_pairs={{0,64},{64,128},{128,192},{192,256},{256,320},{320,384},{384,448},... | collective-permute-start | bytes 663560 | tf_op jit(solution)/shard_map/ppermute | solution.py:377
  95.7 5.1 %collective-permute-start.8 = (bf16[64,768]{1,0:T(8,128)(2,1)}, bf16[64,768]{1,0:T(8,128)(2,1)S(1)}, u32[]{:S(2)}, u32[]{:S(2)}) collective-permute-start(bf16[64,768]{1,0:T(8,128)(2,1)} %bitcast.5.q1_ref), channel_id=1, source_target_pairs={{16,0},{32,16},{48,32},{0,48},{17,1},{33,17},{49,33},{1,49},{18,2}... | collective-permute-start | bytes 294920 | tf_op jit(solution)/shard_map/ppermute | solution.py:398
  100.8 2.3 %collective-permute-start.9 = (bf16[64,768]{1,0:T(8,128)(2,1)}, bf16[64,768]{1,0:T(8,128)(2,1)S(1)}, u32[]{:S(2)}, u32[]{:S(2)}) collective-permute-start(bf16[64,768]{1,0:T(8,128)(2,1)} %bitcast.5.q1_ref), channel_id=1, source_target_pairs={{32,0},{48,16},{0,32},{16,48},{33,1},{49,17},{1,33},{17,49},{34,2}... | collective-permute-start | bytes 294920 | tf_op jit(solution)/shard_map/ppermute | solution.py:398
  103.0 2.1 %collective-permute-start = (bf16[64,768]{1,0:T(8,128)(2,1)}, bf16[64,768]{1,0:T(8,128)(2,1)}, u32[]{:S(2)}, u32[]{:S(2)}) collective-permute-start(bf16[64,768]{1,0:T(8,128)(2,1)} %bitcast.5.q1_ref), channel_id=1, source_target_pairs={{48,0},{0,16},{16,32},{32,48},{49,1},{1,17},{17,33},{33,49},{50,2}... | collective-permute-start | bytes 294920 | tf_op jit(solution)/shard_map/ppermute | solution.py:398
  105.2 0.0 collective-permute-done.8.q0_ref
  105.2 0.0 copy-start.17
  105.2 2.6 %collective-permute-done.9.q1_ref = bf16[64,768]{1,0:T(8,128)(2,1)S(1)} collective-permute-done((bf16[64,768]{1,0:T(8,128)(2,1)}, bf16[64,768]{1,0:T(8,128)(2,1)S(1)}, u32[]{:S(2)}, u32[]{:S(2)}) %collective-permute-start.9) | collective-permute-done | bytes 98336 | tf_op jit(solution)/shard_map/ppermute | solution.py:398
  107.8 0.0 collective-permute-done.7.refs_5_
  107.9 0.0 collective-permute-done.4.refs_4_
  107.9 0.6 copy-done.18
  108.5 0.1 copy-done.15
  108.6 0.7 copy-done.16
  109.3 18.2 %shard_map.180 = (bf16[768,128]{1,0:T(8,128)(2,1)}, bf16[768,128]{1,0:T(8,128)(2,1)}) custom-call(s32[4]{0:T(128)} %pad_add_fusion.ids, bf16[64,768]{1,0:T(8,128)(2,1)} %copy-done.17, bf16[64,768]{1,0:T(8,128)(2,1)} %copy-done.18, bf16[144,768]{1,0:T(8,128)(2,1)} %shard_map.178.refs_0_, bf16[144,768]{1,0:T(8,128)(2,1)} %copy-done.10, ...), custom_call_target="tpu_custom_call" | custom-call | flops 10000000000 | bytes 4194304 | tf_op jit(solution)/shard_map/pallas_call | solution.py:73
  127.5 1.9 %collective-permute-start.10 = (bf16[768,128]{1,0:T(8,128)(2,1)}, bf16[768,128]{1,0:T(8,128)(2,1)S(1)}, u32[]{:S(2)}, u32[]{:S(2)}) collective-permute-start(bf16[768,128]{1,0:T(8,128)(2,1)} %get-tuple-element.16), channel_id=1, source_target_pairs={{0,16},{16,32},{32,48},{48,0},{1,17},{17,33},{33,49},{49,1},{2,18}... | collective-permute-start | bytes 589832 | tf_op jit(solution)/shard_map/ppermute | solution.py:452
  129.4 1.9 %collective-permute-start.11 = (bf16[768,128]{1,0:T(8,128)(2,1)}, bf16[768,128]{1,0:T(8,128)(2,1)S(1)}, u32[]{:S(2)}, u32[]{:S(2)}) collective-permute-start(bf16[768,128]{1,0:T(8,128)(2,1)} %get-tuple-element.17), channel_id=1, source_target_pairs={{0,32},{16,48},{32,0},{48,16},{1,33},{17,49},{33,1},{49,17},{2,34}... | collective-permute-start | bytes 589832 | tf_op jit(solution)/shard_map/ppermute | solution.py:452
  131.3 0.0 all-to-all-done.1.part_ref
  131.3 1.3 copy-done.2
  132.6 3.7 %shard_map.183 = (bf16[768,128]{1,0:T(8,128)(2,1)}, f32[64,256]{1,0:T(8,128)}) custom-call(s32[4]{0:T(128)} %pad_add_fusion.ids, bf16[8,448,256]{2,1,0:T(8,128)(2,1)} %copy-done.2, s32[768,8]{1,0:T(8,128)} %constant.22.clone.table_ref), custom_call_target="tpu_custom_call" | custom-call | flops 1000000000 | bytes 4194304 | tf_op jit(solution)/shard_map/pallas_call | solution.py:73
  136.3 7.3 %all-to-all-start.2 = ((bf16[32,24,128]{2,1,0:T(8,128)(2,1)}), bf16[32,24,128]{2,1,0:T(8,128)(2,1)S(1)}, u32[]{:S(2)}, u32[]{:S(2)}) async-start(bf16[32,24,128]{2,1,0:T(8,128)(2,1)} %bitcast.20), calls=%async_computation.2 | async-start | bytes 393216 | tf_op jit(solution)/shard_map/all_to_all | solution.py:473
  143.6 0.0 copy-start.8
  143.6 0.0 copy-start.9
  143.6 0.0 collective-permute-done.q0_ref
  143.6 17.6 %shard_map.179 = (bf16[768,128]{1,0:T(8,128)(2,1)}, bf16[768,128]{1,0:T(8,128)(2,1)}) custom-call(s32[4]{0:T(128)} %pad_add_fusion.ids, bf16[64,768]{1,0:T(8,128)(2,1)} %collective-permute-done.q0_ref, bf16[64,768]{1,0:T(8,128)(2,1)} %bitcast.5.q1_ref, bf16[144,768]{1,0:T(8,128)(2,1)} %shard_map.178.refs_0_, bf16[144,768]{1,0:T(8,128)(2,1)} %copy-done.10, ...), custom_call_target="tpu_custom_call" | custom-call | flops 10000000000 | bytes 4194304 | tf_op jit(solution)/shard_map/pallas_call | solution.py:73
  161.2 3.5 %collective-permute-start.12 = (bf16[768,128]{1,0:T(8,128)(2,1)}, bf16[768,128]{1,0:T(8,128)(2,1)S(1)}, u32[]{:S(2)}, u32[]{:S(2)}) collective-permute-start(bf16[768,128]{1,0:T(8,128)(2,1)} %get-tuple-element.18), channel_id=1, source_target_pairs={{0,48},{16,0},{32,16},{48,32},{1,49},{17,1},{33,17},{49,33},{2,50}... | collective-permute-start | bytes 589832 | tf_op jit(solution)/shard_map/ppermute | solution.py:452
  164.7 0.0 copy-done.8
  164.7 0.7 copy.19.routes_ref
  165.4 0.7 copy.20.weight_ref
  166.2 0.0 all-to-all-done.2
  166.2 0.7 copy-done.4
  166.8 3.2 %shard_map.184 = (f32[128,128]{1,0:T(8,128)}, f32[128,128]{1,0:T(8,128)}) custom-call(s32[4]{0:T(128)} %pad_add_fusion.ids, bf16[768,128]{1,0:T(8,128)(2,1)} %bitcast.19, s32[128,4]{1,0:T(8,128)} %copy.19.routes_ref, f32[128,4]{1,0:T(8,128)} %copy.20.weight_ref, s32[8,768]{1,0:T(8,128)} %constant.28.table_ref, f32[64,256]{1,0:T(8,128)} %get-tuple-element.21.shared_ref), custom_call_target="tpu_custom_call" | custom-call | flops 1000000000 | bytes 4194304 | tf_op jit(solution)/shard_map/pallas_call | solution.py:73
  170.0 11.7 %collective-permute-start.15 = (f32[128,128]{1,0:T(8,128)}, f32[128,128]{1,0:T(8,128)S(1)}, u32[]{:S(2)}, u32[]{:S(2)}) collective-permute-start(f32[128,128]{1,0:T(8,128)} %get-tuple-element.23), channel_id=1, source_target_pairs={{0,1},{1,0},{2,3},{3,2},{4,5},{5,4},{6,7},{7,6},{8,9},{9,8},{10,11... | collective-permute-start | bytes 196616 | tf_op jit(solution)/shard_map/ppermute | solution.py:501
  181.7 0.0 collective-permute-done.10.refs_1_
  181.7 0.0 collective-permute-done.11.refs_2_
  181.8 0.0 collective-permute-done.12.refs_3_
  181.8 0.6 copy-done.5
  182.4 0.1 copy-done.6
  182.5 0.1 copy-done.7
  182.5 3.8 %shard_map.181 = bf16[64,768]{1,0:T(8,128)(2,1)} custom-call(s32[4]{0:T(128)} %pad_add_fusion.ids, f32[1,64]{1,0:T(1,128)} %bitcast.26, bf16[768,128]{1,0:T(8,128)(2,1)} %get-tuple-element.15.refs_0_, bf16[768,128]{1,0:T(8,128)(2,1)} %copy-done.5, bf16[768,128]{1,0:T(8,128)(2,1)} %copy-done.6, bf16[768,128]{1,0:T(8,128)(2,1)} %copy-done.7), custom_call_target="tpu_custom_call" | custom-call | bytes 4194304 | tf_op jit(solution)/shard_map/pallas_call | solution.py:73
  186.3 0.0 collective-permute-done.15
  186.3 1.5 add_convert_fusion
  (25 shorter events, 0.0 us)
Async XLA Ops:
  5.0 25.2 %all-to-all-start = ((bf16[32,24,512]{2,1,0:T(8,128)(2,1)}), bf16[32,24,512]{2,1,0:T(8,128)(2,1)S(1)}, u32[]{:S(2)}, u32[]{:S(2)}) async-start(bf16[32,24,512]{2,1,0:T(8,128)(2,1)} %bitcast.16), calls=%async_computation | async-start | bytes 1572864 | tf_op jit(solution)/shard_map/all_to_all | solution.py:361
  15.3 17.0 %collective-permute-start.14 = (bf16[480,2048]{1,0:T(8,128)(2,1)}, bf16[480,2048]{1,0:T(8,128)(2,1)S(1)}, u32[]{:S(2)}, u32[]{:S(2)}) collective-permute-start(bf16[480,2048]{1,0:T(8,128)(2,1)} %shard_map.177), channel_id=1, source_target_pairs={{0,1},{1,0},{2,3},{3,2},{4,5},{5,4},{6,7},{7,6},{8,9},{9,8},{10,11... | collective-permute-start | bytes 5898248 | tf_op jit(solution)/shard_map/ppermute | solution.py:393
  30.2 18.3 %copy-start = (bf16[32,24,512]{2,1,0:T(8,128)(2,1)}, bf16[32,24,512]{2,1,0:T(8,128)(2,1)S(1)}, u32[]{:S(2)}) copy-start(bf16[32,24,512]{2,1,0:T(8,128)(2,1)S(1)} %all-to-all-done) | copy-start | bytes 2359300
  30.2 18.3 %collective-permute-start.13 = (bf16[768,512]{1,0:T(8,128)(2,1)S(1)}, bf16[768,512]{1,0:T(8,128)(2,1)S(1)}, u32[]{:S(2)}, u32[]{:S(2)}) collective-permute-start(bf16[768,512]{1,0:T(8,128)(2,1)S(1)} %bitcast.17), channel_id=1, source_target_pairs={{0,2},{2,0},{4,6},{6,4},{8,10},{10,8},{12,14},{14,12},{1,3},{3,1},... | collective-permute-start | bytes 2359304 | tf_op jit(solution)/shard_map/ppermute | solution.py:362
  32.3 16.3 %copy-start.1 = (bf16[480,2048]{1,0:T(8,128)(2,1)}, bf16[480,2048]{1,0:T(8,128)(2,1)S(1)}, u32[]{:S(2)}) copy-start(bf16[480,2048]{1,0:T(8,128)(2,1)S(1)} %collective-permute-done.14.got_ref) | copy-start | bytes 5898244
  48.5 0.9 copy-start.3
  57.4 74.0 %all-to-all-start.1 = ((bf16[8,448,256]{2,1,0:T(8,128)(2,1)}), bf16[8,448,256]{2,1,0:T(8,128)(2,1)S(1)}, u32[]{:S(2)}, u32[]{:S(2)}) async-start(bf16[8,448,256]{2,1,0:T(8,128)(2,1)} %shard_map.182), calls=%async_computation.1 | async-start | bytes 3670016 | tf_op jit(solution)/shard_map/all_to_all | solution.py:436
  66.4 9.8 %collective-permute-start.1 = (bf16[144,768]{1,0:T(8,128)(2,1)}, bf16[144,768]{1,0:T(8,128)(2,1)S(1)}, u32[]{:S(2)}, u32[]{:S(2)}) collective-permute-start(bf16[144,768]{1,0:T(8,128)(2,1)} %shard_map.178.refs_0_), channel_id=1, source_target_pairs={{0,64},{64,128},{128,192},{192,256},{256,320},{320,384},{384,448},... | collective-permute-start | bytes 663560 | tf_op jit(solution)/shard_map/ppermute | solution.py:377
  71.0 8.4 %collective-permute-start.5 = (bf16[144,768]{1,0:T(8,128)(2,1)}, bf16[144,768]{1,0:T(8,128)(2,1)S(1)}, u32[]{:S(2)}, u32[]{:S(2)}) collective-permute-start(bf16[144,768]{1,0:T(8,128)(2,1)} %shard_map.178.refs_0_), channel_id=1, source_target_pairs={{0,448},{64,0},{128,64},{192,128},{256,192},{320,256},{384,320},{4... | collective-permute-start | bytes 663560 | tf_op jit(solution)/shard_map/ppermute | solution.py:379
  76.3 31.6 %copy-start.10 = (bf16[144,768]{1,0:T(8,128)(2,1)}, bf16[144,768]{1,0:T(8,128)(2,1)S(1)}, u32[]{:S(2)}) copy-start(bf16[144,768]{1,0:T(8,128)(2,1)S(1)} %collective-permute-done.1.refs_1_) | copy-start | bytes 663556
  76.3 7.0 %collective-permute-start.2 = (bf16[144,768]{1,0:T(8,128)(2,1)S(1)}, bf16[144,768]{1,0:T(8,128)(2,1)S(1)}, u32[]{:S(2)}, u32[]{:S(2)}) collective-permute-start(bf16[144,768]{1,0:T(8,128)(2,1)S(1)} %collective-permute-done.1.refs_1_), channel_id=1, source_target_pairs={{0,64},{64,128},{128,192},{192,256},{256,320},{320,384},{384,448},... | collective-permute-start | bytes 663560 | tf_op jit(solution)/shard_map/ppermute | solution.py:377
  79.4 28.5 %copy-start.11 = (bf16[144,768]{1,0:T(8,128)(2,1)}, bf16[144,768]{1,0:T(8,128)(2,1)S(1)}, u32[]{:S(2)}) copy-start(bf16[144,768]{1,0:T(8,128)(2,1)S(1)} %collective-permute-done.5.refs_7_) | copy-start | bytes 663556
  79.4 8.2 %collective-permute-start.6 = (bf16[144,768]{1,0:T(8,128)(2,1)S(1)}, bf16[144,768]{1,0:T(8,128)(2,1)S(1)}, u32[]{:S(2)}, u32[]{:S(2)}) collective-permute-start(bf16[144,768]{1,0:T(8,128)(2,1)S(1)} %collective-permute-done.5.refs_7_), channel_id=1, source_target_pairs={{0,448},{64,0},{128,64},{192,128},{256,192},{320,256},{384,320},{4... | collective-permute-start | bytes 663560 | tf_op jit(solution)/shard_map/ppermute | solution.py:379
  83.2 24.6 %copy-start.12 = (bf16[144,768]{1,0:T(8,128)(2,1)}, bf16[144,768]{1,0:T(8,128)(2,1)S(1)}, u32[]{:S(2)}) copy-start(bf16[144,768]{1,0:T(8,128)(2,1)S(1)} %collective-permute-done.2.refs_2_) | copy-start | bytes 663556
  83.2 7.1 %collective-permute-start.3 = (bf16[144,768]{1,0:T(8,128)(2,1)S(1)}, bf16[144,768]{1,0:T(8,128)(2,1)S(1)}, u32[]{:S(2)}, u32[]{:S(2)}) collective-permute-start(bf16[144,768]{1,0:T(8,128)(2,1)S(1)} %collective-permute-done.2.refs_2_), channel_id=1, source_target_pairs={{0,64},{64,128},{128,192},{192,256},{256,320},{320,384},{384,448},... | collective-permute-start | bytes 663560 | tf_op jit(solution)/shard_map/ppermute | solution.py:377
  87.6 20.3 %copy-start.13 = (bf16[144,768]{1,0:T(8,128)(2,1)}, bf16[144,768]{1,0:T(8,128)(2,1)S(1)}, u32[]{:S(2)}) copy-start(bf16[144,768]{1,0:T(8,128)(2,1)S(1)} %collective-permute-done.6.refs_6_) | copy-start | bytes 663556
  87.6 20.3 %collective-permute-start.7 = (bf16[144,768]{1,0:T(8,128)(2,1)S(1)}, bf16[144,768]{1,0:T(8,128)(2,1)S(1)}, u32[]{:S(2)}, u32[]{:S(2)}) collective-permute-start(bf16[144,768]{1,0:T(8,128)(2,1)S(1)} %collective-permute-done.6.refs_6_), channel_id=1, source_target_pairs={{0,448},{64,0},{128,64},{192,128},{256,192},{320,256},{384,320},{4... | collective-permute-start | bytes 663560 | tf_op jit(solution)/shard_map/ppermute | solution.py:379
  90.4 17.5 %copy-start.14 = (bf16[144,768]{1,0:T(8,128)(2,1)}, bf16[144,768]{1,0:T(8,128)(2,1)S(1)}, u32[]{:S(2)}) copy-start(bf16[144,768]{1,0:T(8,128)(2,1)S(1)} %collective-permute-done.3.refs_3_) | copy-start | bytes 663556
  90.4 17.5 %collective-permute-start.4 = (bf16[144,768]{1,0:T(8,128)(2,1)S(1)}, bf16[144,768]{1,0:T(8,128)(2,1)S(1)}, u32[]{:S(2)}, u32[]{:S(2)}) collective-permute-start(bf16[144,768]{1,0:T(8,128)(2,1)S(1)} %collective-permute-done.3.refs_3_), channel_id=1, source_target_pairs={{0,64},{64,128},{128,192},{192,256},{256,320},{320,384},{384,448},... | collective-permute-start | bytes 663560 | tf_op jit(solution)/shard_map/ppermute | solution.py:377
  95.7 9.5 %collective-permute-start.8 = (bf16[64,768]{1,0:T(8,128)(2,1)}, bf16[64,768]{1,0:T(8,128)(2,1)S(1)}, u32[]{:S(2)}, u32[]{:S(2)}) collective-permute-start(bf16[64,768]{1,0:T(8,128)(2,1)} %bitcast.5.q1_ref), channel_id=1, source_target_pairs={{16,0},{32,16},{48,32},{0,48},{17,1},{33,17},{49,33},{1,49},{18,2}... | collective-permute-start | bytes 294920 | tf_op jit(solution)/shard_map/ppermute | solution.py:398
  100.8 7.1 %collective-permute-start.9 = (bf16[64,768]{1,0:T(8,128)(2,1)}, bf16[64,768]{1,0:T(8,128)(2,1)S(1)}, u32[]{:S(2)}, u32[]{:S(2)}) collective-permute-start(bf16[64,768]{1,0:T(8,128)(2,1)} %bitcast.5.q1_ref), channel_id=1, source_target_pairs={{32,0},{48,16},{0,32},{16,48},{33,1},{49,17},{1,33},{17,49},{34,2}... | collective-permute-start | bytes 294920 | tf_op jit(solution)/shard_map/ppermute | solution.py:398
  103.0 40.6 %collective-permute-start = (bf16[64,768]{1,0:T(8,128)(2,1)}, bf16[64,768]{1,0:T(8,128)(2,1)}, u32[]{:S(2)}, u32[]{:S(2)}) collective-permute-start(bf16[64,768]{1,0:T(8,128)(2,1)} %bitcast.5.q1_ref), channel_id=1, source_target_pairs={{48,0},{0,16},{16,32},{32,48},{49,1},{1,17},{17,33},{33,49},{50,2}... | collective-permute-start | bytes 294920 | tf_op jit(solution)/shard_map/ppermute | solution.py:398
  105.2 2.7 %copy-start.17 = (bf16[64,768]{1,0:T(8,128)(2,1)}, bf16[64,768]{1,0:T(8,128)(2,1)S(1)}, u32[]{:S(2)}) copy-start(bf16[64,768]{1,0:T(8,128)(2,1)S(1)} %collective-permute-done.8.q0_ref) | copy-start | bytes 294916
  107.8 0.6 copy-start.18
  107.9 0.7 copy-start.15
  108.6 0.7 copy-start.16
  127.5 54.2 %collective-permute-start.10 = (bf16[768,128]{1,0:T(8,128)(2,1)}, bf16[768,128]{1,0:T(8,128)(2,1)S(1)}, u32[]{:S(2)}, u32[]{:S(2)}) collective-permute-start(bf16[768,128]{1,0:T(8,128)(2,1)} %get-tuple-element.16), channel_id=1, source_target_pairs={{0,16},{16,32},{32,48},{48,0},{1,17},{17,33},{33,49},{49,1},{2,18}... | collective-permute-start | bytes 589832 | tf_op jit(solution)/shard_map/ppermute | solution.py:452
  129.4 52.3 %collective-permute-start.11 = (bf16[768,128]{1,0:T(8,128)(2,1)}, bf16[768,128]{1,0:T(8,128)(2,1)S(1)}, u32[]{:S(2)}, u32[]{:S(2)}) collective-permute-start(bf16[768,128]{1,0:T(8,128)(2,1)} %get-tuple-element.17), channel_id=1, source_target_pairs={{0,32},{16,48},{32,0},{48,16},{1,33},{17,49},{33,1},{49,17},{2,34}... | collective-permute-start | bytes 589832 | tf_op jit(solution)/shard_map/ppermute | solution.py:452
  131.3 1.3 copy-start.2
  136.3 29.9 %all-to-all-start.2 = ((bf16[32,24,128]{2,1,0:T(8,128)(2,1)}), bf16[32,24,128]{2,1,0:T(8,128)(2,1)S(1)}, u32[]{:S(2)}, u32[]{:S(2)}) async-start(bf16[32,24,128]{2,1,0:T(8,128)(2,1)} %bitcast.20), calls=%async_computation.2 | async-start | bytes 393216 | tf_op jit(solution)/shard_map/all_to_all | solution.py:473
  143.6 21.1 %copy-start.8 = (s32[128,4]{0,1:T(4,128)S(1)}, s32[128,4]{0,1:T(4,128)}, u32[]{:S(2)}) copy-start(s32[128,4]{0,1:T(4,128)} %param.24) | copy-start | bytes 6148
  143.6 21.8 %copy-start.9 = (f32[128,4]{0,1:T(4,128)S(1)}, f32[128,4]{0,1:T(4,128)}, u32[]{:S(2)}) copy-start(f32[128,4]{0,1:T(4,128)} %param.25) | copy-start | bytes 6148
  161.2 20.6 %collective-permute-start.12 = (bf16[768,128]{1,0:T(8,128)(2,1)}, bf16[768,128]{1,0:T(8,128)(2,1)S(1)}, u32[]{:S(2)}, u32[]{:S(2)}) collective-permute-start(bf16[768,128]{1,0:T(8,128)(2,1)} %get-tuple-element.18), channel_id=1, source_target_pairs={{0,48},{16,0},{32,16},{48,32},{1,49},{17,1},{33,17},{49,33},{2,50}... | collective-permute-start | bytes 589832 | tf_op jit(solution)/shard_map/ppermute | solution.py:452
  166.2 0.7 copy-start.4
  170.0 16.3 %collective-permute-start.15 = (f32[128,128]{1,0:T(8,128)}, f32[128,128]{1,0:T(8,128)S(1)}, u32[]{:S(2)}, u32[]{:S(2)}) collective-permute-start(f32[128,128]{1,0:T(8,128)} %get-tuple-element.23), channel_id=1, source_target_pairs={{0,1},{1,0},{2,3},{3,2},{4,5},{5,4},{6,7},{7,6},{8,9},{9,8},{10,11... | collective-permute-start | bytes 196616 | tf_op jit(solution)/shard_map/ppermute | solution.py:501
  181.7 0.7 copy-start.5
  181.7 0.7 copy-start.6
  181.8 0.8 copy-start.7

commit v5 on v4

--- a/solution.py
+++ b/solution.py
@@ -267,35 +267,37 @@
         g, u = dot_t(rows[l * n : (l + 1) * n], wg), dot_t(rows[l * n : (l + 1) * n], wu)
         h = gated(g, u).astype(BF16)
         wd = jnp.concatenate([down_ref[l], got_ref[256 + l * 64 : 320 + l * 64, :]], axis=0)
-        for y in range(NY):
-            out_ref[y, l * n : (l + 1) * n, :] = dot(h, wd[:, y * 256 : y * 256 + 256]).astype(BF16)
+        part = dot(h, wd).astype(BF16)
+        for to in range(NY * NC):
+            out_ref[to, l * n : (l + 1) * n, :] = part[:, to * 128 : to * 128 + 128]
     tokens = normed_ref[pl.ds(pl.multiple_of(c * 64, 64), 64), :]
     wg = jnp.concatenate([sgate_ref[...], got_ref[384:416, :]], axis=0)
     wu = jnp.concatenate([sup_ref[...], got_ref[416:448, :]], axis=0)
     h = gated(dot_t(tokens, wg), dot_t(tokens, wu)).astype(BF16)
     wd = jnp.concatenate([sdown_ref[...], got_ref[448:480, :]], axis=0)
-    for y in range(NY):
-        part = dot(h, wd[:, y * 256 : y * 256 + 256])
-        out_ref[y, SLOTS : SLOTS + 64, :] = part.astype(BF16)
+    part = dot(h, wd).astype(BF16)
+    for to in range(NY * NC):
+        out_ref[to, SLOTS : SLOTS + 64, :] = part[:, to * 128 : to * 128 + 128]
 
 
 def sum_body(ids, part_ref, table_ref, out_ref, shared_ref):
-    total = jnp.zeros((SLOTS + 64, 256), F32)
-    for y in range(NY):
-        total = total + part_ref[y].astype(F32)
-    shared_ref[...] = total[SLOTS:]
-    rows = total[:SLOTS].astype(BF16)
+    rows = []
+    for c in range(NC):
+        total = jnp.zeros((SLOTS + 64, 128), F32)
+        for y in range(NY):
+            total = total + part_ref[NC * y + c].astype(F32)
+        shared_ref[c * 64 : c * 64 + 64, :] = total[SLOTS:]
+        rows.append(total[:SLOTS].astype(BF16))
     lane = lax.broadcasted_iota(jnp.int32, (2 * SLOTS, SLOTS), 1)
     place = jnp.where(lane == table_ref[:, 3:4], 1.0, 0.0)
     half = table_ref[:, 2:3]
     first = jnp.where(half == 0, place, 0.0).astype(BF16)
     second = jnp.where(half == 1, place, 0.0).astype(BF16)
-    out_ref[...] = (dot(first, rows[:, :128]) + dot(second, rows[:, 128:])).astype(BF16)
-
-
-def weigh_body(ids, y_ref, routes_ref, weight_ref, table_ref, shared_ref, own_ref, send_ref):
-    c = ids[2]
-    expert = table_ref[0:1, :] + 2 * c
+    out_ref[...] = (dot(first, rows[0]) + dot(second, rows[1])).astype(BF16)
+
+
+def weigh_body(ids, y_ref, routes_ref, weight_ref, table_ref, shared_ref, out_ref):
+    expert = table_ref[0:1, :] + 2 * table_ref[2:3, :]
     member = jnp.zeros((TOK, 2 * SLOTS), F32)
     weight = jnp.zeros((TOK, 2 * SLOTS), F32)
     for k in range(4):
@@ -307,19 +309,10 @@
     earlier = jnp.where(before < after, 1.0, 0.0).astype(BF16)
     rank = dot(earlier, member.astype(BF16))
     weight = jnp.where(rank == table_ref[1:2, :].astype(F32), weight, 0.0)
-    half = table_ref[2:3, :]
-    y = y_ref[...]
-    row = lax.broadcasted_iota(jnp.int32, (TOK, 128), 0)
-    mine = (row >= c * 64) & (row < c * 64 + 64)
-    shared = shared_ref[...]
-    shared = jnp.concatenate([shared, shared], axis=0)
-    for which, ref in ((c, own_ref), (1 - c, send_ref)):
-        part = jnp.where(half == which, weight, 0.0)
-        total = jnp.zeros((TOK, 128), F32)
-        for piece in three_pieces(part):
-            total = total + dot(piece, y)
-        columns = jnp.where(which == 0, shared[:, :128], shared[:, 128:])
-        ref[...] = total + jnp.where(mine, columns, 0.0)
+    total = shared_ref[...]
+    for piece in three_pieces(weight):
+        total = total + dot(piece, y_ref[...])
+    out_ref[...] = total.astype(BF16)
 
 
 def on_device(
@@ -370,13 +363,13 @@
         whole((KVG, ROWS)),
         (keys.T, values.T, cum_gate.reshape(1, ROWS), sent),
     )
-    later = [(i, (i + 1) % NZ) for i in range(NZ)]
-    earlier = [(i, (i - 1) % NZ) for i in range(NZ)]
     rising, falling = [packed], [packed]
     for turn in range(1, 5):
-        rising.append(lax.ppermute(rising[-1], "z", later))
+        up = [(i, i + 1) for i in range(turn - 1, NZ - 1)]
+        rising.append(lax.ppermute(rising[-1], "z", up))
         if turn < 4:
-            falling.append(lax.ppermute(falling[-1], "z", earlier))
+            down = [(i % NZ, (i - 1) % NZ) for i in range(1 - turn, 4 - turn)]
+            falling.append(lax.ppermute(falling[-1], "z", down))
     kvg = rising + falling[:0:-1]
 
     other = pl.BlockSpec((LOCAL, 64, D), lambda i, s: (1 - s[2], 0, 0))
@@ -400,7 +393,7 @@
     mine = pl.BlockSpec((LOCAL, 64, D), lambda i, s: (s[2], 0, 0))
     products = call(
         experts_body,
-        jax.ShapeDtypeStruct((NY, SLOTS + 64, 256), BF16),
+        jax.ShapeDtypeStruct((NY * NC, SLOTS + 64, 128), BF16),
         ids,
         (1,),
         [
@@ -416,7 +409,7 @@
             whole((32, D)),
             whole((SLOTS, 8)),
         ],
-        whole((NY, SLOTS + 64, 256)),
+        whole((NY * NC, SLOTS + 64, 128)),
         (
             arrived,
             arrived_too,
@@ -433,7 +426,7 @@
         scratch=[pltpu.VMEM((2 * SLOTS, D // 4), BF16)] * 2,
         flops=1_000_000_000,
     )
-    products = lax.all_to_all(products, "y", 0, 0, tiled=True)
+    products = lax.all_to_all(products, ("y", "c"), 0, 0, tiled=True)
 
     def attend(turns):
         return call(
@@ -461,12 +454,12 @@
         sum_body,
         (
             jax.ShapeDtypeStruct((2 * SLOTS, 128), BF16),
-            jax.ShapeDtypeStruct((64, 256), F32),
+            jax.ShapeDtypeStruct((TOK, 128), F32),
         ),
         ids,
         (1,),
-        [whole((NY, SLOTS + 64, 256)), whole((2 * SLOTS, 8))],
-        (whole((2 * SLOTS, 128)), whole((64, 256))),
+        [whole((NY * NC, SLOTS + 64, 128)), whole((2 * SLOTS, 8))],
+        (whole((2 * SLOTS, 128)), whole((TOK, 128))),
         (products, table),
         flops=1_000_000_000,
     )
@@ -482,9 +475,9 @@
         (head_gain.reshape(1, HEAD), part0, part1, part2, part3),
     ).T
 
-    own, give = call(
+    expert_out = call(
         weigh_body,
-        (jax.ShapeDtypeStruct((TOK, 128), F32), jax.ShapeDtypeStruct((TOK, 128), F32)),
+        jax.ShapeDtypeStruct((TOK, 128), BF16),
         ids,
         (1,),
         [
@@ -492,14 +485,12 @@
             whole((TOK, 4)),
             whole((TOK, 4)),
             whole((8, 2 * SLOTS)),
-            whole((64, 256)),
+            whole((TOK, 128)),
         ],
-        (whole((TOK, 128)), whole((TOK, 128))),
+        whole((TOK, 128)),
         (returned, routes, route_weight, table.T, shared),
         flops=1_000_000_000,
     )
-    taken = lax.ppermute(give, "c", swap)
-    expert_out = (own + taken).astype(BF16)
     return (mixed, expert_out)
 
 

time: 189 us -> 184 us (0.974)
  the two profiles are of different devices: /device:TPU:473 before, /device:TPU:454 now
where the time goes in v5:
time: 184 us; the launch traced here: 183 us
  Pallas kernels  61.3 us (33%)
  starting transfers between devices  58.7 us (32%)
  waiting for transfers between devices  55 us (30%)
  local copies, waits for them, and re-layouts  6.34 us (3%)
    pallas_call x9, Pallas kernels, call(): pl.pallas_call(body, out_shape=out_shape, grid_spec=pltpu.PrefetchScalarG...  61.3 us
    ppermute x1, waiting for transfers between devices, on_device(): arrived_too = lax.ppermute(arrived, 'y', [(i, i ^ 1) for i in range(NY)])  14.8 us
    ppermute x4, waiting for transfers between devices, on_device(): rising.append(lax.ppermute(rising[-1], 'z', up))  14.6 us
    all_to_all x1, waiting for transfers between devices, on_device(): arrived = lax.all_to_all(sent, ('z', 'x'), 0, 0, tiled=True)  13.4 us
    ppermute x3, starting transfers between devices, send_part(): return lax.ppermute(part, 'x', [(i, (i + d) % NX) for i in range(NX)])  10.9 us
    ppermute x3, starting transfers between devices, on_device(): lax.ppermute(mine, 'x', [((i + d) % NX, i) for i in range(NX)])  9.47 us
    all_to_all x1, starting transfers between devices, on_device(): returned = lax.all_to_all(rows, ('z', 'x'), 0, 0, tiled=True)  8.37 us
    all_to_all x1, starting transfers between devices, on_device(): products = lax.all_to_all(products, ('y', 'c'), 0, 0, tiled=True)  7.2 us
  transfers between devices with their start and end apart: 18, of which 9 were waited for; matrix products, arithmetic and copies ran while one was open for 1% of the time, Pallas kernels for 25%

profile of v5, /device:TPU:454, one launch (start us, length us, event | category | flops | bytes accessed | tf_op | source)
XLA Modules:
  0.0 182.9 jit_solution(18071400247390152642)
XLA Ops:
  0.6 0.7 pad_add_fusion.ids
  1.3 3.8 %shard_map.176 = (bf16[128,2048]{1,0:T(8,128)(2,1)}, bf16[768,512]{1,0:T(8,128)(2,1)}) custom-call(s32[4]{0:T(128)} %pad_add_fusion.ids, bf16[128,2048]{1,0:T(8,128)(2,1)} %x_ref.1, f32[1,2048]{1,0:T(1,128)} %bitcast.27, s32[4,128]{1,0:T(4,128)} %bitcast.25, s32[768,8]{1,0:T(8,128)} %constant.22.clone.table_ref), custom_call_target="tpu_custom_call" | custom-call | flops 1000000000 | bytes 4194304 | tf_op jit(solution)/shard_map/pallas_call | solution.py:73
  5.1 7.1 %all-to-all-start = ((bf16[32,24,512]{2,1,0:T(8,128)(2,1)}), bf16[32,24,512]{2,1,0:T(8,128)(2,1)S(1)}, u32[]{:S(2)}, u32[]{:S(2)}) async-start(bf16[32,24,512]{2,1,0:T(8,128)(2,1)} %bitcast.16), calls=%async_computation | async-start | bytes 1572864 | tf_op jit(solution)/shard_map/all_to_all | solution.py:354
  12.2 3.6 %shard_map.177 = bf16[480,2048]{1,0:T(8,128)(2,1)} custom-call(s32[4]{0:T(128)} %pad_add_fusion.ids, bf16[4,64,2048]{2,1,0:T(8,128)(2,1)} %gate_ref.3, bf16[4,64,2048]{2,1,0:T(8,128)(2,1)} %up_ref.3, bf16[4,64,2048]{2,1,0:T(8,128)(2,1)} %down_ref.3, bf16[32,2048]{1,0:T(8,128)(2,1)} %sgate_ref.3, bf16[32,2048]{1,0:T(8,128)(2,1)} %sup_ref.3, ...), custom_call_target="tpu_custom_call" | custom-call | flops 1000000000 | bytes 4194304 | tf_op jit(solution)/shard_map/pallas_call | solution.py:73
  15.8 1.9 %collective-permute-start.14 = (bf16[480,2048]{1,0:T(8,128)(2,1)}, bf16[480,2048]{1,0:T(8,128)(2,1)S(1)}, u32[]{:S(2)}, u32[]{:S(2)}) collective-permute-start(bf16[480,2048]{1,0:T(8,128)(2,1)} %shard_map.177), channel_id=1, source_target_pairs={{0,1},{1,0},{2,3},{3,2},{4,5},{5,4},{6,7},{7,6},{8,9},{9,8},{10,11... | collective-permute-start | bytes 5898248 | tf_op jit(solution)/shard_map/ppermute | solution.py:386
  17.7 13.4 %all-to-all-done = bf16[32,24,512]{2,1,0:T(8,128)(2,1)S(1)} async-done(((bf16[32,24,512]{2,1,0:T(8,128)(2,1)}), bf16[32,24,512]{2,1,0:T(8,128)(2,1)S(1)}, u32[]{:S(2)}, u32[]{:S(2)}) %all-to-all-start) | async-done | bytes 786464 | tf_op jit(solution)/shard_map/all_to_all | solution.py:354
  31.1 3.5 %collective-permute-start.13 = (bf16[768,512]{1,0:T(8,128)(2,1)S(1)}, bf16[768,512]{1,0:T(8,128)(2,1)S(1)}, u32[]{:S(2)}, u32[]{:S(2)}) collective-permute-start(bf16[768,512]{1,0:T(8,128)(2,1)S(1)} %bitcast.17), channel_id=1, source_target_pairs={{0,2},{2,0},{4,6},{6,4},{8,10},{10,8},{12,14},{14,12},{1,3},{3,1},... | collective-permute-start | bytes 2359304 | tf_op jit(solution)/shard_map/ppermute | solution.py:355
  34.6 0.0 collective-permute-done.14.got_ref
  34.6 0.0 copy-start.1
  34.6 14.8 %collective-permute-done.13.x_got_ref = bf16[768,512]{1,0:T(8,128)(2,1)S(1)} collective-permute-done((bf16[768,512]{1,0:T(8,128)(2,1)S(1)}, bf16[768,512]{1,0:T(8,128)(2,1)S(1)}, u32[]{:S(2)}, u32[]{:S(2)}) %collective-permute-start.13) | collective-permute-done | bytes 786464 | tf_op jit(solution)/shard_map/ppermute | solution.py:355
  49.4 0.0 copy-done
  49.4 0.0 copy-done.1
  49.4 0.9 copy-done.3
  50.3 8.0 %shard_map.182 = bf16[16,448,128]{2,1,0:T(8,128)(2,1)} custom-call(s32[4]{0:T(128)} %pad_add_fusion.ids, bf16[768,512]{1,0:T(8,128)(2,1)} %bitcast.18, bf16[768,512]{1,0:T(8,128)(2,1)} %copy-done.3, bf16[4,64,2048]{2,1,0:T(8,128)(2,1)} %gate_ref.3, bf16[4,64,2048]{2,1,0:T(8,128)(2,1)} %up_ref.3, bf16[4,64,2048]{2,1,0:T(8,128)(2,1)} %down_ref.3, ...), custom_call_target="tpu_custom_call" | custom-call | flops 1000000000 | bytes 4194304 | tf_op jit(solution)/shard_map/pallas_call | solution.py:73
  58.3 7.2 %all-to-all-start.1 = ((bf16[16,448,128]{2,1,0:T(8,128)(2,1)}), bf16[16,448,128]{2,1,0:T(8,128)(2,1)S(1)}, u32[]{:S(2)}, u32[]{:S(2)}) async-start(bf16[16,448,128]{2,1,0:T(8,128)(2,1)} %shard_map.182), calls=%async_computation.1 | async-start | bytes 3670016 | tf_op jit(solution)/shard_map/all_to_all | solution.py:429
  65.5 2.3 %shard_map.178.refs_0_ = bf16[144,768]{1,0:T(8,128)(2,1)} custom-call(s32[4]{0:T(128)} %pad_add_fusion.ids, bf16[64,768]{1,0:T(8,128)(2,1)} %bitcast.21, bf16[64,768]{1,0:T(8,128)(2,1)} %bitcast.22, f32[1,768]{1,0:T(1,128)} %bitcast.24, bf16[768,512]{1,0:T(8,128)(2,1)} %get-tuple-element.11.after_ref), custom_call_target="tpu_custom_call" | custom-call | bytes 4194304 | tf_op jit(solution)/shard_map/pallas_call | solution.py:73
  67.8 1.3 collective-permute-start.1
  69.1 1.3 collective-permute-start.5
  70.4 10.0 %collective-permute-done.1.refs_1_ = bf16[144,768]{1,0:T(8,128)(2,1)S(1)} collective-permute-done((bf16[144,768]{1,0:T(8,128)(2,1)}, bf16[144,768]{1,0:T(8,128)(2,1)S(1)}, u32[]{:S(2)}, u32[]{:S(2)}) %collective-permute-start.1) | collective-permute-done | bytes 221216 | tf_op jit(solution)/shard_map/ppermute | solution.py:369
  80.4 1.3 collective-permute-start.2
  81.7 2.6 %collective-permute-done.5.refs_7_ = bf16[144,768]{1,0:T(8,128)(2,1)S(1)} collective-permute-done((bf16[144,768]{1,0:T(8,128)(2,1)}, bf16[144,768]{1,0:T(8,128)(2,1)S(1)}, u32[]{:S(2)}, u32[]{:S(2)}) %collective-permute-start.5) | collective-permute-done | bytes 221216 | tf_op jit(solution)/shard_map/ppermute | solution.py:372
  84.4 1.9 %collective-permute-start.6 = (bf16[144,768]{1,0:T(8,128)(2,1)S(1)}, bf16[144,768]{1,0:T(8,128)(2,1)S(1)}, u32[]{:S(2)}, u32[]{:S(2)}) collective-permute-start(bf16[144,768]{1,0:T(8,128)(2,1)S(1)} %collective-permute-done.5.refs_7_), channel_id=1, source_target_pairs={{448,384},{0,448},{64,0},{449,385},{1,449},{65,1},{450,386},{2,450... | collective-permute-start | bytes 663560 | tf_op jit(solution)/shard_map/ppermute | solution.py:372
  86.3 3.2 %collective-permute-done.2.refs_2_ = bf16[144,768]{1,0:T(8,128)(2,1)S(1)} collective-permute-done((bf16[144,768]{1,0:T(8,128)(2,1)S(1)}, bf16[144,768]{1,0:T(8,128)(2,1)S(1)}, u32[]{:S(2)}, u32[]{:S(2)}) %collective-permute-start.2) | collective-permute-done | bytes 221216 | tf_op jit(solution)/shard_map/ppermute | solution.py:369
  89.5 1.3 collective-permute-start.3
  90.8 3.6 %collective-permute-done.6.refs_6_ = bf16[144,768]{1,0:T(8,128)(2,1)S(1)} collective-permute-done((bf16[144,768]{1,0:T(8,128)(2,1)S(1)}, bf16[144,768]{1,0:T(8,128)(2,1)S(1)}, u32[]{:S(2)}, u32[]{:S(2)}) %collective-permute-start.6) | collective-permute-done | bytes 221216 | tf_op jit(solution)/shard_map/ppermute | solution.py:372
  94.3 1.9 %collective-permute-start.7 = (bf16[144,768]{1,0:T(8,128)(2,1)S(1)}, bf16[144,768]{1,0:T(8,128)(2,1)S(1)}, u32[]{:S(2)}, u32[]{:S(2)}) collective-permute-start(bf16[144,768]{1,0:T(8,128)(2,1)S(1)} %collective-permute-done.6.refs_6_), channel_id=1, source_target_pairs={{384,320},{448,384},{0,448},{385,321},{449,385},{1,449},{386,322},... | collective-permute-start | bytes 663560 | tf_op jit(solution)/shard_map/ppermute | solution.py:372
  96.3 1.4 collective-permute-done.3.refs_3_
  97.7 1.3 collective-permute-start.4
  99.0 2.5 %collective-permute-start.8 = (bf16[64,768]{1,0:T(8,128)(2,1)}, bf16[64,768]{1,0:T(8,128)(2,1)S(1)}, u32[]{:S(2)}, u32[]{:S(2)}) collective-permute-start(bf16[64,768]{1,0:T(8,128)(2,1)} %bitcast.5.q1_ref), channel_id=1, source_target_pairs={{16,0},{32,16},{48,32},{0,48},{17,1},{33,17},{49,33},{1,49},{18,2}... | collective-permute-start | bytes 294920 | tf_op jit(solution)/shard_map/ppermute | solution.py:391
  101.5 3.5 %collective-permute-start.9 = (bf16[64,768]{1,0:T(8,128)(2,1)}, bf16[64,768]{1,0:T(8,128)(2,1)S(1)}, u32[]{:S(2)}, u32[]{:S(2)}) collective-permute-start(bf16[64,768]{1,0:T(8,128)(2,1)} %bitcast.5.q1_ref), channel_id=1, source_target_pairs={{32,0},{48,16},{0,32},{16,48},{33,1},{49,17},{1,33},{17,49},{34,2}... | collective-permute-start | bytes 294920 | tf_op jit(solution)/shard_map/ppermute | solution.py:391
  105.0 3.4 %collective-permute-start = (bf16[64,768]{1,0:T(8,128)(2,1)}, bf16[64,768]{1,0:T(8,128)(2,1)}, u32[]{:S(2)}, u32[]{:S(2)}) collective-permute-start(bf16[64,768]{1,0:T(8,128)(2,1)} %bitcast.5.q1_ref), channel_id=1, source_target_pairs={{48,0},{0,16},{16,32},{32,48},{49,1},{1,17},{17,33},{33,49},{50,2}... | collective-permute-start | bytes 294920 | tf_op jit(solution)/shard_map/ppermute | solution.py:391
  108.4 0.0 collective-permute-done.8.q0_ref
  108.5 0.0 copy-start.17
  108.5 1.2 collective-permute-done.9.q1_ref
  109.7 0.0 collective-permute-done.7.refs_5_
  109.7 0.0 collective-permute-done.4.refs_4_
  109.7 0.0 copy-done.10
  109.7 0.0 copy-done.11
  109.7 0.0 copy-done.12
  109.8 0.6 copy-done.18
  110.3 0.1 copy-done.15
  110.4 0.7 copy-done.16
  111.1 16.6 %shard_map.180 = (bf16[768,128]{1,0:T(8,128)(2,1)}, bf16[768,128]{1,0:T(8,128)(2,1)}) custom-call(s32[4]{0:T(128)} %pad_add_fusion.ids, bf16[64,768]{1,0:T(8,128)(2,1)} %copy-done.17, bf16[64,768]{1,0:T(8,128)(2,1)} %copy-done.18, bf16[144,768]{1,0:T(8,128)(2,1)} %shard_map.178.refs_0_, bf16[144,768]{1,0:T(8,128)(2,1)} %copy-done.10, ...), custom_call_target="tpu_custom_call" | custom-call | flops 10000000000 | bytes 4194304 | tf_op jit(solution)/shard_map/pallas_call | solution.py:73
  127.7 6.2 %collective-permute-start.10 = (bf16[768,128]{1,0:T(8,128)(2,1)}, bf16[768,128]{1,0:T(8,128)(2,1)S(1)}, u32[]{:S(2)}, u32[]{:S(2)}) collective-permute-start(bf16[768,128]{1,0:T(8,128)(2,1)} %get-tuple-element.14), channel_id=1, source_target_pairs={{0,16},{16,32},{32,48},{48,0},{1,17},{17,33},{33,49},{49,1},{2,18}... | collective-permute-start | bytes 589832 | tf_op jit(solution)/shard_map/ppermute | solution.py:445
  133.9 1.9 %collective-permute-start.11 = (bf16[768,128]{1,0:T(8,128)(2,1)}, bf16[768,128]{1,0:T(8,128)(2,1)S(1)}, u32[]{:S(2)}, u32[]{:S(2)}) collective-permute-start(bf16[768,128]{1,0:T(8,128)(2,1)} %get-tuple-element.15), channel_id=1, source_target_pairs={{0,32},{16,48},{32,0},{48,16},{1,33},{17,49},{33,1},{49,17},{2,34}... | collective-permute-start | bytes 589832 | tf_op jit(solution)/shard_map/ppermute | solution.py:445
  135.8 0.0 all-to-all-done.1.part_ref
  135.8 1.2 copy-done.2
  137.1 3.6 %shard_map.183 = (bf16[768,128]{1,0:T(8,128)(2,1)}, f32[128,128]{1,0:T(8,128)}) custom-call(s32[4]{0:T(128)} %pad_add_fusion.ids, bf16[16,448,128]{2,1,0:T(8,128)(2,1)} %copy-done.2, s32[768,8]{1,0:T(8,128)} %constant.22.clone.table_ref), custom_call_target="tpu_custom_call" | custom-call | flops 1000000000 | bytes 4194304 | tf_op jit(solution)/shard_map/pallas_call | solution.py:73
  140.7 8.4 %all-to-all-start.2 = ((bf16[32,24,128]{2,1,0:T(8,128)(2,1)}), bf16[32,24,128]{2,1,0:T(8,128)(2,1)S(1)}, u32[]{:S(2)}, u32[]{:S(2)}) async-start(bf16[32,24,128]{2,1,0:T(8,128)(2,1)} %bitcast.20), calls=%async_computation.2 | async-start | bytes 393216 | tf_op jit(solution)/shard_map/all_to_all | solution.py:466
  149.1 0.0 copy-start.8
  149.1 0.0 copy-start.9
  149.1 0.0 collective-permute-done.q0_ref
  149.1 16.7 %shard_map.179 = (bf16[768,128]{1,0:T(8,128)(2,1)}, bf16[768,128]{1,0:T(8,128)(2,1)}) custom-call(s32[4]{0:T(128)} %pad_add_fusion.ids, bf16[64,768]{1,0:T(8,128)(2,1)} %collective-permute-done.q0_ref, bf16[64,768]{1,0:T(8,128)(2,1)} %bitcast.5.q1_ref, bf16[144,768]{1,0:T(8,128)(2,1)} %shard_map.178.refs_0_, bf16[144,768]{1,0:T(8,128)(2,1)} %copy-done.10, ...), custom_call_target="tpu_custom_call" | custom-call | flops 10000000000 | bytes 4194304 | tf_op jit(solution)/shard_map/pallas_call | solution.py:73
  165.9 2.7 %collective-permute-start.12 = (bf16[768,128]{1,0:T(8,128)(2,1)}, bf16[768,128]{1,0:T(8,128)(2,1)S(1)}, u32[]{:S(2)}, u32[]{:S(2)}) collective-permute-start(bf16[768,128]{1,0:T(8,128)(2,1)} %get-tuple-element.16), channel_id=1, source_target_pairs={{0,48},{16,0},{32,16},{48,32},{1,49},{17,1},{33,17},{49,33},{2,50}... | collective-permute-start | bytes 589832 | tf_op jit(solution)/shard_map/ppermute | solution.py:445
  168.6 0.7 copy.19.routes_ref
  169.3 0.7 copy.20.weight_ref
  170.1 0.0 collective-permute-done.10.refs_1_
  170.1 0.0 collective-permute-done.11.refs_2_
  170.1 4.7 %collective-permute-done.12.refs_3_ = bf16[768,128]{1,0:T(8,128)(2,1)S(1)} collective-permute-done((bf16[768,128]{1,0:T(8,128)(2,1)}, bf16[768,128]{1,0:T(8,128)(2,1)S(1)}, u32[]{:S(2)}, u32[]{:S(2)}) %collective-permute-start.12) | collective-permute-done | bytes 196640 | tf_op jit(solution)/shard_map/ppermute | solution.py:445
  174.8 0.7 copy-done.7
  175.5 3.8 %shard_map.181 = bf16[64,768]{1,0:T(8,128)(2,1)} custom-call(s32[4]{0:T(128)} %pad_add_fusion.ids, f32[1,64]{1,0:T(1,128)} %bitcast.26, bf16[768,128]{1,0:T(8,128)(2,1)} %get-tuple-element.13.refs_0_, bf16[768,128]{1,0:T(8,128)(2,1)} %copy-done.5, bf16[768,128]{1,0:T(8,128)(2,1)} %copy-done.6, bf16[768,128]{1,0:T(8,128)(2,1)} %copy-done.7), custom_call_target="tpu_custom_call" | custom-call | bytes 4194304 | tf_op jit(solution)/shard_map/pallas_call | solution.py:73
  179.3 0.0 all-to-all-done.2
  179.3 0.7 copy-done.4
  179.9 2.9 %shard_map.184 = bf16[128,128]{1,0:T(8,128)(2,1)} custom-call(s32[4]{0:T(128)} %pad_add_fusion.ids, bf16[768,128]{1,0:T(8,128)(2,1)} %bitcast.19, s32[128,4]{1,0:T(8,128)} %copy.19.routes_ref, f32[128,4]{1,0:T(8,128)} %copy.20.weight_ref, s32[8,768]{1,0:T(8,128)} %constant.28.table_ref, f32[128,128]{1,0:T(8,128)} %get-tuple-element.19.shared_ref), custom_call_target="tpu_custom_call" | custom-call | flops 1000000000 | bytes 4194304 | tf_op jit(solution)/shard_map/pallas_call | solution.py:73
  (22 shorter events, 0.0 us)
Async XLA Ops:
  5.1 26.0 %all-to-all-start = ((bf16[32,24,512]{2,1,0:T(8,128)(2,1)}), bf16[32,24,512]{2,1,0:T(8,128)(2,1)S(1)}, u32[]{:S(2)}, u32[]{:S(2)}) async-start(bf16[32,24,512]{2,1,0:T(8,128)(2,1)} %bitcast.16), calls=%async_computation | async-start | bytes 1572864 | tf_op jit(solution)/shard_map/all_to_all | solution.py:354
  15.8 18.8 %collective-permute-start.14 = (bf16[480,2048]{1,0:T(8,128)(2,1)}, bf16[480,2048]{1,0:T(8,128)(2,1)S(1)}, u32[]{:S(2)}, u32[]{:S(2)}) collective-permute-start(bf16[480,2048]{1,0:T(8,128)(2,1)} %shard_map.177), channel_id=1, source_target_pairs={{0,1},{1,0},{2,3},{3,2},{4,5},{5,4},{6,7},{7,6},{8,9},{9,8},{10,11... | collective-permute-start | bytes 5898248 | tf_op jit(solution)/shard_map/ppermute | solution.py:386
  31.1 18.3 %copy-start = (bf16[32,24,512]{2,1,0:T(8,128)(2,1)}, bf16[32,24,512]{2,1,0:T(8,128)(2,1)S(1)}, u32[]{:S(2)}) copy-start(bf16[32,24,512]{2,1,0:T(8,128)(2,1)S(1)} %all-to-all-done) | copy-start | bytes 2359300
  31.1 18.3 %collective-permute-start.13 = (bf16[768,512]{1,0:T(8,128)(2,1)S(1)}, bf16[768,512]{1,0:T(8,128)(2,1)S(1)}, u32[]{:S(2)}, u32[]{:S(2)}) collective-permute-start(bf16[768,512]{1,0:T(8,128)(2,1)S(1)} %bitcast.17), channel_id=1, source_target_pairs={{0,2},{2,0},{4,6},{6,4},{8,10},{10,8},{12,14},{14,12},{1,3},{3,1},... | collective-permute-start | bytes 2359304 | tf_op jit(solution)/shard_map/ppermute | solution.py:355
  34.6 14.8 %copy-start.1 = (bf16[480,2048]{1,0:T(8,128)(2,1)}, bf16[480,2048]{1,0:T(8,128)(2,1)S(1)}, u32[]{:S(2)}) copy-start(bf16[480,2048]{1,0:T(8,128)(2,1)S(1)} %collective-permute-done.14.got_ref) | copy-start | bytes 5898244
  49.4 0.9 copy-start.3
  58.3 77.5 %all-to-all-start.1 = ((bf16[16,448,128]{2,1,0:T(8,128)(2,1)}), bf16[16,448,128]{2,1,0:T(8,128)(2,1)S(1)}, u32[]{:S(2)}, u32[]{:S(2)}) async-start(bf16[16,448,128]{2,1,0:T(8,128)(2,1)} %shard_map.182), calls=%async_computation.1 | async-start | bytes 3670016 | tf_op jit(solution)/shard_map/all_to_all | solution.py:429
  67.8 12.6 %collective-permute-start.1 = (bf16[144,768]{1,0:T(8,128)(2,1)}, bf16[144,768]{1,0:T(8,128)(2,1)S(1)}, u32[]{:S(2)}, u32[]{:S(2)}) collective-permute-start(bf16[144,768]{1,0:T(8,128)(2,1)} %shard_map.178.refs_0_), channel_id=1, source_target_pairs={{0,64},{64,128},{128,192},{192,256},{256,320},{320,384},{384,448},... | collective-permute-start | bytes 663560 | tf_op jit(solution)/shard_map/ppermute | solution.py:369
  69.1 15.3 %collective-permute-start.5 = (bf16[144,768]{1,0:T(8,128)(2,1)}, bf16[144,768]{1,0:T(8,128)(2,1)S(1)}, u32[]{:S(2)}, u32[]{:S(2)}) collective-permute-start(bf16[144,768]{1,0:T(8,128)(2,1)} %shard_map.178.refs_0_), channel_id=1, source_target_pairs={{0,448},{64,0},{128,64},{1,449},{65,1},{129,65},{2,450},{66,2},{13... | collective-permute-start | bytes 663560 | tf_op jit(solution)/shard_map/ppermute | solution.py:372
  80.4 29.3 %copy-start.10 = (bf16[144,768]{1,0:T(8,128)(2,1)}, bf16[144,768]{1,0:T(8,128)(2,1)S(1)}, u32[]{:S(2)}) copy-start(bf16[144,768]{1,0:T(8,128)(2,1)S(1)} %collective-permute-done.1.refs_1_) | copy-start | bytes 663556
  80.4 9.0 %collective-permute-start.2 = (bf16[144,768]{1,0:T(8,128)(2,1)S(1)}, bf16[144,768]{1,0:T(8,128)(2,1)S(1)}, u32[]{:S(2)}, u32[]{:S(2)}) collective-permute-start(bf16[144,768]{1,0:T(8,128)(2,1)S(1)} %collective-permute-done.1.refs_1_), channel_id=1, source_target_pairs={{64,128},{128,192},{192,256},{256,320},{320,384},{384,448},{65,129... | collective-permute-start | bytes 663560 | tf_op jit(solution)/shard_map/ppermute | solution.py:369
  84.4 25.4 %copy-start.11 = (bf16[144,768]{1,0:T(8,128)(2,1)}, bf16[144,768]{1,0:T(8,128)(2,1)S(1)}, u32[]{:S(2)}) copy-start(bf16[144,768]{1,0:T(8,128)(2,1)S(1)} %collective-permute-done.5.refs_7_) | copy-start | bytes 663556
  84.4 10.0 %collective-permute-start.6 = (bf16[144,768]{1,0:T(8,128)(2,1)S(1)}, bf16[144,768]{1,0:T(8,128)(2,1)S(1)}, u32[]{:S(2)}, u32[]{:S(2)}) collective-permute-start(bf16[144,768]{1,0:T(8,128)(2,1)S(1)} %collective-permute-done.5.refs_7_), channel_id=1, source_target_pairs={{448,384},{0,448},{64,0},{449,385},{1,449},{65,1},{450,386},{2,450... | collective-permute-start | bytes 663560 | tf_op jit(solution)/shard_map/ppermute | solution.py:372
  89.5 20.3 %copy-start.12 = (bf16[144,768]{1,0:T(8,128)(2,1)}, bf16[144,768]{1,0:T(8,128)(2,1)S(1)}, u32[]{:S(2)}) copy-start(bf16[144,768]{1,0:T(8,128)(2,1)S(1)} %collective-permute-done.2.refs_2_) | copy-start | bytes 663556
  89.5 8.2 %collective-permute-start.3 = (bf16[144,768]{1,0:T(8,128)(2,1)S(1)}, bf16[144,768]{1,0:T(8,128)(2,1)S(1)}, u32[]{:S(2)}, u32[]{:S(2)}) collective-permute-start(bf16[144,768]{1,0:T(8,128)(2,1)S(1)} %collective-permute-done.2.refs_2_), channel_id=1, source_target_pairs={{128,192},{192,256},{256,320},{320,384},{384,448},{129,193},{193,2... | collective-permute-start | bytes 663560 | tf_op jit(solution)/shard_map/ppermute | solution.py:369
  94.3 15.4 %copy-start.13 = (bf16[144,768]{1,0:T(8,128)(2,1)}, bf16[144,768]{1,0:T(8,128)(2,1)S(1)}, u32[]{:S(2)}) copy-start(bf16[144,768]{1,0:T(8,128)(2,1)S(1)} %collective-permute-done.6.refs_6_) | copy-start | bytes 663556
  94.3 15.4 %collective-permute-start.7 = (bf16[144,768]{1,0:T(8,128)(2,1)S(1)}, bf16[144,768]{1,0:T(8,128)(2,1)S(1)}, u32[]{:S(2)}, u32[]{:S(2)}) collective-permute-start(bf16[144,768]{1,0:T(8,128)(2,1)S(1)} %collective-permute-done.6.refs_6_), channel_id=1, source_target_pairs={{384,320},{448,384},{0,448},{385,321},{449,385},{1,449},{386,322},... | collective-permute-start | bytes 663560 | tf_op jit(solution)/shard_map/ppermute | solution.py:372
  97.7 12.1 %copy-start.14 = (bf16[144,768]{1,0:T(8,128)(2,1)}, bf16[144,768]{1,0:T(8,128)(2,1)S(1)}, u32[]{:S(2)}) copy-start(bf16[144,768]{1,0:T(8,128)(2,1)S(1)} %collective-permute-done.3.refs_3_) | copy-start | bytes 663556
  97.7 12.0 %collective-permute-start.4 = (bf16[144,768]{1,0:T(8,128)(2,1)S(1)}, bf16[144,768]{1,0:T(8,128)(2,1)S(1)}, u32[]{:S(2)}, u32[]{:S(2)}) collective-permute-start(bf16[144,768]{1,0:T(8,128)(2,1)S(1)} %collective-permute-done.3.refs_3_), channel_id=1, source_target_pairs={{192,256},{256,320},{320,384},{384,448},{193,257},{257,321},{321,3... | collective-permute-start | bytes 663560 | tf_op jit(solution)/shard_map/ppermute | solution.py:369
  99.0 9.5 %collective-permute-start.8 = (bf16[64,768]{1,0:T(8,128)(2,1)}, bf16[64,768]{1,0:T(8,128)(2,1)S(1)}, u32[]{:S(2)}, u32[]{:S(2)}) collective-permute-start(bf16[64,768]{1,0:T(8,128)(2,1)} %bitcast.5.q1_ref), channel_id=1, source_target_pairs={{16,0},{32,16},{48,32},{0,48},{17,1},{33,17},{49,33},{1,49},{18,2}... | collective-permute-start | bytes 294920 | tf_op jit(solution)/shard_map/ppermute | solution.py:391
  101.5 8.2 %collective-permute-start.9 = (bf16[64,768]{1,0:T(8,128)(2,1)}, bf16[64,768]{1,0:T(8,128)(2,1)S(1)}, u32[]{:S(2)}, u32[]{:S(2)}) collective-permute-start(bf16[64,768]{1,0:T(8,128)(2,1)} %bitcast.5.q1_ref), channel_id=1, source_target_pairs={{32,0},{48,16},{0,32},{16,48},{33,1},{49,17},{1,33},{17,49},{34,2}... | collective-permute-start | bytes 294920 | tf_op jit(solution)/shard_map/ppermute | solution.py:391
  105.0 44.1 %collective-permute-start = (bf16[64,768]{1,0:T(8,128)(2,1)}, bf16[64,768]{1,0:T(8,128)(2,1)}, u32[]{:S(2)}, u32[]{:S(2)}) collective-permute-start(bf16[64,768]{1,0:T(8,128)(2,1)} %bitcast.5.q1_ref), channel_id=1, source_target_pairs={{48,0},{0,16},{16,32},{32,48},{49,1},{1,17},{17,33},{33,49},{50,2}... | collective-permute-start | bytes 294920 | tf_op jit(solution)/shard_map/ppermute | solution.py:391
  108.5 1.3 copy-start.17
  109.7 0.6 copy-start.18
  109.7 0.7 copy-start.15
  110.4 0.7 copy-start.16
  127.7 42.4 %collective-permute-start.10 = (bf16[768,128]{1,0:T(8,128)(2,1)}, bf16[768,128]{1,0:T(8,128)(2,1)S(1)}, u32[]{:S(2)}, u32[]{:S(2)}) collective-permute-start(bf16[768,128]{1,0:T(8,128)(2,1)} %get-tuple-element.14), channel_id=1, source_target_pairs={{0,16},{16,32},{32,48},{48,0},{1,17},{17,33},{33,49},{49,1},{2,18}... | collective-permute-start | bytes 589832 | tf_op jit(solution)/shard_map/ppermute | solution.py:445
  133.9 36.2 %collective-permute-start.11 = (bf16[768,128]{1,0:T(8,128)(2,1)}, bf16[768,128]{1,0:T(8,128)(2,1)S(1)}, u32[]{:S(2)}, u32[]{:S(2)}) collective-permute-start(bf16[768,128]{1,0:T(8,128)(2,1)} %get-tuple-element.15), channel_id=1, source_target_pairs={{0,32},{16,48},{32,0},{48,16},{1,33},{17,49},{33,1},{49,17},{2,34}... | collective-permute-start | bytes 589832 | tf_op jit(solution)/shard_map/ppermute | solution.py:445
  135.8 1.3 copy-start.2
  140.7 38.6 %all-to-all-start.2 = ((bf16[32,24,128]{2,1,0:T(8,128)(2,1)}), bf16[32,24,128]{2,1,0:T(8,128)(2,1)S(1)}, u32[]{:S(2)}, u32[]{:S(2)}) async-start(bf16[32,24,128]{2,1,0:T(8,128)(2,1)} %bitcast.20), calls=%async_computation.2 | async-start | bytes 393216 | tf_op jit(solution)/shard_map/all_to_all | solution.py:466
  149.1 19.5 %copy-start.8 = (s32[128,4]{0,1:T(4,128)S(1)}, s32[128,4]{0,1:T(4,128)}, u32[]{:S(2)}) copy-start(s32[128,4]{0,1:T(4,128)} %param.24) | copy-start | bytes 6148
  149.1 20.2 %copy-start.9 = (f32[128,4]{0,1:T(4,128)S(1)}, f32[128,4]{0,1:T(4,128)}, u32[]{:S(2)}) copy-start(f32[128,4]{0,1:T(4,128)} %param.25) | copy-start | bytes 6148
  165.9 9.0 %collective-permute-start.12 = (bf16[768,128]{1,0:T(8,128)(2,1)}, bf16[768,128]{1,0:T(8,128)(2,1)S(1)}, u32[]{:S(2)}, u32[]{:S(2)}) collective-permute-start(bf16[768,128]{1,0:T(8,128)(2,1)} %get-tuple-element.16), channel_id=1, source_target_pairs={{0,48},{16,0},{32,16},{48,32},{1,49},{17,1},{33,17},{49,33},{2,50}... | collective-permute-start | bytes 589832 | tf_op jit(solution)/shard_map/ppermute | solution.py:445
  170.1 4.8 %copy-start.5 = (bf16[768,128]{1,0:T(8,128)(2,1)}, bf16[768,128]{1,0:T(8,128)(2,1)S(1)}, u32[]{:S(2)}) copy-start(bf16[768,128]{1,0:T(8,128)(2,1)S(1)} %collective-permute-done.10.refs_1_) | copy-start | bytes 589828
  170.1 4.8 %copy-start.6 = (bf16[768,128]{1,0:T(8,128)(2,1)}, bf16[768,128]{1,0:T(8,128)(2,1)S(1)}, u32[]{:S(2)}) copy-start(bf16[768,128]{1,0:T(8,128)(2,1)S(1)} %collective-permute-done.11.refs_2_) | copy-start | bytes 589828
  174.8 0.7 copy-start.7
  179.3 0.7 copy-start.4

commit v6 on v5

--- a/solution.py
+++ b/solution.py
@@ -1,5 +1,3 @@
-import functools
-
 import jax
 import jax.numpy as jnp
 import numpy as np
@@ -122,8 +120,9 @@
 DEPTH = 2 * HEAD + 16
 
 
-def attend_body(turns, ids, q0_ref, q1_ref, *refs):
-    chunks, (out0_ref, out1_ref, ka_ref, v_ref) = refs[:NZ], refs[NZ:]
+def attend_body(ids, *refs):
+    queries, chunks, outs = refs[:NX], refs[NX : NX + NZ], refs[NX + NZ : -2]
+    ka_ref, v_ref = refs[-2:]
     z, x = ids[0], ids[1]
     for back, ref in enumerate(chunks):
         place = lax.rem(z + NZ - back, NZ)
@@ -131,7 +130,7 @@
         ka_ref[place, HEAD:DEPTH, :] = ref[0:KG, :]
         v_ref[place] = ref[KG:KVG, :]
     tiles = []
-    for ref in (q0_ref, q1_ref):
+    for ref in queries:
         scaled = ref[...].astype(F32).T * (0.125 * LOG2E)
         hi = scaled.astype(BF16)
         lo = (scaled - hi.astype(F32)).astype(BF16)
@@ -153,11 +152,11 @@
                 scores[i] = jnp.where(col <= row, scores[i], NEG)
         return tuple(weigh(s, values, *c) for s, c in zip(scores, carry))
 
-    start = ((jnp.full((TILE, 1), NEG, F32), jnp.zeros((TILE, HEAD), F32)),) * (2 * TILES)
+    start = ((jnp.full((TILE, 1), NEG, F32), jnp.zeros((TILE, HEAD), F32)),) * (NX * TILES)
     carry = lax.fori_loop(0, z, lambda i, c: update(i, c, tiles, False), start)
     lane = lax.broadcasted_iota(jnp.int32, (ROWS, HEAD), 1)
-    for n, (turn, ref) in enumerate(zip(turns, (out0_ref, out1_ref))):
-        mine = slice(n * TILES, (n + 1) * TILES)
+    for turn, ref in enumerate(outs):
+        mine = slice(turn * TILES, (turn + 1) * TILES)
         if turn == 0:
             last = update(z, carry[mine], tiles[mine], True)
         else:
@@ -428,27 +427,21 @@
     )
     products = lax.all_to_all(products, ("y", "c"), 0, 0, tiled=True)
 
-    def attend(turns):
-        return call(
-            functools.partial(attend_body, turns),
-            (jax.ShapeDtypeStruct((ROWS, 128), BF16),) * 2,
-            ids,
-            (1,),
-            [whole((HEAD, ROWS))] * 2 + [whole((KVG, ROWS))] * NZ,
-            (whole((ROWS, 128)),) * 2,
-            (q_all[turns[0]], q_all[turns[1]], *kvg),
-            scratch=[pltpu.VMEM((NZ, DEPTH, ROWS), BF16), pltpu.VMEM((NZ, HEAD, ROWS), BF16)],
-            flops=10_000_000_000,
-        )
-
-    def send_part(part, d):
-        return lax.ppermute(part, "x", [(i, (i + d) % NX) for i in range(NX)])
-
-    part1, part2 = attend((1, 2))
-    part1, part2 = send_part(part1, 1), send_part(part2, 2)
-
-    part3, part0 = attend((3, 0))
-    part3 = send_part(part3, 3)
+    parts = call(
+        attend_body,
+        (jax.ShapeDtypeStruct((ROWS, 128), BF16),) * NX,
+        ids,
+        (1,),
+        [whole((HEAD, ROWS))] * NX + [whole((KVG, ROWS))] * NZ,
+        (whole((ROWS, 128)),) * NX,
+        (*q_all, *kvg),
+        scratch=[pltpu.VMEM((NZ, DEPTH, ROWS), BF16), pltpu.VMEM((NZ, HEAD, ROWS), BF16)],
+        flops=20_000_000_000,
+    )
+    parts = [parts[0]] + [
+        lax.ppermute(parts[d], "x", [(i, (i + d) % NX) for i in range(NX)])
+        for d in range(1, NX)
+    ]
 
     rows, shared = call(
         sum_body,
@@ -472,7 +465,7 @@
         (1,),
         [whole((1, HEAD))] + [whole((ROWS, 128))] * NX,
         whole((HEAD, ROWS)),
-        (head_gain.reshape(1, HEAD), part0, part1, part2, part3),
+        (head_gain.reshape(1, HEAD), *parts),
     ).T
 
     expert_out = call(

time: 184 us -> 185 us (level)
  the two profiles are of different devices: /device:TPU:454 before, /device:TPU:450 now
where the time goes in v6:
time: 185 us; the launch traced here: 184 us
  starting transfers between devices  64.3 us (35%)
  Pallas kernels  59.4 us (32%)
  waiting for transfers between devices  52 us (28%)
  local copies, waits for them, and re-layouts  6.33 us (3%)
    pallas_call x8, Pallas kernels, call(): pl.pallas_call(body, out_shape=out_shape, grid_spec=pltpu.PrefetchScalarG...  59.4 us
    ppermute x1, waiting for transfers between devices, on_device(): arrived_too = lax.ppermute(arrived, 'y', [(i, i ^ 1) for i in range(NY)])  15.4 us
    ppermute x4, waiting for transfers between devices, on_device(): rising.append(lax.ppermute(rising[-1], 'z', up))  15 us
    all_to_all x1, waiting for transfers between devices, on_device(): arrived = lax.all_to_all(sent, ('z', 'x'), 0, 0, tiled=True)  13 us
    all_to_all x1, starting transfers between devices, on_device(): returned = lax.all_to_all(rows, ('z', 'x'), 0, 0, tiled=True)  12.5 us
    ppermute x3, starting transfers between devices, on_device(): lax.ppermute(mine, 'x', [((i + d) % NX, i) for i in range(NX)])  10.8 us
    ppermute x3, starting transfers between devices, on_device(): lax.ppermute(parts[d], 'x', [(i, (i + d) % NX) for i in range(NX)])  9.18 us
    all_to_all x1, starting transfers between devices, on_device(): products = lax.all_to_all(products, ('y', 'c'), 0, 0, tiled=True)  7.34 us
  transfers between devices with their start and end apart: 18, of which 9 were waited for; matrix products, arithmetic and copies ran while one was open for 1% of the time, Pallas kernels for 24%

profile of v6, /device:TPU:450, one launch (start us, length us, event | category | flops | bytes accessed | tf_op | source)
XLA Modules:
  0.0 183.6 jit_solution(16009015107984840620)
XLA Ops:
  0.6 0.6 pad_add_fusion.ids
  1.3 3.8 %shard_map.176 = (bf16[128,2048]{1,0:T(8,128)(2,1)}, bf16[768,512]{1,0:T(8,128)(2,1)}) custom-call(s32[4]{0:T(128)} %pad_add_fusion.ids, bf16[128,2048]{1,0:T(8,128)(2,1)} %x_ref.1, f32[1,2048]{1,0:T(1,128)} %bitcast.31, s32[4,128]{1,0:T(4,128)} %bitcast.25, s32[768,8]{1,0:T(8,128)} %constant.22.clone.table_ref), custom_call_target="tpu_custom_call" | custom-call | flops 1000000000 | bytes 4194304 | tf_op jit(solution)/shard_map/pallas_call | solution.py:71
  5.0 7.2 %all-to-all-start = ((bf16[32,24,512]{2,1,0:T(8,128)(2,1)}), bf16[32,24,512]{2,1,0:T(8,128)(2,1)S(1)}, u32[]{:S(2)}, u32[]{:S(2)}) async-start(bf16[32,24,512]{2,1,0:T(8,128)(2,1)} %bitcast.16), calls=%async_computation | async-start | bytes 1572864 | tf_op jit(solution)/shard_map/all_to_all | solution.py:353
  12.2 3.6 %shard_map.177 = bf16[480,2048]{1,0:T(8,128)(2,1)} custom-call(s32[4]{0:T(128)} %pad_add_fusion.ids, bf16[4,64,2048]{2,1,0:T(8,128)(2,1)} %gate_ref.3, bf16[4,64,2048]{2,1,0:T(8,128)(2,1)} %up_ref.3, bf16[4,64,2048]{2,1,0:T(8,128)(2,1)} %down_ref.3, bf16[32,2048]{1,0:T(8,128)(2,1)} %sgate_ref.3, bf16[32,2048]{1,0:T(8,128)(2,1)} %sup_ref.3, ...), custom_call_target="tpu_custom_call" | custom-call | flops 1000000000 | bytes 4194304 | tf_op jit(solution)/shard_map/pallas_call | solution.py:71
  15.8 1.9 %collective-permute-start.14 = (bf16[480,2048]{1,0:T(8,128)(2,1)}, bf16[480,2048]{1,0:T(8,128)(2,1)S(1)}, u32[]{:S(2)}, u32[]{:S(2)}) collective-permute-start(bf16[480,2048]{1,0:T(8,128)(2,1)} %shard_map.177), channel_id=1, source_target_pairs={{0,1},{1,0},{2,3},{3,2},{4,5},{5,4},{6,7},{7,6},{8,9},{9,8},{10,11... | collective-permute-start | bytes 5898248 | tf_op jit(solution)/shard_map/ppermute | solution.py:385
  17.7 13.0 %all-to-all-done = bf16[32,24,512]{2,1,0:T(8,128)(2,1)S(1)} async-done(((bf16[32,24,512]{2,1,0:T(8,128)(2,1)}), bf16[32,24,512]{2,1,0:T(8,128)(2,1)S(1)}, u32[]{:S(2)}, u32[]{:S(2)}) %all-to-all-start) | async-done | bytes 786464 | tf_op jit(solution)/shard_map/all_to_all | solution.py:353
  30.7 3.5 %collective-permute-start.13 = (bf16[768,512]{1,0:T(8,128)(2,1)S(1)}, bf16[768,512]{1,0:T(8,128)(2,1)S(1)}, u32[]{:S(2)}, u32[]{:S(2)}) collective-permute-start(bf16[768,512]{1,0:T(8,128)(2,1)S(1)} %bitcast.17), channel_id=1, source_target_pairs={{0,2},{2,0},{4,6},{6,4},{8,10},{10,8},{12,14},{14,12},{1,3},{3,1},... | collective-permute-start | bytes 2359304 | tf_op jit(solution)/shard_map/ppermute | solution.py:354
  34.2 0.0 collective-permute-done.14.got_ref
  34.2 0.0 copy-start.1
  34.2 15.4 %collective-permute-done.13.x_got_ref = bf16[768,512]{1,0:T(8,128)(2,1)S(1)} collective-permute-done((bf16[768,512]{1,0:T(8,128)(2,1)S(1)}, bf16[768,512]{1,0:T(8,128)(2,1)S(1)}, u32[]{:S(2)}, u32[]{:S(2)}) %collective-permute-start.13) | collective-permute-done | bytes 786464 | tf_op jit(solution)/shard_map/ppermute | solution.py:354
  49.6 0.0 copy-done
  49.6 0.0 copy-done.1
  49.6 0.9 copy-done.3
  50.5 8.0 %shard_map.181 = bf16[16,448,128]{2,1,0:T(8,128)(2,1)} custom-call(s32[4]{0:T(128)} %pad_add_fusion.ids, bf16[768,512]{1,0:T(8,128)(2,1)} %bitcast.18, bf16[768,512]{1,0:T(8,128)(2,1)} %copy-done.3, bf16[4,64,2048]{2,1,0:T(8,128)(2,1)} %gate_ref.3, bf16[4,64,2048]{2,1,0:T(8,128)(2,1)} %up_ref.3, bf16[4,64,2048]{2,1,0:T(8,128)(2,1)} %down_ref.3, ...), custom_call_target="tpu_custom_call" | custom-call | flops 1000000000 | bytes 4194304 | tf_op jit(solution)/shard_map/pallas_call | solution.py:71
  58.5 7.3 %all-to-all-start.1 = ((bf16[16,448,128]{2,1,0:T(8,128)(2,1)}), bf16[16,448,128]{2,1,0:T(8,128)(2,1)S(1)}, u32[]{:S(2)}, u32[]{:S(2)}) async-start(bf16[16,448,128]{2,1,0:T(8,128)(2,1)} %shard_map.181), calls=%async_computation.1 | async-start | bytes 3670016 | tf_op jit(solution)/shard_map/all_to_all | solution.py:428
  65.8 2.3 %shard_map.178.refs_4_ = bf16[144,768]{1,0:T(8,128)(2,1)} custom-call(s32[4]{0:T(128)} %pad_add_fusion.ids, bf16[64,768]{1,0:T(8,128)(2,1)} %bitcast.21, bf16[64,768]{1,0:T(8,128)(2,1)} %bitcast.22, f32[1,768]{1,0:T(1,128)} %bitcast.24, bf16[768,512]{1,0:T(8,128)(2,1)} %get-tuple-element.11.after_ref), custom_call_target="tpu_custom_call" | custom-call | bytes 4194304 | tf_op jit(solution)/shard_map/pallas_call | solution.py:71
  68.2 1.3 collective-permute-start.3
  69.5 1.3 collective-permute-start.7
  70.8 9.5 %collective-permute-done.3.refs_5_ = bf16[144,768]{1,0:T(8,128)(2,1)S(1)} collective-permute-done((bf16[144,768]{1,0:T(8,128)(2,1)}, bf16[144,768]{1,0:T(8,128)(2,1)S(1)}, u32[]{:S(2)}, u32[]{:S(2)}) %collective-permute-start.3) | collective-permute-done | bytes 221216 | tf_op jit(solution)/shard_map/ppermute | solution.py:368
  80.2 1.3 collective-permute-start.4
  81.5 1.3 collective-permute-done.7.refs_11_
  82.8 3.3 %collective-permute-start.8 = (bf16[144,768]{1,0:T(8,128)(2,1)S(1)}, bf16[144,768]{1,0:T(8,128)(2,1)S(1)}, u32[]{:S(2)}, u32[]{:S(2)}) collective-permute-start(bf16[144,768]{1,0:T(8,128)(2,1)S(1)} %collective-permute-done.7.refs_11_), channel_id=1, source_target_pairs={{448,384},{0,448},{64,0},{449,385},{1,449},{65,1},{450,386},{2,450... | collective-permute-start | bytes 663560 | tf_op jit(solution)/shard_map/ppermute | solution.py:371
  86.1 3.2 %collective-permute-done.4.refs_6_ = bf16[144,768]{1,0:T(8,128)(2,1)S(1)} collective-permute-done((bf16[144,768]{1,0:T(8,128)(2,1)S(1)}, bf16[144,768]{1,0:T(8,128)(2,1)S(1)}, u32[]{:S(2)}, u32[]{:S(2)}) %collective-permute-start.4) | collective-permute-done | bytes 221216 | tf_op jit(solution)/shard_map/ppermute | solution.py:368
  89.3 1.3 collective-permute-start.5
  90.6 2.2 %collective-permute-done.8.refs_10_ = bf16[144,768]{1,0:T(8,128)(2,1)S(1)} collective-permute-done((bf16[144,768]{1,0:T(8,128)(2,1)S(1)}, bf16[144,768]{1,0:T(8,128)(2,1)S(1)}, u32[]{:S(2)}, u32[]{:S(2)}) %collective-permute-start.8) | collective-permute-done | bytes 221216 | tf_op jit(solution)/shard_map/ppermute | solution.py:371
  92.8 2.3 %collective-permute-start.9 = (bf16[144,768]{1,0:T(8,128)(2,1)S(1)}, bf16[144,768]{1,0:T(8,128)(2,1)S(1)}, u32[]{:S(2)}, u32[]{:S(2)}) collective-permute-start(bf16[144,768]{1,0:T(8,128)(2,1)S(1)} %collective-permute-done.8.refs_10_), channel_id=1, source_target_pairs={{384,320},{448,384},{0,448},{385,321},{449,385},{1,449},{386,322},... | collective-permute-start | bytes 663560 | tf_op jit(solution)/shard_map/ppermute | solution.py:371
  95.1 2.3 %collective-permute-done.5.refs_7_ = bf16[144,768]{1,0:T(8,128)(2,1)S(1)} collective-permute-done((bf16[144,768]{1,0:T(8,128)(2,1)S(1)}, bf16[144,768]{1,0:T(8,128)(2,1)S(1)}, u32[]{:S(2)}, u32[]{:S(2)}) %collective-permute-start.5) | collective-permute-done | bytes 221216 | tf_op jit(solution)/shard_map/ppermute | solution.py:368
  97.5 1.3 collective-permute-start.6
  98.8 0.0 copy-done.17
  98.8 3.0 %collective-permute-start = (bf16[64,768]{1,0:T(8,128)(2,1)S(1)}, bf16[64,768]{1,0:T(8,128)(2,1)}, u32[]{:S(2)}, u32[]{:S(2)}) collective-permute-start(bf16[64,768]{1,0:T(8,128)(2,1)S(1)} %bitcast.28), channel_id=1, source_target_pairs={{16,0},{32,16},{48,32},{0,48},{17,1},{33,17},{49,33},{1,49},{18,2}... | collective-permute-start | bytes 294920 | tf_op jit(solution)/shard_map/ppermute | solution.py:390
  101.8 3.8 %collective-permute-start.1 = (bf16[64,768]{1,0:T(8,128)(2,1)S(1)}, bf16[64,768]{1,0:T(8,128)(2,1)}, u32[]{:S(2)}, u32[]{:S(2)}) collective-permute-start(bf16[64,768]{1,0:T(8,128)(2,1)S(1)} %bitcast.29), channel_id=1, source_target_pairs={{32,0},{48,16},{0,32},{16,48},{33,1},{49,17},{1,33},{17,49},{34,2}... | collective-permute-start | bytes 294920 | tf_op jit(solution)/shard_map/ppermute | solution.py:390
  105.6 4.0 %collective-permute-start.2 = (bf16[64,768]{1,0:T(8,128)(2,1)S(1)}, bf16[64,768]{1,0:T(8,128)(2,1)}, u32[]{:S(2)}, u32[]{:S(2)}) collective-permute-start(bf16[64,768]{1,0:T(8,128)(2,1)S(1)} %bitcast.30), channel_id=1, source_target_pairs={{48,0},{0,16},{16,32},{32,48},{49,1},{1,17},{17,33},{33,49},{50,2}... | collective-permute-start | bytes 294920 | tf_op jit(solution)/shard_map/ppermute | solution.py:390
  109.6 0.0 all-to-all-done.1.part_ref
  109.6 0.0 copy-start.2
  109.6 1.2 copy-done.2
  110.8 3.6 %shard_map.182 = (bf16[768,128]{1,0:T(8,128)(2,1)}, f32[128,128]{1,0:T(8,128)}) custom-call(s32[4]{0:T(128)} %pad_add_fusion.ids, bf16[16,448,128]{2,1,0:T(8,128)(2,1)} %copy-done.2, s32[768,8]{1,0:T(8,128)} %constant.22.clone.table_ref), custom_call_target="tpu_custom_call" | custom-call | flops 1000000000 | bytes 4194304 | tf_op jit(solution)/shard_map/pallas_call | solution.py:71
  114.5 12.5 %all-to-all-start.2 = ((bf16[32,24,128]{2,1,0:T(8,128)(2,1)}), bf16[32,24,128]{2,1,0:T(8,128)(2,1)S(1)}, u32[]{:S(2)}, u32[]{:S(2)}) async-start(bf16[32,24,128]{2,1,0:T(8,128)(2,1)} %bitcast.20), calls=%async_computation.2 | async-start | bytes 393216 | tf_op jit(solution)/shard_map/all_to_all | solution.py:459
  127.0 0.0 copy-start.8
  127.0 0.0 copy-start.9
  127.0 0.0 collective-permute-done.refs_1_
  127.0 0.0 collective-permute-done.1.refs_2_
  127.0 0.0 collective-permute-done.2.refs_3_
  127.0 0.0 collective-permute-done.9.refs_9_
  127.0 0.0 copy-start.15
  127.0 0.0 collective-permute-done.6.refs_8_
  127.1 0.0 copy-done.10
  127.1 0.0 copy-done.11
  127.1 0.6 copy-done.15
  127.7 0.7 copy-done.16
  128.4 31.4 %shard_map.179 = (bf16[768,128]{1,0:T(8,128)(2,1)}, bf16[768,128]{1,0:T(8,128)(2,1)}, bf16[768,128]{1,0:T(8,128)(2,1)}, bf16[768,128]{1,0:T(8,128)(2,1)}) custom-call(s32[4]{0:T(128)} %pad_add_fusion.ids, bf16[64,768]{1,0:T(8,128)(2,1)} %bitcast.27, bf16[64,768]{1,0:T(8,128)(2,1)} %collective-permute-done.refs_1_, ...), custom_call_target="tpu_custom_call" | custom-call | flops 20000000000 | bytes 4194304 | tf_op jit(solution)/shard_map/pallas_call | solution.py:71
  159.8 2.5 %collective-permute-start.10 = (bf16[768,128]{1,0:T(8,128)(2,1)}, bf16[768,128]{1,0:T(8,128)(2,1)S(1)}, u32[]{:S(2)}, u32[]{:S(2)}) collective-permute-start(bf16[768,128]{1,0:T(8,128)(2,1)} %get-tuple-element.14), channel_id=1, source_target_pairs={{0,16},{16,32},{32,48},{48,0},{1,17},{17,33},{33,49},{49,1},{2,18}... | collective-permute-start | bytes 589832 | tf_op jit(solution)/shard_map/ppermute | solution.py:442
  162.3 4.7 %collective-permute-start.11 = (bf16[768,128]{1,0:T(8,128)(2,1)}, bf16[768,128]{1,0:T(8,128)(2,1)S(1)}, u32[]{:S(2)}, u32[]{:S(2)}) collective-permute-start(bf16[768,128]{1,0:T(8,128)(2,1)} %get-tuple-element.15), channel_id=1, source_target_pairs={{0,32},{16,48},{32,0},{48,16},{1,33},{17,49},{33,1},{49,17},{2,34}... | collective-permute-start | bytes 589832 | tf_op jit(solution)/shard_map/ppermute | solution.py:442
  167.1 1.9 %collective-permute-start.12 = (bf16[768,128]{1,0:T(8,128)(2,1)}, bf16[768,128]{1,0:T(8,128)(2,1)S(1)}, u32[]{:S(2)}, u32[]{:S(2)}) collective-permute-start(bf16[768,128]{1,0:T(8,128)(2,1)} %get-tuple-element.16), channel_id=1, source_target_pairs={{0,48},{16,0},{32,16},{48,32},{1,49},{17,1},{33,17},{49,33},{2,50}... | collective-permute-start | bytes 589832 | tf_op jit(solution)/shard_map/ppermute | solution.py:442
  169.0 0.0 copy-done.8
  169.0 0.7 copy.19.routes_ref
  169.7 0.7 copy.20.weight_ref
  170.5 0.0 collective-permute-done.10.refs_1_
  170.5 2.6 %collective-permute-done.11.refs_2_ = bf16[768,128]{1,0:T(8,128)(2,1)S(1)} collective-permute-done((bf16[768,128]{1,0:T(8,128)(2,1)}, bf16[768,128]{1,0:T(8,128)(2,1)S(1)}, u32[]{:S(2)}, u32[]{:S(2)}) %collective-permute-start.11) | collective-permute-done | bytes 196640 | tf_op jit(solution)/shard_map/ppermute | solution.py:442
  173.1 2.5 %collective-permute-done.12.refs_3_ = bf16[768,128]{1,0:T(8,128)(2,1)S(1)} collective-permute-done((bf16[768,128]{1,0:T(8,128)(2,1)}, bf16[768,128]{1,0:T(8,128)(2,1)S(1)}, u32[]{:S(2)}, u32[]{:S(2)}) %collective-permute-start.12) | collective-permute-done | bytes 196640 | tf_op jit(solution)/shard_map/ppermute | solution.py:442
  175.6 0.7 copy-done.7
  176.3 3.8 %shard_map.180 = bf16[64,768]{1,0:T(8,128)(2,1)} custom-call(s32[4]{0:T(128)} %pad_add_fusion.ids, f32[1,64]{1,0:T(1,128)} %bitcast.26, bf16[768,128]{1,0:T(8,128)(2,1)} %get-tuple-element.13.refs_0_, bf16[768,128]{1,0:T(8,128)(2,1)} %copy-done.5, bf16[768,128]{1,0:T(8,128)(2,1)} %copy-done.6, bf16[768,128]{1,0:T(8,128)(2,1)} %copy-done.7), custom_call_target="tpu_custom_call" | custom-call | bytes 4194304 | tf_op jit(solution)/shard_map/pallas_call | solution.py:71
  180.0 0.0 all-to-all-done.2
  180.0 0.7 copy-done.4
  180.7 2.9 %shard_map.183 = bf16[128,128]{1,0:T(8,128)(2,1)} custom-call(s32[4]{0:T(128)} %pad_add_fusion.ids, bf16[768,128]{1,0:T(8,128)(2,1)} %bitcast.19, s32[128,4]{1,0:T(8,128)} %copy.19.routes_ref, f32[128,4]{1,0:T(8,128)} %copy.20.weight_ref, s32[8,768]{1,0:T(8,128)} %constant.28.table_ref, f32[128,128]{1,0:T(8,128)} %get-tuple-element.19.shared_ref), custom_call_target="tpu_custom_call" | custom-call | flops 1000000000 | bytes 4194304 | tf_op jit(solution)/shard_map/pallas_call | solution.py:71
  (19 shorter events, 0.0 us)
Async XLA Ops:
  5.0 25.7 %all-to-all-start = ((bf16[32,24,512]{2,1,0:T(8,128)(2,1)}), bf16[32,24,512]{2,1,0:T(8,128)(2,1)S(1)}, u32[]{:S(2)}, u32[]{:S(2)}) async-start(bf16[32,24,512]{2,1,0:T(8,128)(2,1)} %bitcast.16), calls=%async_computation | async-start | bytes 1572864 | tf_op jit(solution)/shard_map/all_to_all | solution.py:353
  15.8 18.4 %collective-permute-start.14 = (bf16[480,2048]{1,0:T(8,128)(2,1)}, bf16[480,2048]{1,0:T(8,128)(2,1)S(1)}, u32[]{:S(2)}, u32[]{:S(2)}) collective-permute-start(bf16[480,2048]{1,0:T(8,128)(2,1)} %shard_map.177), channel_id=1, source_target_pairs={{0,1},{1,0},{2,3},{3,2},{4,5},{5,4},{6,7},{7,6},{8,9},{9,8},{10,11... | collective-permute-start | bytes 5898248 | tf_op jit(solution)/shard_map/ppermute | solution.py:385
  30.7 18.9 %copy-start = (bf16[32,24,512]{2,1,0:T(8,128)(2,1)}, bf16[32,24,512]{2,1,0:T(8,128)(2,1)S(1)}, u32[]{:S(2)}) copy-start(bf16[32,24,512]{2,1,0:T(8,128)(2,1)S(1)} %all-to-all-done) | copy-start | bytes 2359300
  30.7 18.9 %collective-permute-start.13 = (bf16[768,512]{1,0:T(8,128)(2,1)S(1)}, bf16[768,512]{1,0:T(8,128)(2,1)S(1)}, u32[]{:S(2)}, u32[]{:S(2)}) collective-permute-start(bf16[768,512]{1,0:T(8,128)(2,1)S(1)} %bitcast.17), channel_id=1, source_target_pairs={{0,2},{2,0},{4,6},{6,4},{8,10},{10,8},{12,14},{14,12},{1,3},{3,1},... | collective-permute-start | bytes 2359304 | tf_op jit(solution)/shard_map/ppermute | solution.py:354
  34.2 15.4 %copy-start.1 = (bf16[480,2048]{1,0:T(8,128)(2,1)}, bf16[480,2048]{1,0:T(8,128)(2,1)S(1)}, u32[]{:S(2)}) copy-start(bf16[480,2048]{1,0:T(8,128)(2,1)S(1)} %collective-permute-done.14.got_ref) | copy-start | bytes 5898244
  49.6 0.9 copy-start.3
  58.5 40.3 %copy-start.17 = (bf16[768,64]{0,1:T(8,128)(2,1)S(1)}, bf16[768,64]{0,1:T(8,128)(2,1)}, u32[]{:S(2)}) copy-start(bf16[768,64]{0,1:T(8,128)(2,1)} %param.17) | copy-start | bytes 294916
  58.5 51.1 %all-to-all-start.1 = ((bf16[16,448,128]{2,1,0:T(8,128)(2,1)}), bf16[16,448,128]{2,1,0:T(8,128)(2,1)S(1)}, u32[]{:S(2)}, u32[]{:S(2)}) async-start(bf16[16,448,128]{2,1,0:T(8,128)(2,1)} %shard_map.181), calls=%async_computation.1 | async-start | bytes 3670016 | tf_op jit(solution)/shard_map/all_to_all | solution.py:428
  68.2 12.0 %collective-permute-start.3 = (bf16[144,768]{1,0:T(8,128)(2,1)}, bf16[144,768]{1,0:T(8,128)(2,1)S(1)}, u32[]{:S(2)}, u32[]{:S(2)}) collective-permute-start(bf16[144,768]{1,0:T(8,128)(2,1)} %shard_map.178.refs_4_), channel_id=1, source_target_pairs={{0,64},{64,128},{128,192},{192,256},{256,320},{320,384},{384,448},... | collective-permute-start | bytes 663560 | tf_op jit(solution)/shard_map/ppermute | solution.py:368
  69.5 13.4 %collective-permute-start.7 = (bf16[144,768]{1,0:T(8,128)(2,1)}, bf16[144,768]{1,0:T(8,128)(2,1)S(1)}, u32[]{:S(2)}, u32[]{:S(2)}) collective-permute-start(bf16[144,768]{1,0:T(8,128)(2,1)} %shard_map.178.refs_4_), channel_id=1, source_target_pairs={{0,448},{64,0},{128,64},{1,449},{65,1},{129,65},{2,450},{66,2},{13... | collective-permute-start | bytes 663560 | tf_op jit(solution)/shard_map/ppermute | solution.py:371
  80.2 46.8 %copy-start.10 = (bf16[144,768]{1,0:T(8,128)(2,1)}, bf16[144,768]{1,0:T(8,128)(2,1)S(1)}, u32[]{:S(2)}) copy-start(bf16[144,768]{1,0:T(8,128)(2,1)S(1)} %collective-permute-done.3.refs_5_) | copy-start | bytes 663556
  80.2 9.0 %collective-permute-start.4 = (bf16[144,768]{1,0:T(8,128)(2,1)S(1)}, bf16[144,768]{1,0:T(8,128)(2,1)S(1)}, u32[]{:S(2)}, u32[]{:S(2)}) collective-permute-start(bf16[144,768]{1,0:T(8,128)(2,1)S(1)} %collective-permute-done.3.refs_5_), channel_id=1, source_target_pairs={{64,128},{128,192},{192,256},{256,320},{320,384},{384,448},{65,129... | collective-permute-start | bytes 663560 | tf_op jit(solution)/shard_map/ppermute | solution.py:368
  82.8 44.2 %copy-start.11 = (bf16[144,768]{1,0:T(8,128)(2,1)}, bf16[144,768]{1,0:T(8,128)(2,1)S(1)}, u32[]{:S(2)}) copy-start(bf16[144,768]{1,0:T(8,128)(2,1)S(1)} %collective-permute-done.7.refs_11_) | copy-start | bytes 663556
  82.8 10.0 %collective-permute-start.8 = (bf16[144,768]{1,0:T(8,128)(2,1)S(1)}, bf16[144,768]{1,0:T(8,128)(2,1)S(1)}, u32[]{:S(2)}, u32[]{:S(2)}) collective-permute-start(bf16[144,768]{1,0:T(8,128)(2,1)S(1)} %collective-permute-done.7.refs_11_), channel_id=1, source_target_pairs={{448,384},{0,448},{64,0},{449,385},{1,449},{65,1},{450,386},{2,450... | collective-permute-start | bytes 663560 | tf_op jit(solution)/shard_map/ppermute | solution.py:371
  89.3 37.8 %copy-start.12 = (bf16[144,768]{1,0:T(8,128)(2,1)}, bf16[144,768]{1,0:T(8,128)(2,1)S(1)}, u32[]{:S(2)}) copy-start(bf16[144,768]{1,0:T(8,128)(2,1)S(1)} %collective-permute-done.4.refs_6_) | copy-start | bytes 663556
  89.3 8.2 %collective-permute-start.5 = (bf16[144,768]{1,0:T(8,128)(2,1)S(1)}, bf16[144,768]{1,0:T(8,128)(2,1)S(1)}, u32[]{:S(2)}, u32[]{:S(2)}) collective-permute-start(bf16[144,768]{1,0:T(8,128)(2,1)S(1)} %collective-permute-done.4.refs_6_), channel_id=1, source_target_pairs={{128,192},{192,256},{256,320},{320,384},{384,448},{129,193},{193,2... | collective-permute-start | bytes 663560 | tf_op jit(solution)/shard_map/ppermute | solution.py:368
  92.8 34.3 %copy-start.13 = (bf16[144,768]{1,0:T(8,128)(2,1)}, bf16[144,768]{1,0:T(8,128)(2,1)S(1)}, u32[]{:S(2)}) copy-start(bf16[144,768]{1,0:T(8,128)(2,1)S(1)} %collective-permute-done.8.refs_10_) | copy-start | bytes 663556
  92.8 34.2 %collective-permute-start.9 = (bf16[144,768]{1,0:T(8,128)(2,1)S(1)}, bf16[144,768]{1,0:T(8,128)(2,1)S(1)}, u32[]{:S(2)}, u32[]{:S(2)}) collective-permute-start(bf16[144,768]{1,0:T(8,128)(2,1)S(1)} %collective-permute-done.8.refs_10_), channel_id=1, source_target_pairs={{384,320},{448,384},{0,448},{385,321},{449,385},{1,449},{386,322},... | collective-permute-start | bytes 663560 | tf_op jit(solution)/shard_map/ppermute | solution.py:371
  97.5 29.6 %copy-start.14 = (bf16[144,768]{1,0:T(8,128)(2,1)}, bf16[144,768]{1,0:T(8,128)(2,1)S(1)}, u32[]{:S(2)}) copy-start(bf16[144,768]{1,0:T(8,128)(2,1)S(1)} %collective-permute-done.5.refs_7_) | copy-start | bytes 663556
  97.5 29.6 %collective-permute-start.6 = (bf16[144,768]{1,0:T(8,128)(2,1)S(1)}, bf16[144,768]{1,0:T(8,128)(2,1)S(1)}, u32[]{:S(2)}, u32[]{:S(2)}) collective-permute-start(bf16[144,768]{1,0:T(8,128)(2,1)S(1)} %collective-permute-done.5.refs_7_), channel_id=1, source_target_pairs={{192,256},{256,320},{320,384},{384,448},{193,257},{257,321},{321,3... | collective-permute-start | bytes 663560 | tf_op jit(solution)/shard_map/ppermute | solution.py:368
  98.8 28.2 %collective-permute-start = (bf16[64,768]{1,0:T(8,128)(2,1)S(1)}, bf16[64,768]{1,0:T(8,128)(2,1)}, u32[]{:S(2)}, u32[]{:S(2)}) collective-permute-start(bf16[64,768]{1,0:T(8,128)(2,1)S(1)} %bitcast.28), channel_id=1, source_target_pairs={{16,0},{32,16},{48,32},{0,48},{17,1},{33,17},{49,33},{1,49},{18,2}... | collective-permute-start | bytes 294920 | tf_op jit(solution)/shard_map/ppermute | solution.py:390
  101.8 25.2 %collective-permute-start.1 = (bf16[64,768]{1,0:T(8,128)(2,1)S(1)}, bf16[64,768]{1,0:T(8,128)(2,1)}, u32[]{:S(2)}, u32[]{:S(2)}) collective-permute-start(bf16[64,768]{1,0:T(8,128)(2,1)S(1)} %bitcast.29), channel_id=1, source_target_pairs={{32,0},{48,16},{0,32},{16,48},{33,1},{49,17},{1,33},{17,49},{34,2}... | collective-permute-start | bytes 294920 | tf_op jit(solution)/shard_map/ppermute | solution.py:390
  105.6 21.4 %collective-permute-start.2 = (bf16[64,768]{1,0:T(8,128)(2,1)S(1)}, bf16[64,768]{1,0:T(8,128)(2,1)}, u32[]{:S(2)}, u32[]{:S(2)}) collective-permute-start(bf16[64,768]{1,0:T(8,128)(2,1)S(1)} %bitcast.30), channel_id=1, source_target_pairs={{48,0},{0,16},{16,32},{32,48},{49,1},{1,17},{17,33},{33,49},{50,2}... | collective-permute-start | bytes 294920 | tf_op jit(solution)/shard_map/ppermute | solution.py:390
  109.6 1.3 copy-start.2
  114.5 65.5 %all-to-all-start.2 = ((bf16[32,24,128]{2,1,0:T(8,128)(2,1)}), bf16[32,24,128]{2,1,0:T(8,128)(2,1)S(1)}, u32[]{:S(2)}, u32[]{:S(2)}) async-start(bf16[32,24,128]{2,1,0:T(8,128)(2,1)} %bitcast.20), calls=%async_computation.2 | async-start | bytes 393216 | tf_op jit(solution)/shard_map/all_to_all | solution.py:459
  127.0 42.0 %copy-start.8 = (s32[128,4]{0,1:T(4,128)S(1)}, s32[128,4]{0,1:T(4,128)}, u32[]{:S(2)}) copy-start(s32[128,4]{0,1:T(4,128)} %param.24) | copy-start | bytes 6148
  127.0 42.8 %copy-start.9 = (f32[128,4]{0,1:T(4,128)S(1)}, f32[128,4]{0,1:T(4,128)}, u32[]{:S(2)}) copy-start(f32[128,4]{0,1:T(4,128)} %param.25) | copy-start | bytes 6148
  127.0 0.7 copy-start.15
  127.7 0.7 copy-start.16
  159.8 10.7 %collective-permute-start.10 = (bf16[768,128]{1,0:T(8,128)(2,1)}, bf16[768,128]{1,0:T(8,128)(2,1)S(1)}, u32[]{:S(2)}, u32[]{:S(2)}) collective-permute-start(bf16[768,128]{1,0:T(8,128)(2,1)} %get-tuple-element.14), channel_id=1, source_target_pairs={{0,16},{16,32},{32,48},{48,0},{1,17},{17,33},{33,49},{49,1},{2,18}... | collective-permute-start | bytes 589832 | tf_op jit(solution)/shard_map/ppermute | solution.py:442
  162.3 10.7 %collective-permute-start.11 = (bf16[768,128]{1,0:T(8,128)(2,1)}, bf16[768,128]{1,0:T(8,128)(2,1)S(1)}, u32[]{:S(2)}, u32[]{:S(2)}) collective-permute-start(bf16[768,128]{1,0:T(8,128)(2,1)} %get-tuple-element.15), channel_id=1, source_target_pairs={{0,32},{16,48},{32,0},{48,16},{1,33},{17,49},{33,1},{49,17},{2,34}... | collective-permute-start | bytes 589832 | tf_op jit(solution)/shard_map/ppermute | solution.py:442
  167.1 8.5 %collective-permute-start.12 = (bf16[768,128]{1,0:T(8,128)(2,1)}, bf16[768,128]{1,0:T(8,128)(2,1)S(1)}, u32[]{:S(2)}, u32[]{:S(2)}) collective-permute-start(bf16[768,128]{1,0:T(8,128)(2,1)} %get-tuple-element.16), channel_id=1, source_target_pairs={{0,48},{16,0},{32,16},{48,32},{1,49},{17,1},{33,17},{49,33},{2,50}... | collective-permute-start | bytes 589832 | tf_op jit(solution)/shard_map/ppermute | solution.py:442
  170.5 5.1 %copy-start.5 = (bf16[768,128]{1,0:T(8,128)(2,1)}, bf16[768,128]{1,0:T(8,128)(2,1)S(1)}, u32[]{:S(2)}) copy-start(bf16[768,128]{1,0:T(8,128)(2,1)S(1)} %collective-permute-done.10.refs_1_) | copy-start | bytes 589828
  173.1 2.5 %copy-start.6 = (bf16[768,128]{1,0:T(8,128)(2,1)}, bf16[768,128]{1,0:T(8,128)(2,1)S(1)}, u32[]{:S(2)}) copy-start(bf16[768,128]{1,0:T(8,128)(2,1)S(1)} %collective-permute-done.11.refs_2_) | copy-start | bytes 589828
  175.6 0.7 copy-start.7
  180.0 0.7 copy-start.4

commit v7 on v6

--- a/solution.py
+++ b/solution.py
@@ -226,7 +226,8 @@
 def experts_body(
     ids,
     x_ref,
-    x_got_ref,
+    x_below_ref,
+    x_above_ref,
     gate_ref,
     up_ref,
     down_ref,
@@ -246,11 +247,13 @@
     @pl.when(even)
     def _():
         low_ref[...] = x_ref[...]
-        high_ref[...] = x_got_ref[...]
+        high_ref[0:SLOTS, :] = x_below_ref[...]
+        high_ref[SLOTS:, :] = x_above_ref[...]
 
     @pl.when(jnp.logical_not(even))
     def _():
-        low_ref[...] = x_got_ref[...]
+        low_ref[0:SLOTS, :] = x_below_ref[...]
+        low_ref[SLOTS:, :] = x_above_ref[...]
         high_ref[...] = x_ref[...]
 
     lane = lax.broadcasted_iota(jnp.int32, (SLOTS, 2 * SLOTS), 1)
@@ -351,7 +354,10 @@
         flops=1_000_000_000,
     )
     arrived = lax.all_to_all(sent, ("z", "x"), 0, 0, tiled=True)
-    arrived_too = lax.ppermute(arrived, "y", [(i, i ^ 1) for i in range(NY)])
+    arrived_too = [
+        lax.ppermute(arrived[:SLOTS], "y", [(i, (i + 1) % NY) for i in range(NY)]),
+        lax.ppermute(arrived[SLOTS:], "y", [(i, (i - 1) % NY) for i in range(NY)]),
+    ]
 
     packed = call(
         pack_body,
@@ -397,7 +403,8 @@
         (1,),
         [
             whole((2 * SLOTS, D // 4)),
-            whole((2 * SLOTS, D // 4)),
+            whole((SLOTS, D // 4)),
+            whole((SLOTS, D // 4)),
             mine,
             mine,
             mine,
@@ -411,7 +418,7 @@
         whole((NY * NC, SLOTS + 64, 128)),
         (
             arrived,
-            arrived_too,
+            *arrived_too,
             expert_gate,
             expert_up,
             expert_down,

time: 185 us -> 180 us (0.973)
  waiting for transfers between devices: 52 us -> 43 us
  starting transfers between devices: 64.3 us -> 68.3 us
    ppermute x1 -> x2, waiting for transfers between devices: 15.4 us -> 6.42 us  [the longest x1 4.94 us: on_device(): lax.ppermute(arrived[:SLOTS], 'y', [(i, (i + 1) % NY) for i in range(NY)])]
    ppermute x1 -> x2, starting transfers between devices: 3.48 us -> 7.3 us  [the longest x1 3.81 us: on_device(): lax.ppermute(arrived[SLOTS:], 'y', [(i, (i - 1) % NY) for i in range(NY)])]
    unnamed x38 -> x40, local copies, waits for them, and re-layouts: 6.33 us -> 6.87 us
  transfers between devices with their start and end apart: 18 -> 19, of which waited for: 9 -> 10; matrix products, arithmetic and copies ran while one was open for 1% -> 1% of each run, Pallas kernels for 24% -> 25%
where the time goes in v7:
time: 180 us; the launch traced here: 179 us
  starting transfers between devices  68.3 us (38%)
  Pallas kernels  59.4 us (33%)
  waiting for transfers between devices  43 us (24%)
  local copies, waits for them, and re-layouts  6.92 us (4%)
    pallas_call x8, Pallas kernels, call(): pl.pallas_call(body, out_shape=out_shape, grid_spec=pltpu.PrefetchScalarG...  59.4 us
    ppermute x4, waiting for transfers between devices, on_device(): rising.append(lax.ppermute(rising[-1], 'z', up))  15 us
    all_to_all x1, waiting for transfers between devices, on_device(): arrived = lax.all_to_all(sent, ('z', 'x'), 0, 0, tiled=True)  13 us
    all_to_all x1, starting transfers between devices, on_device(): returned = lax.all_to_all(rows, ('z', 'x'), 0, 0, tiled=True)  12.5 us
    ppermute x3, starting transfers between devices, on_device(): lax.ppermute(mine, 'x', [((i + d) % NX, i) for i in range(NX)])  10.8 us
    ppermute x3, starting transfers between devices, on_device(): lax.ppermute(parts[d], 'x', [(i, (i + d) % NX) for i in range(NX)])  9.17 us
    all_to_all x1, starting transfers between devices, on_device(): products = lax.all_to_all(products, ('y', 'c'), 0, 0, tiled=True)  7.52 us
    all_to_all x1, starting transfers between devices, on_device(): arrived = lax.all_to_all(sent, ('z', 'x'), 0, 0, tiled=True)  7.18 us
  transfers between devices with their start and end apart: 19, of which 10 were waited for; matrix products, arithmetic and copies ran while one was open for 1% of the time, Pallas kernels for 25%

profile of v7, /device:TPU:450, one launch (start us, length us, event | category | flops | bytes accessed | tf_op | source)
XLA Modules:
  0.0 179.2 jit_solution(3598678307741596378)
XLA Ops:
  0.6 0.6 pad_add_fusion.ids
  1.2 3.8 %shard_map.176 = (bf16[128,2048]{1,0:T(8,128)(2,1)}, bf16[768,512]{1,0:T(8,128)(2,1)}) custom-call(s32[4]{0:T(128)} %pad_add_fusion.ids, bf16[128,2048]{1,0:T(8,128)(2,1)} %x_ref.1, f32[1,2048]{1,0:T(1,128)} %bitcast.34, s32[4,128]{1,0:T(4,128)} %bitcast.28, s32[768,8]{1,0:T(8,128)} %constant.22.clone.table_ref), custom_call_target="tpu_custom_call" | custom-call | flops 1000000000 | bytes 4194304 | tf_op jit(solution)/shard_map/pallas_call | solution.py:71
  5.0 7.2 %all-to-all-start = ((bf16[32,24,512]{2,1,0:T(8,128)(2,1)}), bf16[32,24,512]{2,1,0:T(8,128)(2,1)S(1)}, u32[]{:S(2)}, u32[]{:S(2)}) async-start(bf16[32,24,512]{2,1,0:T(8,128)(2,1)} %bitcast.18), calls=%async_computation | async-start | bytes 1572864 | tf_op jit(solution)/shard_map/all_to_all | solution.py:356
  12.2 3.6 %shard_map.177 = bf16[480,2048]{1,0:T(8,128)(2,1)} custom-call(s32[4]{0:T(128)} %pad_add_fusion.ids, bf16[4,64,2048]{2,1,0:T(8,128)(2,1)} %gate_ref.3, bf16[4,64,2048]{2,1,0:T(8,128)(2,1)} %up_ref.3, bf16[4,64,2048]{2,1,0:T(8,128)(2,1)} %down_ref.3, bf16[32,2048]{1,0:T(8,128)(2,1)} %sgate_ref.3, bf16[32,2048]{1,0:T(8,128)(2,1)} %sup_ref.3, ...), custom_call_target="tpu_custom_call" | custom-call | flops 1000000000 | bytes 4194304 | tf_op jit(solution)/shard_map/pallas_call | solution.py:71
  15.8 1.9 %collective-permute-start.15 = (bf16[480,2048]{1,0:T(8,128)(2,1)}, bf16[480,2048]{1,0:T(8,128)(2,1)S(1)}, u32[]{:S(2)}, u32[]{:S(2)}) collective-permute-start(bf16[480,2048]{1,0:T(8,128)(2,1)} %shard_map.177), channel_id=1, source_target_pairs={{0,1},{1,0},{2,3},{3,2},{4,5},{5,4},{6,7},{7,6},{8,9},{9,8},{10,11... | collective-permute-start | bytes 5898248 | tf_op jit(solution)/shard_map/ppermute | solution.py:391
  17.7 13.0 %all-to-all-done = bf16[32,24,512]{2,1,0:T(8,128)(2,1)S(1)} async-done(((bf16[32,24,512]{2,1,0:T(8,128)(2,1)}), bf16[32,24,512]{2,1,0:T(8,128)(2,1)S(1)}, u32[]{:S(2)}, u32[]{:S(2)}) %all-to-all-start) | async-done | bytes 786464 | tf_op jit(solution)/shard_map/all_to_all | solution.py:356
  30.7 0.1 fusion
  30.7 3.5 %collective-permute-start.13 = (bf16[384,512]{1,0:T(8,128)(2,1)S(1)}, bf16[384,512]{1,0:T(8,128)(2,1)S(1)}, u32[]{:S(2)}, u32[]{:S(2)}) collective-permute-start(bf16[384,512]{1,0:T(8,128)(2,1)S(1)} %bitcast.21), channel_id=1, source_target_pairs={{0,2},{2,4},{4,6},{6,8},{8,10},{10,12},{12,14},{14,0},{1,3},{3,5},... | collective-permute-start | bytes 1179656 | tf_op jit(solution)/shard_map/ppermute | solution.py:358
  34.2 3.8 %collective-permute-start.14 = (bf16[384,512]{1,0:T(8,128)(2,1)S(1)}, bf16[384,512]{1,0:T(8,128)(2,1)S(1)}, u32[]{:S(2)}, u32[]{:S(2)}) collective-permute-start(bf16[384,512]{1,0:T(8,128)(2,1)S(1)} %bitcast.20), channel_id=1, source_target_pairs={{0,14},{2,0},{4,2},{6,4},{8,6},{10,8},{12,10},{14,12},{1,15},{3,1}... | collective-permute-start | bytes 1179656 | tf_op jit(solution)/shard_map/ppermute | solution.py:359
  38.1 4.9 %collective-permute-done.13.x_below_ref = bf16[384,512]{1,0:T(8,128)(2,1)S(1)} collective-permute-done((bf16[384,512]{1,0:T(8,128)(2,1)S(1)}, bf16[384,512]{1,0:T(8,128)(2,1)S(1)}, u32[]{:S(2)}, u32[]{:S(2)}) %collective-permute-start.13) | collective-permute-done | bytes 393248 | tf_op jit(solution)/shard_map/ppermute | solution.py:358
  43.0 1.5 collective-permute-done.14.x_above_ref
  44.5 0.0 collective-permute-done.15.got_ref
  44.5 0.0 copy-done
  44.5 0.0 copy-done.3
  44.5 0.7 copy-done.4
  45.2 0.7 copy-done.1
  45.9 8.0 %shard_map.181 = bf16[16,448,128]{2,1,0:T(8,128)(2,1)} custom-call(s32[4]{0:T(128)} %pad_add_fusion.ids, bf16[768,512]{1,0:T(8,128)(2,1)} %bitcast.19, bf16[384,512]{1,0:T(8,128)(2,1)} %copy-done.3, bf16[384,512]{1,0:T(8,128)(2,1)} %copy-done.4, bf16[4,64,2048]{2,1,0:T(8,128)(2,1)} %gate_ref.3, bf16[4,64,2048]{2,1,0:T(8,128)(2,1)} %up_ref.3, ...), custom_call_target="tpu_custom_call" | custom-call | flops 1000000000 | bytes 4194304 | tf_op jit(solution)/shard_map/pallas_call | solution.py:71
  53.9 7.5 %all-to-all-start.1 = ((bf16[16,448,128]{2,1,0:T(8,128)(2,1)}), bf16[16,448,128]{2,1,0:T(8,128)(2,1)S(1)}, u32[]{:S(2)}, u32[]{:S(2)}) async-start(bf16[16,448,128]{2,1,0:T(8,128)(2,1)} %shard_map.181), calls=%async_computation.1 | async-start | bytes 3670016 | tf_op jit(solution)/shard_map/all_to_all | solution.py:435
  61.4 2.3 %shard_map.178.refs_4_ = bf16[144,768]{1,0:T(8,128)(2,1)} custom-call(s32[4]{0:T(128)} %pad_add_fusion.ids, bf16[64,768]{1,0:T(8,128)(2,1)} %bitcast.24, bf16[64,768]{1,0:T(8,128)(2,1)} %bitcast.25, f32[1,768]{1,0:T(1,128)} %bitcast.27, bf16[768,512]{1,0:T(8,128)(2,1)} %get-tuple-element.11.after_ref), custom_call_target="tpu_custom_call" | custom-call | bytes 4194304 | tf_op jit(solution)/shard_map/pallas_call | solution.py:71
  63.7 1.3 collective-permute-start.3
  65.0 1.3 collective-permute-start.7
  66.3 9.5 %collective-permute-done.3.refs_5_ = bf16[144,768]{1,0:T(8,128)(2,1)S(1)} collective-permute-done((bf16[144,768]{1,0:T(8,128)(2,1)}, bf16[144,768]{1,0:T(8,128)(2,1)S(1)}, u32[]{:S(2)}, u32[]{:S(2)}) %collective-permute-start.3) | collective-permute-done | bytes 221216 | tf_op jit(solution)/shard_map/ppermute | solution.py:374
  75.8 1.3 collective-permute-start.4
  77.1 1.3 collective-permute-done.7.refs_11_
  78.4 3.3 %collective-permute-start.8 = (bf16[144,768]{1,0:T(8,128)(2,1)S(1)}, bf16[144,768]{1,0:T(8,128)(2,1)S(1)}, u32[]{:S(2)}, u32[]{:S(2)}) collective-permute-start(bf16[144,768]{1,0:T(8,128)(2,1)S(1)} %collective-permute-done.7.refs_11_), channel_id=1, source_target_pairs={{448,384},{0,448},{64,0},{449,385},{1,449},{65,1},{450,386},{2,450... | collective-permute-start | bytes 663560 | tf_op jit(solution)/shard_map/ppermute | solution.py:377
  81.7 3.2 %collective-permute-done.4.refs_6_ = bf16[144,768]{1,0:T(8,128)(2,1)S(1)} collective-permute-done((bf16[144,768]{1,0:T(8,128)(2,1)S(1)}, bf16[144,768]{1,0:T(8,128)(2,1)S(1)}, u32[]{:S(2)}, u32[]{:S(2)}) %collective-permute-start.4) | collective-permute-done | bytes 221216 | tf_op jit(solution)/shard_map/ppermute | solution.py:374
  84.8 1.3 collective-permute-start.5
  86.1 2.2 %collective-permute-done.8.refs_10_ = bf16[144,768]{1,0:T(8,128)(2,1)S(1)} collective-permute-done((bf16[144,768]{1,0:T(8,128)(2,1)S(1)}, bf16[144,768]{1,0:T(8,128)(2,1)S(1)}, u32[]{:S(2)}, u32[]{:S(2)}) %collective-permute-start.8) | collective-permute-done | bytes 221216 | tf_op jit(solution)/shard_map/ppermute | solution.py:377
  88.4 2.3 %collective-permute-start.9 = (bf16[144,768]{1,0:T(8,128)(2,1)S(1)}, bf16[144,768]{1,0:T(8,128)(2,1)S(1)}, u32[]{:S(2)}, u32[]{:S(2)}) collective-permute-start(bf16[144,768]{1,0:T(8,128)(2,1)S(1)} %collective-permute-done.8.refs_10_), channel_id=1, source_target_pairs={{384,320},{448,384},{0,448},{385,321},{449,385},{1,449},{386,322},... | collective-permute-start | bytes 663560 | tf_op jit(solution)/shard_map/ppermute | solution.py:377
  90.7 2.3 %collective-permute-done.5.refs_7_ = bf16[144,768]{1,0:T(8,128)(2,1)S(1)} collective-permute-done((bf16[144,768]{1,0:T(8,128)(2,1)S(1)}, bf16[144,768]{1,0:T(8,128)(2,1)S(1)}, u32[]{:S(2)}, u32[]{:S(2)}) %collective-permute-start.5) | collective-permute-done | bytes 221216 | tf_op jit(solution)/shard_map/ppermute | solution.py:374
  93.0 1.3 collective-permute-start.6
  94.3 0.0 copy-done.18
  94.3 3.0 %collective-permute-start = (bf16[64,768]{1,0:T(8,128)(2,1)S(1)}, bf16[64,768]{1,0:T(8,128)(2,1)}, u32[]{:S(2)}, u32[]{:S(2)}) collective-permute-start(bf16[64,768]{1,0:T(8,128)(2,1)S(1)} %bitcast.31), channel_id=1, source_target_pairs={{16,0},{32,16},{48,32},{0,48},{17,1},{33,17},{49,33},{1,49},{18,2}... | collective-permute-start | bytes 294920 | tf_op jit(solution)/shard_map/ppermute | solution.py:396
  97.4 3.8 %collective-permute-start.1 = (bf16[64,768]{1,0:T(8,128)(2,1)S(1)}, bf16[64,768]{1,0:T(8,128)(2,1)}, u32[]{:S(2)}, u32[]{:S(2)}) collective-permute-start(bf16[64,768]{1,0:T(8,128)(2,1)S(1)} %bitcast.32), channel_id=1, source_target_pairs={{32,0},{48,16},{0,32},{16,48},{33,1},{49,17},{1,33},{17,49},{34,2}... | collective-permute-start | bytes 294920 | tf_op jit(solution)/shard_map/ppermute | solution.py:396
  101.2 4.0 %collective-permute-start.2 = (bf16[64,768]{1,0:T(8,128)(2,1)S(1)}, bf16[64,768]{1,0:T(8,128)(2,1)}, u32[]{:S(2)}, u32[]{:S(2)}) collective-permute-start(bf16[64,768]{1,0:T(8,128)(2,1)S(1)} %bitcast.33), channel_id=1, source_target_pairs={{48,0},{0,16},{16,32},{32,48},{49,1},{1,17},{17,33},{33,49},{50,2}... | collective-permute-start | bytes 294920 | tf_op jit(solution)/shard_map/ppermute | solution.py:396
  105.1 0.0 all-to-all-done.1.part_ref
  105.1 0.0 copy-start.2
  105.2 1.3 copy-done.2
  106.4 3.6 %shard_map.182 = (bf16[768,128]{1,0:T(8,128)(2,1)}, f32[128,128]{1,0:T(8,128)}) custom-call(s32[4]{0:T(128)} %pad_add_fusion.ids, bf16[16,448,128]{2,1,0:T(8,128)(2,1)} %copy-done.2, s32[768,8]{1,0:T(8,128)} %constant.22.clone.table_ref), custom_call_target="tpu_custom_call" | custom-call | flops 1000000000 | bytes 4194304 | tf_op jit(solution)/shard_map/pallas_call | solution.py:71
  110.0 12.5 %all-to-all-start.2 = ((bf16[32,24,128]{2,1,0:T(8,128)(2,1)}), bf16[32,24,128]{2,1,0:T(8,128)(2,1)S(1)}, u32[]{:S(2)}, u32[]{:S(2)}) async-start(bf16[32,24,128]{2,1,0:T(8,128)(2,1)} %bitcast.23), calls=%async_computation.2 | async-start | bytes 393216 | tf_op jit(solution)/shard_map/all_to_all | solution.py:466
  122.5 0.0 copy-start.9
  122.5 0.0 copy-start.10
  122.5 0.0 collective-permute-done.refs_1_
  122.6 0.0 collective-permute-done.1.refs_2_
  122.6 0.0 collective-permute-done.2.refs_3_
  122.6 0.0 collective-permute-done.9.refs_9_
  122.6 0.0 collective-permute-done.6.refs_8_
  122.7 0.6 copy-done.16
  123.3 0.7 copy-done.17
  124.0 31.4 %shard_map.179 = (bf16[768,128]{1,0:T(8,128)(2,1)}, bf16[768,128]{1,0:T(8,128)(2,1)}, bf16[768,128]{1,0:T(8,128)(2,1)}, bf16[768,128]{1,0:T(8,128)(2,1)}) custom-call(s32[4]{0:T(128)} %pad_add_fusion.ids, bf16[64,768]{1,0:T(8,128)(2,1)} %bitcast.30, bf16[64,768]{1,0:T(8,128)(2,1)} %collective-permute-done.refs_1_, ...), custom_call_target="tpu_custom_call" | custom-call | flops 20000000000 | bytes 4194304 | tf_op jit(solution)/shard_map/pallas_call | solution.py:71
  155.4 2.5 %collective-permute-start.10 = (bf16[768,128]{1,0:T(8,128)(2,1)}, bf16[768,128]{1,0:T(8,128)(2,1)S(1)}, u32[]{:S(2)}, u32[]{:S(2)}) collective-permute-start(bf16[768,128]{1,0:T(8,128)(2,1)} %get-tuple-element.14), channel_id=1, source_target_pairs={{0,16},{16,32},{32,48},{48,0},{1,17},{17,33},{33,49},{49,1},{2,18}... | collective-permute-start | bytes 589832 | tf_op jit(solution)/shard_map/ppermute | solution.py:449
  157.9 4.7 %collective-permute-start.11 = (bf16[768,128]{1,0:T(8,128)(2,1)}, bf16[768,128]{1,0:T(8,128)(2,1)S(1)}, u32[]{:S(2)}, u32[]{:S(2)}) collective-permute-start(bf16[768,128]{1,0:T(8,128)(2,1)} %get-tuple-element.15), channel_id=1, source_target_pairs={{0,32},{16,48},{32,0},{48,16},{1,33},{17,49},{33,1},{49,17},{2,34}... | collective-permute-start | bytes 589832 | tf_op jit(solution)/shard_map/ppermute | solution.py:449
  162.6 1.9 %collective-permute-start.12 = (bf16[768,128]{1,0:T(8,128)(2,1)}, bf16[768,128]{1,0:T(8,128)(2,1)S(1)}, u32[]{:S(2)}, u32[]{:S(2)}) collective-permute-start(bf16[768,128]{1,0:T(8,128)(2,1)} %get-tuple-element.16), channel_id=1, source_target_pairs={{0,48},{16,0},{32,16},{48,32},{1,49},{17,1},{33,17},{49,33},{2,50}... | collective-permute-start | bytes 589832 | tf_op jit(solution)/shard_map/ppermute | solution.py:449
  164.6 0.7 copy.19.routes_ref
  165.3 0.7 copy.20.weight_ref
  166.0 0.0 collective-permute-done.10.refs_1_
  166.0 2.6 %collective-permute-done.11.refs_2_ = bf16[768,128]{1,0:T(8,128)(2,1)S(1)} collective-permute-done((bf16[768,128]{1,0:T(8,128)(2,1)}, bf16[768,128]{1,0:T(8,128)(2,1)S(1)}, u32[]{:S(2)}, u32[]{:S(2)}) %collective-permute-start.11) | collective-permute-done | bytes 196640 | tf_op jit(solution)/shard_map/ppermute | solution.py:449
  168.6 2.5 %collective-permute-done.12.refs_3_ = bf16[768,128]{1,0:T(8,128)(2,1)S(1)} collective-permute-done((bf16[768,128]{1,0:T(8,128)(2,1)}, bf16[768,128]{1,0:T(8,128)(2,1)S(1)}, u32[]{:S(2)}, u32[]{:S(2)}) %collective-permute-start.12) | collective-permute-done | bytes 196640 | tf_op jit(solution)/shard_map/ppermute | solution.py:449
  171.1 0.0 copy-done.7
  171.1 0.7 copy-done.8
  171.8 3.8 %shard_map.180 = bf16[64,768]{1,0:T(8,128)(2,1)} custom-call(s32[4]{0:T(128)} %pad_add_fusion.ids, f32[1,64]{1,0:T(1,128)} %bitcast.29, bf16[768,128]{1,0:T(8,128)(2,1)} %get-tuple-element.13.refs_0_, bf16[768,128]{1,0:T(8,128)(2,1)} %copy-done.6, bf16[768,128]{1,0:T(8,128)(2,1)} %copy-done.7, bf16[768,128]{1,0:T(8,128)(2,1)} %copy-done.8), custom_call_target="tpu_custom_call" | custom-call | bytes 4194304 | tf_op jit(solution)/shard_map/pallas_call | solution.py:71
  175.6 0.0 all-to-all-done.2
  175.6 0.7 copy-done.5
  176.3 2.9 %shard_map.183 = bf16[128,128]{1,0:T(8,128)(2,1)} custom-call(s32[4]{0:T(128)} %pad_add_fusion.ids, bf16[768,128]{1,0:T(8,128)(2,1)} %bitcast.22, s32[128,4]{1,0:T(8,128)} %copy.19.routes_ref, f32[128,4]{1,0:T(8,128)} %copy.20.weight_ref, s32[8,768]{1,0:T(8,128)} %constant.28.table_ref, f32[128,128]{1,0:T(8,128)} %get-tuple-element.19.shared_ref), custom_call_target="tpu_custom_call" | custom-call | flops 1000000000 | bytes 4194304 | tf_op jit(solution)/shard_map/pallas_call | solution.py:71
  (24 shorter events, 0.0 us)
Async XLA Ops:
  5.0 25.7 %all-to-all-start = ((bf16[32,24,512]{2,1,0:T(8,128)(2,1)}), bf16[32,24,512]{2,1,0:T(8,128)(2,1)S(1)}, u32[]{:S(2)}, u32[]{:S(2)}) async-start(bf16[32,24,512]{2,1,0:T(8,128)(2,1)} %bitcast.18), calls=%async_computation | async-start | bytes 1572864 | tf_op jit(solution)/shard_map/all_to_all | solution.py:356
  15.8 28.7 %collective-permute-start.15 = (bf16[480,2048]{1,0:T(8,128)(2,1)}, bf16[480,2048]{1,0:T(8,128)(2,1)S(1)}, u32[]{:S(2)}, u32[]{:S(2)}) collective-permute-start(bf16[480,2048]{1,0:T(8,128)(2,1)} %shard_map.177), channel_id=1, source_target_pairs={{0,1},{1,0},{2,3},{3,2},{4,5},{5,4},{6,7},{7,6},{8,9},{9,8},{10,11... | collective-permute-start | bytes 5898248 | tf_op jit(solution)/shard_map/ppermute | solution.py:391
  30.7 13.8 %copy-start = (bf16[32,24,512]{2,1,0:T(8,128)(2,1)}, bf16[32,24,512]{2,1,0:T(8,128)(2,1)S(1)}, u32[]{:S(2)}) copy-start(bf16[32,24,512]{2,1,0:T(8,128)(2,1)S(1)} %all-to-all-done) | copy-start | bytes 2359300
  30.7 12.3 %collective-permute-start.13 = (bf16[384,512]{1,0:T(8,128)(2,1)S(1)}, bf16[384,512]{1,0:T(8,128)(2,1)S(1)}, u32[]{:S(2)}, u32[]{:S(2)}) collective-permute-start(bf16[384,512]{1,0:T(8,128)(2,1)S(1)} %bitcast.21), channel_id=1, source_target_pairs={{0,2},{2,4},{4,6},{6,8},{8,10},{10,12},{12,14},{14,0},{1,3},{3,5},... | collective-permute-start | bytes 1179656 | tf_op jit(solution)/shard_map/ppermute | solution.py:358
  34.2 10.2 %collective-permute-start.14 = (bf16[384,512]{1,0:T(8,128)(2,1)S(1)}, bf16[384,512]{1,0:T(8,128)(2,1)S(1)}, u32[]{:S(2)}, u32[]{:S(2)}) collective-permute-start(bf16[384,512]{1,0:T(8,128)(2,1)S(1)} %bitcast.20), channel_id=1, source_target_pairs={{0,14},{2,0},{4,2},{6,4},{8,6},{10,8},{12,10},{14,12},{1,15},{3,1}... | collective-permute-start | bytes 1179656 | tf_op jit(solution)/shard_map/ppermute | solution.py:359
  43.0 1.5 copy-start.3
  44.5 0.8 copy-start.4
  44.5 1.4 copy-start.1
  53.9 40.4 %copy-start.18 = (bf16[768,64]{0,1:T(8,128)(2,1)S(1)}, bf16[768,64]{0,1:T(8,128)(2,1)}, u32[]{:S(2)}) copy-start(bf16[768,64]{0,1:T(8,128)(2,1)} %param.17) | copy-start | bytes 294916
  53.9 51.3 %all-to-all-start.1 = ((bf16[16,448,128]{2,1,0:T(8,128)(2,1)}), bf16[16,448,128]{2,1,0:T(8,128)(2,1)S(1)}, u32[]{:S(2)}, u32[]{:S(2)}) async-start(bf16[16,448,128]{2,1,0:T(8,128)(2,1)} %shard_map.181), calls=%async_computation.1 | async-start | bytes 3670016 | tf_op jit(solution)/shard_map/all_to_all | solution.py:435
  63.7 12.0 %collective-permute-start.3 = (bf16[144,768]{1,0:T(8,128)(2,1)}, bf16[144,768]{1,0:T(8,128)(2,1)S(1)}, u32[]{:S(2)}, u32[]{:S(2)}) collective-permute-start(bf16[144,768]{1,0:T(8,128)(2,1)} %shard_map.178.refs_4_), channel_id=1, source_target_pairs={{0,64},{64,128},{128,192},{192,256},{256,320},{320,384},{384,448},... | collective-permute-start | bytes 663560 | tf_op jit(solution)/shard_map/ppermute | solution.py:374
  65.0 13.4 %collective-permute-start.7 = (bf16[144,768]{1,0:T(8,128)(2,1)}, bf16[144,768]{1,0:T(8,128)(2,1)S(1)}, u32[]{:S(2)}, u32[]{:S(2)}) collective-permute-start(bf16[144,768]{1,0:T(8,128)(2,1)} %shard_map.178.refs_4_), channel_id=1, source_target_pairs={{0,448},{64,0},{128,64},{1,449},{65,1},{129,65},{2,450},{66,2},{13... | collective-permute-start | bytes 663560 | tf_op jit(solution)/shard_map/ppermute | solution.py:377
  75.8 46.8 %copy-start.11 = (bf16[144,768]{1,0:T(8,128)(2,1)}, bf16[144,768]{1,0:T(8,128)(2,1)S(1)}, u32[]{:S(2)}) copy-start(bf16[144,768]{1,0:T(8,128)(2,1)S(1)} %collective-permute-done.3.refs_5_) | copy-start | bytes 663556
  75.8 9.0 %collective-permute-start.4 = (bf16[144,768]{1,0:T(8,128)(2,1)S(1)}, bf16[144,768]{1,0:T(8,128)(2,1)S(1)}, u32[]{:S(2)}, u32[]{:S(2)}) collective-permute-start(bf16[144,768]{1,0:T(8,128)(2,1)S(1)} %collective-permute-done.3.refs_5_), channel_id=1, source_target_pairs={{64,128},{128,192},{192,256},{256,320},{320,384},{384,448},{65,129... | collective-permute-start | bytes 663560 | tf_op jit(solution)/shard_map/ppermute | solution.py:374
  78.4 44.2 %copy-start.12 = (bf16[144,768]{1,0:T(8,128)(2,1)}, bf16[144,768]{1,0:T(8,128)(2,1)S(1)}, u32[]{:S(2)}) copy-start(bf16[144,768]{1,0:T(8,128)(2,1)S(1)} %collective-permute-done.7.refs_11_) | copy-start | bytes 663556
  78.4 10.0 %collective-permute-start.8 = (bf16[144,768]{1,0:T(8,128)(2,1)S(1)}, bf16[144,768]{1,0:T(8,128)(2,1)S(1)}, u32[]{:S(2)}, u32[]{:S(2)}) collective-permute-start(bf16[144,768]{1,0:T(8,128)(2,1)S(1)} %collective-permute-done.7.refs_11_), channel_id=1, source_target_pairs={{448,384},{0,448},{64,0},{449,385},{1,449},{65,1},{450,386},{2,450... | collective-permute-start | bytes 663560 | tf_op jit(solution)/shard_map/ppermute | solution.py:377
  84.8 37.8 %copy-start.13 = (bf16[144,768]{1,0:T(8,128)(2,1)}, bf16[144,768]{1,0:T(8,128)(2,1)S(1)}, u32[]{:S(2)}) copy-start(bf16[144,768]{1,0:T(8,128)(2,1)S(1)} %collective-permute-done.4.refs_6_) | copy-start | bytes 663556
  84.8 8.2 %collective-permute-start.5 = (bf16[144,768]{1,0:T(8,128)(2,1)S(1)}, bf16[144,768]{1,0:T(8,128)(2,1)S(1)}, u32[]{:S(2)}, u32[]{:S(2)}) collective-permute-start(bf16[144,768]{1,0:T(8,128)(2,1)S(1)} %collective-permute-done.4.refs_6_), channel_id=1, source_target_pairs={{128,192},{192,256},{256,320},{320,384},{384,448},{129,193},{193,2... | collective-permute-start | bytes 663560 | tf_op jit(solution)/shard_map/ppermute | solution.py:374
  88.4 34.3 %copy-start.14 = (bf16[144,768]{1,0:T(8,128)(2,1)}, bf16[144,768]{1,0:T(8,128)(2,1)S(1)}, u32[]{:S(2)}) copy-start(bf16[144,768]{1,0:T(8,128)(2,1)S(1)} %collective-permute-done.8.refs_10_) | copy-start | bytes 663556
  88.4 34.2 %collective-permute-start.9 = (bf16[144,768]{1,0:T(8,128)(2,1)S(1)}, bf16[144,768]{1,0:T(8,128)(2,1)S(1)}, u32[]{:S(2)}, u32[]{:S(2)}) collective-permute-start(bf16[144,768]{1,0:T(8,128)(2,1)S(1)} %collective-permute-done.8.refs_10_), channel_id=1, source_target_pairs={{384,320},{448,384},{0,448},{385,321},{449,385},{1,449},{386,322},... | collective-permute-start | bytes 663560 | tf_op jit(solution)/shard_map/ppermute | solution.py:377
  93.0 29.6 %copy-start.15 = (bf16[144,768]{1,0:T(8,128)(2,1)}, bf16[144,768]{1,0:T(8,128)(2,1)S(1)}, u32[]{:S(2)}) copy-start(bf16[144,768]{1,0:T(8,128)(2,1)S(1)} %collective-permute-done.5.refs_7_) | copy-start | bytes 663556
  93.0 29.6 %collective-permute-start.6 = (bf16[144,768]{1,0:T(8,128)(2,1)S(1)}, bf16[144,768]{1,0:T(8,128)(2,1)S(1)}, u32[]{:S(2)}, u32[]{:S(2)}) collective-permute-start(bf16[144,768]{1,0:T(8,128)(2,1)S(1)} %collective-permute-done.5.refs_7_), channel_id=1, source_target_pairs={{192,256},{256,320},{320,384},{384,448},{193,257},{257,321},{321,3... | collective-permute-start | bytes 663560 | tf_op jit(solution)/shard_map/ppermute | solution.py:374
  94.3 28.2 %collective-permute-start = (bf16[64,768]{1,0:T(8,128)(2,1)S(1)}, bf16[64,768]{1,0:T(8,128)(2,1)}, u32[]{:S(2)}, u32[]{:S(2)}) collective-permute-start(bf16[64,768]{1,0:T(8,128)(2,1)S(1)} %bitcast.31), channel_id=1, source_target_pairs={{16,0},{32,16},{48,32},{0,48},{17,1},{33,17},{49,33},{1,49},{18,2}... | collective-permute-start | bytes 294920 | tf_op jit(solution)/shard_map/ppermute | solution.py:396
  97.4 25.2 %collective-permute-start.1 = (bf16[64,768]{1,0:T(8,128)(2,1)S(1)}, bf16[64,768]{1,0:T(8,128)(2,1)}, u32[]{:S(2)}, u32[]{:S(2)}) collective-permute-start(bf16[64,768]{1,0:T(8,128)(2,1)S(1)} %bitcast.32), channel_id=1, source_target_pairs={{32,0},{48,16},{0,32},{16,48},{33,1},{49,17},{1,33},{17,49},{34,2}... | collective-permute-start | bytes 294920 | tf_op jit(solution)/shard_map/ppermute | solution.py:396
  101.2 21.4 %collective-permute-start.2 = (bf16[64,768]{1,0:T(8,128)(2,1)S(1)}, bf16[64,768]{1,0:T(8,128)(2,1)}, u32[]{:S(2)}, u32[]{:S(2)}) collective-permute-start(bf16[64,768]{1,0:T(8,128)(2,1)S(1)} %bitcast.33), channel_id=1, source_target_pairs={{48,0},{0,16},{16,32},{32,48},{49,1},{1,17},{17,33},{33,49},{50,2}... | collective-permute-start | bytes 294920 | tf_op jit(solution)/shard_map/ppermute | solution.py:396
  105.1 1.3 copy-start.2
  110.0 65.6 %all-to-all-start.2 = ((bf16[32,24,128]{2,1,0:T(8,128)(2,1)}), bf16[32,24,128]{2,1,0:T(8,128)(2,1)S(1)}, u32[]{:S(2)}, u32[]{:S(2)}) async-start(bf16[32,24,128]{2,1,0:T(8,128)(2,1)} %bitcast.23), calls=%async_computation.2 | async-start | bytes 393216 | tf_op jit(solution)/shard_map/all_to_all | solution.py:466
  122.5 42.0 %copy-start.9 = (s32[128,4]{0,1:T(4,128)S(1)}, s32[128,4]{0,1:T(4,128)}, u32[]{:S(2)}) copy-start(s32[128,4]{0,1:T(4,128)} %param.24) | copy-start | bytes 6148
  122.5 42.8 %copy-start.10 = (f32[128,4]{0,1:T(4,128)S(1)}, f32[128,4]{0,1:T(4,128)}, u32[]{:S(2)}) copy-start(f32[128,4]{0,1:T(4,128)} %param.25) | copy-start | bytes 6148
  122.6 0.7 copy-start.16
  123.3 0.7 copy-start.17
  155.4 10.7 %collective-permute-start.10 = (bf16[768,128]{1,0:T(8,128)(2,1)}, bf16[768,128]{1,0:T(8,128)(2,1)S(1)}, u32[]{:S(2)}, u32[]{:S(2)}) collective-permute-start(bf16[768,128]{1,0:T(8,128)(2,1)} %get-tuple-element.14), channel_id=1, source_target_pairs={{0,16},{16,32},{32,48},{48,0},{1,17},{17,33},{33,49},{49,1},{2,18}... | collective-permute-start | bytes 589832 | tf_op jit(solution)/shard_map/ppermute | solution.py:449
  157.9 10.7 %collective-permute-start.11 = (bf16[768,128]{1,0:T(8,128)(2,1)}, bf16[768,128]{1,0:T(8,128)(2,1)S(1)}, u32[]{:S(2)}, u32[]{:S(2)}) collective-permute-start(bf16[768,128]{1,0:T(8,128)(2,1)} %get-tuple-element.15), channel_id=1, source_target_pairs={{0,32},{16,48},{32,0},{48,16},{1,33},{17,49},{33,1},{49,17},{2,34}... | collective-permute-start | bytes 589832 | tf_op jit(solution)/shard_map/ppermute | solution.py:449
  162.6 8.5 %collective-permute-start.12 = (bf16[768,128]{1,0:T(8,128)(2,1)}, bf16[768,128]{1,0:T(8,128)(2,1)S(1)}, u32[]{:S(2)}, u32[]{:S(2)}) collective-permute-start(bf16[768,128]{1,0:T(8,128)(2,1)} %get-tuple-element.16), channel_id=1, source_target_pairs={{0,48},{16,0},{32,16},{48,32},{1,49},{17,1},{33,17},{49,33},{2,50}... | collective-permute-start | bytes 589832 | tf_op jit(solution)/shard_map/ppermute | solution.py:449
  166.0 5.1 %copy-start.6 = (bf16[768,128]{1,0:T(8,128)(2,1)}, bf16[768,128]{1,0:T(8,128)(2,1)S(1)}, u32[]{:S(2)}) copy-start(bf16[768,128]{1,0:T(8,128)(2,1)S(1)} %collective-permute-done.10.refs_1_) | copy-start | bytes 589828
  168.6 2.5 %copy-start.7 = (bf16[768,128]{1,0:T(8,128)(2,1)}, bf16[768,128]{1,0:T(8,128)(2,1)S(1)}, u32[]{:S(2)}) copy-start(bf16[768,128]{1,0:T(8,128)(2,1)S(1)} %collective-permute-done.11.refs_2_) | copy-start | bytes 589828
  171.1 0.7 copy-start.8
  175.6 0.7 copy-start.5
